TPU v7x, 512 devices: a whole 4x4x16 slice. The times are simulated.
512 devices in a mesh: sp: 64 (over z, y), tp: 8 (over x, core).
Axes of the slice: x: 4, y: 4, z: 16, core: 2. Of those that a mesh axis runs over, the one named last changes fastest.
Arguments:
- tokens: bfloat16 [8192, 2048], P('sp'), may hold values from -6 to 6
- input_norm_scale: float32 [2048], replicated, may hold values from 0.1 to 1.9
- input_norm_bias: float32 [2048], replicated, may hold values from -2 to 2
- query_projection: bfloat16 [2048, 1024], P('sp', 'tp'), may hold values from -0.125 to 0.125
- key_projection: bfloat16 [2048, 1024], P('sp', 'tp'), may hold values from -0.125 to 0.125
- value_projection: bfloat16 [2048, 1024], P('sp', 'tp'), may hold values from -0.125 to 0.125
- pooling_input_projection: bfloat16 [2048, 1024], P('sp', 'tp'), may hold values from -0.125 to 0.125
- decay_input_weight: bfloat16 [2048, 128], P('sp'), may hold values from -0.125 to 0.125
- rate_input_weight: bfloat16 [2048, 128], P('sp'), may hold values from -0.125 to 0.125
- gate_input_weight: bfloat16 [2048, 256], P('sp'), may hold values from -0.125 to 0.125
- decay_output_weight: bfloat16 [128, 1024], P(None, 'tp'), may hold values from -0.5 to 0.5
- rate_output_weight: bfloat16 [128, 1024], P(None, 'tp'), may hold values from -0.5 to 0.5
- gate_output_weight: bfloat16 [256, 1024], P(None, 'tp'), may hold values from -0.375 to 0.375
- decay_bias_base: float32 [1024], P('tp'), may hold values from -13 to -2.5
- learning_rate_base: float32 [1024], P('tp'), may hold values from -4 to 4
- key_prenorm_scale: float32 [1024], P('tp'), may hold values from 0.1 to 1.9
- key_learning_scale: float32 [1024], P('tp'), may hold values from 0.1 to 1.9
- self_term_weight: float32 [1024], P('tp'), may hold values from -3 to 3
- head_norm_scale: float32 [1024], P('tp'), may hold values from 0.1 to 1.9
- head_norm_bias: float32 [1024], P('tp'), may hold values from -3 to 3
- rate_extra_log: float32 [8192, 1024], P('sp', 'tp'), may hold values from -0.7 to 0.7
- decay_extra_log: float32 [8192, 1024], P('sp', 'tp'), may hold values from -0.7 to 0
- starting_head_state: float32 [16, 64, 64], P('tp'), may hold values from -12 to 12
- pooling_group_matrix: bfloat16 [8, 128, 128], P('tp'), may hold values from -0.5 to 0.5
- pooling_output_scale: float32 [1024], P('tp'), may hold values from 0.1 to 1.9
- output_attention_rows: bfloat16 [1024, 2048], P('tp', 'sp'), may hold values from -0.125 to 0.125
- output_pooling_rows: bfloat16 [1024, 2048], P('tp', 'sp'), may hold values from -0.125 to 0.125
Outputs:
- mixed: bfloat16 [8192, 2048], P(('sp', 'tp'))
All inputs are finite; a program needn't handle non-finite values.
Results may differ from a plain program's by a relative error of at most 0.019.
Values may be sent and summed in bfloat16 or wider, within the bound.
No kernel may reach another device: no remote copies, remote signals or barrier semaphores. Data moves between devices by JAX's collectives and lax.ppermute only.
A program may use at most 64 MiB of HBM per device.

v0:
```python
import math

import jax
import jax.numpy as jnp
from jax import lax
from jax.sharding import Mesh
from jax.sharding import PartitionSpec as P

HEAD_CHANNELS = 64
POOL_GROUPS = 8
POOL_GROUP = 128
SP = ("sp_0", "sp_1")
SP_TP = ("sp_0", "sp_1", "tp")


pool_windows = (2, 4, 8, 16)
pool_reach = 16
span_most = 64


def side_by_side(arrays, axis, dim, along):
    ends, at = ([], 0)
    for a in arrays[:-1]:
        at += a.shape[along]
        ends.append(at)
    both = jnp.concatenate(arrays, axis=along)
    return tuple(jnp.split(lax.all_gather(both, axis, axis=dim, tiled=True), ends, axis=along))


def nothing_yet(x, identity):
    return jax.tree.map(
        lambda a, e: jnp.broadcast_to(jnp.asarray(e, a.dtype), a.shape), x, identity
    )


def gathered_once(x, axis):
    leaves = jax.tree.leaves(x)
    sequence = sorted(range(len(leaves)), key=lambda k: -leaves[k].size)
    width = (1, *leaves[sequence[0]].shape)[-1]
    lines = [
        jnp.pad(leaves[k].reshape(-1), (0, -leaves[k].size % width)).reshape(-1, width)
        for k in sequence
    ]
    both, at, found = (lax.all_gather(jnp.concatenate(lines), axis), 0, {})
    for k, line in zip(sequence, lines):
        piece = both[:, at : at + len(line)].reshape(len(both), -1)
        found[k] = piece[:, : leaves[k].size].reshape(-1, *leaves[k].shape)
        at += len(line)
    numbers = iter(range(len(leaves)))
    return jax.tree.map(lambda _: found[next(numbers)], x)


def prefix_by_axis(x, axes, combine, identity):
    before = start = nothing_yet(x, identity)
    running = x
    for axis in reversed(axes):
        peers, mine = (lax.axis_size(axis), lax.axis_index(axis))
        pieces = gathered_once(
            jax.tree.map(
                lambda part, kind: part.astype(kind), running, (jnp.bfloat16, jnp.bfloat16)
            ),
            axis,
        )
        inside, running = (start, start)
        for k in range(peers):
            passed = k < mine
            running = combine(
                running, jax.tree.map(lambda part, own: part[k].astype(own.dtype), pieces, x)
            )
            inside = jax.tree.map(lambda new, old: jnp.where(passed, new, old), running, inside)
        before = combine(inside, before)
    return before


def passed_along(value, axis, steps):
    count = lax.axis_size(axis)
    leading, last = (max(0, -steps), min(count, count - steps))
    return lax.ppermute(value, axis, [(source, source + steps) for source in range(leading, last)])


def gather_turned(arrays, axis, dims):
    turned = [jnp.moveaxis(a, dim, 0) for a, dim in zip(arrays, dims)]
    both = jnp.concatenate([t.reshape(len(t), -1) for t in turned], axis=1)
    result, at, gathered = (lax.all_gather(both, axis, axis=0, tiled=True), 0, [])
    for t, dim in zip(turned, dims):
        piece = result[:, at : at + t[0].size].reshape(-1, *t.shape[1:])
        gathered.append(jnp.moveaxis(piece, 0, dim))
        at += t[0].size
    return tuple(gathered)


def split_up(x, dim, peers):
    before, after = (x.shape[:dim], x.shape[dim + 1 :])
    return jnp.moveaxis(x.reshape(*before, peers, -1, *after), dim, 0)


def sent_and_summed(x, axis, dim):
    peers = lax.axis_size(axis)
    parts = lax.all_to_all(split_up(x, dim, peers), axis, 0, 0, tiled=True)
    return jnp.sum(parts.astype(jnp.float32), axis=0)


def compose(earlier, later):
    joined_map = jnp.einsum("hij,hjk->hik", earlier[0], later[0])
    joined_state = jnp.einsum("hij,hjk->hik", earlier[1], later[0]) + later[1]
    return (joined_map, joined_state)


def block_recurrence(carry, inputs):
    run_local, run_map = carry
    recv, decay_logarithm, key_t, value_t, alpha_t, beta_t = inputs
    span_len = recv.shape[1]
    total = jnp.cumsum(decay_logarithm, axis=1)
    before = total - decay_logarithm
    rows = jnp.arange(span_len, dtype=jnp.int32)[:, None]
    cols = jnp.arange(span_len, dtype=jnp.int32)[None, :]
    strict = (rows > cols)[None, :, :, None]
    upto = (rows >= cols)[None, :, :, None]
    weight_before = jnp.exp(
        jnp.where(strict, before[:, :, None, :] - total[:, None, :, :], -jnp.inf)
    )
    weight_now = jnp.exp(jnp.where(upto, total[:, :, None, :] - total[:, None, :, :], -jnp.inf))
    lower_a = jnp.einsum("htk,hsk,htsk->hts", alpha_t, beta_t, weight_before)
    lower_b = jnp.einsum("htk,hsk,htsk->hts", alpha_t, key_t, weight_before)
    read_b = jnp.einsum("htk,hsk,htsk->hts", recv, beta_t, weight_now)
    read_k = jnp.einsum("htk,hsk,htsk->hts", recv, key_t, weight_now)
    system = jnp.eye(span_len, dtype=jnp.float32)[None] - lower_a
    a_hat = alpha_t * jnp.exp(before)
    r_hat = recv * jnp.exp(total)
    w_part = jax.scipy.linalg.solve_triangular(system, a_hat, lower=True, unit_diagonal=True)
    u_right = jnp.einsum("hts,hsv->htv", lower_b, value_t)
    u_part = jax.scipy.linalg.solve_triangular(system, u_right, lower=True, unit_diagonal=True)
    y_map = r_hat + jnp.einsum("hts,hsk->htk", read_b, w_part)
    y_local = jnp.einsum("hts,hsv->htv", read_b, u_part) + jnp.einsum(
        "hts,hsv->htv", read_k, value_t
    )
    end_decay = jnp.exp(total[:, -1:, :] - total)
    beta_end = beta_t * end_decay
    key_end = key_t * end_decay
    last_decay = jnp.exp(total[:, -1, :])
    map_block = jnp.eye(last_decay.shape[1], dtype=jnp.float32)[None] * last_decay[
        :, None, :
    ] + jnp.einsum("hsi,hsk->hik", w_part, beta_end)
    local_block = jnp.einsum("hsv,hsk->hvk", u_part, beta_end) + jnp.einsum(
        "hsv,hsk->hvk", value_t, key_end
    )
    out_local = y_local + jnp.einsum("hvk,htk->htv", run_local, y_map)
    out_map = jnp.einsum("hjk,htk->htj", run_map, y_map)
    new_local = jnp.einsum("hvj,hjk->hvk", run_local, map_block) + local_block
    new_map = jnp.einsum("hij,hjk->hik", run_map, map_block)
    return ((new_local, new_map), (out_local, out_map))


def window_width(scale_index):
    result = jnp.zeros(scale_index.shape, jnp.float32)
    for level, width in enumerate(pool_windows):
        result = jnp.where(scale_index == level, jnp.float32(width), result)
    return result


def window_sums(extended, scale_index, row_total):
    running = jnp.zeros((row_total, extended.shape[1]), jnp.float32)
    chosen = jnp.zeros((row_total, extended.shape[1]), jnp.float32)
    for offset in range(pool_reach):
        running = running + extended[pool_reach - offset : pool_reach - offset + row_total]
        for level, width in enumerate(pool_windows):
            if offset + 1 == width:
                chosen = jnp.where(scale_index[None, :] == level, running, chosen)
    return chosen


def on_device(
    tokens,
    input_norm_scale,
    input_norm_bias,
    query_projection,
    key_projection,
    value_projection,
    pooling_input_projection,
    decay_input_weight,
    rate_input_weight,
    gate_input_weight,
    decay_output_weight,
    rate_output_weight,
    gate_output_weight,
    decay_bias_base,
    learning_rate_base,
    key_prenorm_scale,
    key_learning_scale,
    self_term_weight,
    head_norm_scale,
    head_norm_bias,
    rate_extra_log,
    decay_extra_log,
    starting_head_state,
    pooling_group_matrix,
    pooling_output_scale,
    output_attention_rows,
    output_pooling_rows,
):
    f32 = jnp.float32
    bf16 = jnp.bfloat16
    row_total = tokens.shape[0]
    wide = tokens.astype(f32)
    center = jnp.mean(wide, axis=-1, keepdims=True)
    spread = jnp.mean(jnp.square(wide - center), axis=-1, keepdims=True)
    normed = (
        (wide - center) * lax.rsqrt(spread + 1e-05) * input_norm_scale + input_norm_bias
    ).astype(bf16)
    pieces = side_by_side(
        (
            query_projection,
            key_projection,
            value_projection,
            pooling_input_projection,
            decay_input_weight,
            rate_input_weight,
            gate_input_weight,
        ),
        SP,
        0,
        1,
    )
    totals = tuple((jnp.dot(normed, piece, preferred_element_type=f32) for piece in pieces))
    rounded = [total.astype(bf16) for total in totals]
    decay_low, rate_low, gate_low = (rounded[4], rounded[5], rounded[6])
    recept, keys, values, pool_in = (rounded[0], rounded[1], rounded[2], rounded[3])
    decay_tanh = jnp.tanh(decay_low.astype(f32)).astype(bf16)
    gate_sig = jax.nn.sigmoid(gate_low.astype(f32)).astype(bf16)
    rate_logarithm = (
        -jax.nn.softplus(
            -(
                decay_bias_base
                + jnp.dot(decay_tanh, decay_output_weight, preferred_element_type=f32)
            )
        )
        - 0.5
        + rate_extra_log
    )
    decay_logarithm = -jnp.exp(rate_logarithm) + decay_extra_log
    rate = jax.nn.sigmoid(
        learning_rate_base + jnp.dot(rate_low, rate_output_weight, preferred_element_type=f32)
    )
    gate = jnp.dot(gate_sig, gate_output_weight, preferred_element_type=f32)
    mix_width = recept.shape[1]
    heads_dev = mix_width // HEAD_CHANNELS

    def head_number(array):
        return array.astype(f32).reshape(row_total, heads_dev, HEAD_CHANNELS)

    def channel_heads(vector):
        return vector.reshape(heads_dev, HEAD_CHANNELS)

    key_wide = keys.astype(f32)
    unit = head_number(key_wide * key_prenorm_scale)
    unit = unit * lax.rsqrt(jnp.sum(unit * unit, axis=-1, keepdims=True) + 1e-06)
    effective_key = head_number(key_wide * (1.0 + (rate - 1.0) * key_learning_scale))
    query_per_head, value_per_head = (head_number(recept), head_number(values))
    span_len = math.gcd(span_most, row_total)
    block_count = row_total // span_len

    def blocked(array):
        return array.reshape(block_count, span_len, heads_dev, HEAD_CHANNELS).transpose(0, 2, 1, 3)

    def unblocked(array):
        return array.transpose(0, 2, 1, 3).reshape(row_total, heads_dev, HEAD_CHANNELS)

    identity_map = jnp.broadcast_to(
        jnp.eye(HEAD_CHANNELS, dtype=f32), (heads_dev, HEAD_CHANNELS, HEAD_CHANNELS)
    )
    zero_state = jnp.zeros((heads_dev, HEAD_CHANNELS, HEAD_CHANNELS), f32)
    final, outputs = lax.scan(
        block_recurrence,
        (zero_state, identity_map),
        (
            blocked(query_per_head),
            blocked(head_number(decay_logarithm)),
            blocked(effective_key),
            blocked(value_per_head),
            blocked(-unit),
            blocked(unit * head_number(rate)),
        ),
    )
    local_state, block_map = final
    read_local = unblocked(outputs[0])
    read_map = unblocked(outputs[1])
    prior_map, prior_state = prefix_by_axis(
        (block_map, local_state), SP, compose, (identity_map, zero_state)
    )
    entry = jnp.einsum("hvj,hjk->hvk", starting_head_state, prior_map) + prior_state
    reading = read_local + jnp.einsum("hvk,thk->thv", entry, read_map)
    center_h = jnp.mean(reading, axis=-1, keepdims=True)
    spread_h = jnp.mean(jnp.square(reading - center_h), axis=-1, keepdims=True)
    split_by_head = (reading - center_h) * lax.rsqrt(
        spread_h + 1e-05 * HEAD_CHANNELS
    ) * channel_heads(head_norm_scale) + channel_heads(head_norm_bias)
    split_by_head = (
        split_by_head
        + jnp.sum(
            query_per_head * effective_key * channel_heads(self_term_weight), axis=-1, keepdims=True
        )
        * value_per_head
    )
    attn_out = (split_by_head.reshape(row_total, mix_width) * gate).astype(bf16)
    pool_width_dev = pool_in.shape[1]
    groups_dev = pool_width_dev // POOL_GROUP
    previous = passed_along(pool_in[row_total - pool_reach :], SP, 1)
    extended = jnp.concatenate([previous, pool_in], axis=0).astype(f32)
    group_ids = (
        lax.axis_index("tp") * groups_dev
        + jnp.arange(pool_width_dev, dtype=jnp.int32) // POOL_GROUP
    )
    scale_index = group_ids // (POOL_GROUPS // 4)
    chosen = window_sums(extended, scale_index, row_total)
    position = (lax.axis_index(SP) * row_total + jnp.arange(row_total, dtype=jnp.int32)).astype(f32)
    counted = jnp.minimum(position[:, None] + 1.0, window_width(scale_index)[None, :])
    pooled = (chosen / counted - pool_in.astype(f32)).astype(bf16)
    grouped = jnp.einsum(
        "tgc,gcd->tgd",
        pooled.reshape(row_total, groups_dev, POOL_GROUP),
        pooling_group_matrix,
        preferred_element_type=f32,
    )
    pool_out = (grouped.reshape(row_total, pool_width_dev) * pooling_output_scale).astype(bf16)
    mix_columns, pool_columns = gather_turned(
        (output_attention_rows, output_pooling_rows), SP, (1, 1)
    )
    mixed = sent_and_summed(
        (
            jnp.dot(attn_out, mix_columns, preferred_element_type=f32)
            + jnp.dot(pool_out, pool_columns, preferred_element_type=f32)
        ).astype(jnp.bfloat16),
        "tp",
        0,
    )
    return mixed.astype(bf16)


def solution(mesh):
    split = Mesh(mesh.devices.reshape(16, 4, mesh.shape["tp"]), ("sp_0", "sp_1", "tp"))
    in_specs = (
        P(SP, None),
        P(),
        P(),
        P(SP, "tp"),
        P(SP, "tp"),
        P(SP, "tp"),
        P(SP, "tp"),
        P(SP, None),
        P(SP, None),
        P(SP, None),
        P(None, "tp"),
        P(None, "tp"),
        P(None, "tp"),
        P("tp"),
        P("tp"),
        P("tp"),
        P("tp"),
        P("tp"),
        P("tp"),
        P("tp"),
        P(SP, "tp"),
        P(SP, "tp"),
        P("tp", None, None),
        P("tp", None, None),
        P("tp"),
        P("tp", SP),
        P("tp", SP),
    )
    out_specs = P(SP_TP, None)
    return jax.shard_map(
        on_device, mesh=split, in_specs=in_specs, out_specs=out_specs, check_vma=False
    )
```

profile of v0, /device:TPU:1, one launch (start us, length us, event | category | flops | bytes accessed | tf_op | source)
XLA Modules:
  0.0 327.1 jit_solution(14291199337088816337)
XLA Ops:
  6.6 0.8 constant_dynamic-update-slice_fusion.6
  7.4 0.7 constant_dynamic-update-slice_fusion.5
  8.1 0.7 constant_dynamic-update-slice_fusion.4
  8.8 0.7 constant_dynamic-update-slice_fusion.3
  9.5 0.7 constant_dynamic-update-slice_fusion.2
  10.2 0.7 constant_dynamic-update-slice_fusion.1
  10.9 0.7 constant_dynamic-update-slice_fusion
  11.6 0.6 copy-done.1
  12.3 1.3 pad_maximum_fusion.2
  13.8 1.2 convert_reduce_fusion
  15.0 1.3 fusion.73
  16.4 0.7 add.354
  17.2 0.7 mul.159
  17.9 0.7 mul.164
  18.7 1.5 fusion.76
  20.1 134.5 %all-gather.5.cloned.1.call-done = bf16[2048,1024]{1,0:T(8,128)(2,1)} async-done(((bf16[32,1024]{1,0:T(8,128)(2,1)}), bf16[2048,1024]{1,0:T(8,128)(2,1)}) %all-gather.5.cloned.1.call-update) | async-done | bytes 4194320 | tf_op jit(solution)/shard_map/all_gather | solution.py:27
  154.7 1.4 bitcast_reduce_fusion
  156.4 1.5 fusion.63
  158.2 1.5 fusion.95
  159.8 1.4 fusion.203
  161.7 1.4 fusion.68
  163.4 67.9 %while.17 = (s32[]{:T(128)}, bf16[2,64,64]{1,2,0:T(8,128)(2,1)S(1)}, bf16[2,64,64]{1,2,0:T(8,128)(2,1)S(1)}, f32[2,2,64,64]{3,2,1,0:T(8,128)S(1)}, bf16[2,2,64,6...) while((s32[]{:T(128)}, ...), condition=%wide.region_5.7_spmd.clone, body=%wide.region_3.6_spmd.clone.sunk | while | flops 33214532 | bytes 19938492 | solution.py:272
  163.6 4.2 %select_exponential_fusion.3 = (f32[2,64,64,64]{3,2,1,0:T(8,128)}, f32[2,64,64,64]{3,2,1,0:T(8,128)}) fusion(f32[2,64,64]{2,1,0:T(8,128)S(1)} %reduce_window_sum.13, pred[64,64]{1,0:T(8,128)(4,1)S(1)} %get-tuple-element.309, f32[2,64,64]{2,1,0:T(8,128)S(1)} %sub.226, pred[64,64]{1,0:T(8,128)(4,1)S(1)} %get-tuple-element.310), kind=kLoop, calls=%fused_computation.8.clone.1 | loop fusion | flops 2097152 | bytes 4268032 | tf_op jit(solution)/shard_map/while/body/eval_jaxpr/exp | solution.py:122
  167.8 5.6 %copy.144 = f32[2,64,64,64]{1,2,3,0:T(8,128)} copy(f32[2,64,64,64]{3,2,1,0:T(8,128)} %get-tuple-element.311) | data formatting | bytes 4194304 | tf_op jit(solution)/shard_map/while
  173.4 5.6 %copy.148 = f32[2,64,64,64]{1,2,3,0:T(8,128)} copy(f32[2,64,64,64]{3,2,1,0:T(8,128)} %get-tuple-element.314) | data formatting | bytes 4194304 | tf_op jit(solution)/shard_map/while
  179.4 5.1 %fusion.393 = (bf16[2,64,64]{1,2,0:T(8,128)(2,1)S(1)}, f32[2,64,64]{1,2,0:T(8,128)S(1)}, bf16[2,64,64]{1,2,0:T(8,128)(2,1)S(1)}, bf16[2,64,64]{1,2,0:T(8,128)(2,1)S(1)}) fusion(f32[2,64,64,64]{1,2,3,0:T(8,128)} %copy.144, f32[2,64,64]{2,1,0:T(8,128)S(1)} %copy.145, f32[2,64,64]{2,1,0:T(8,128)S(1)} %copy.146, f32[2,64,64]{2,1,0:T(8,128)S(1)} %copy.147, ...), kind=kLoop, calls=%fused_computation.5.clone.1 | loop fusion | flops 6258688 | bytes 4407296 | tf_op jit(solution)/shard_map/while/body/eval_jaxpr/htk,hsk,htsk->hts/dot_general | solution.py:124
  184.7 9.9 %custom-call.12 = f32[2,1,64,64]{2,3,1,0:T(8,128)S(1)} custom-call(f32[2,1,64,64]{3,2,1,0:T(8,128)S(1)} %add_bitcast_fusion.2), custom_call_target="InvertDiagBlocksLowerTriangular" | custom-call | tf_op jit(solution)/shard_map/while/body/eval_jaxpr/jit(_solve_triangular)/vmap()/triangular_solve | solution.py:130
  194.6 0.2 fusion.397
  194.8 0.3 fusion.398
  195.1 0.2 fusion.399
  195.3 0.3 fusion.395
  195.6 0.2 convolution_add_fusion.32
  195.8 0.2 convolution_bitcast_fusion.7
  196.0 0.2 convolution_add_fusion.34
  196.4 0.2 convolution_add_fusion.33
  196.8 0.2 fusion.400
  197.5 4.2 %select_exponential_fusion.3 = (f32[2,64,64,64]{3,2,1,0:T(8,128)}, f32[2,64,64,64]{3,2,1,0:T(8,128)}) fusion(f32[2,64,64]{2,1,0:T(8,128)S(1)} %reduce_window_sum.13, pred[64,64]{1,0:T(8,128)(4,1)S(1)} %get-tuple-element.309, f32[2,64,64]{2,1,0:T(8,128)S(1)} %sub.226, pred[64,64]{1,0:T(8,128)(4,1)S(1)} %get-tuple-element.310), kind=kLoop, calls=%fused_computation.8.clone.1 | loop fusion | flops 2097152 | bytes 4268032 | tf_op jit(solution)/shard_map/while/body/eval_jaxpr/exp | solution.py:122
  201.7 5.6 %copy.144 = f32[2,64,64,64]{1,2,3,0:T(8,128)} copy(f32[2,64,64,64]{3,2,1,0:T(8,128)} %get-tuple-element.311) | data formatting | bytes 4194304 | tf_op jit(solution)/shard_map/while
  207.3 5.6 %copy.148 = f32[2,64,64,64]{1,2,3,0:T(8,128)} copy(f32[2,64,64,64]{3,2,1,0:T(8,128)} %get-tuple-element.314) | data formatting | bytes 4194304 | tf_op jit(solution)/shard_map/while
  213.3 5.1 %fusion.393 = (bf16[2,64,64]{1,2,0:T(8,128)(2,1)S(1)}, f32[2,64,64]{1,2,0:T(8,128)S(1)}, bf16[2,64,64]{1,2,0:T(8,128)(2,1)S(1)}, bf16[2,64,64]{1,2,0:T(8,128)(2,1)S(1)}) fusion(f32[2,64,64,64]{1,2,3,0:T(8,128)} %copy.144, f32[2,64,64]{2,1,0:T(8,128)S(1)} %copy.145, f32[2,64,64]{2,1,0:T(8,128)S(1)} %copy.146, f32[2,64,64]{2,1,0:T(8,128)S(1)} %copy.147, ...), kind=kLoop, calls=%fused_computation.5.clone.1 | loop fusion | flops 6258688 | bytes 4407296 | tf_op jit(solution)/shard_map/while/body/eval_jaxpr/htk,hsk,htsk->hts/dot_general | solution.py:124
  218.7 9.8 %custom-call.12 = f32[2,1,64,64]{2,3,1,0:T(8,128)S(1)} custom-call(f32[2,1,64,64]{3,2,1,0:T(8,128)S(1)} %add_bitcast_fusion.2), custom_call_target="InvertDiagBlocksLowerTriangular" | custom-call | tf_op jit(solution)/shard_map/while/body/eval_jaxpr/jit(_solve_triangular)/vmap()/triangular_solve | solution.py:130
  228.5 0.2 fusion.397
  228.7 0.3 fusion.398
  229.0 0.2 fusion.399
  229.3 0.3 fusion.395
  229.6 0.2 convolution_add_fusion.32
  229.8 0.2 convolution_bitcast_fusion.7
  230.0 0.2 convolution_add_fusion.34
  230.4 0.2 convolution_add_fusion.33
  230.7 0.2 fusion.400
  231.6 9.1 %all-gather = bf16[1024,64]{0,1:T(8,128)(2,1)S(1)} all-gather(bf16[256,64]{0,1:T(8,128)(2,1)S(1)} %pad_maximum_fusion.1), channel_id=2, replica_groups=mesh['sp_0'=16,'sp_1'=4,'tp'=8] {'sp_1'}, dimensions={0}, use_global_device_ids=true | all-gather | bytes 163840 | tf_op jit(solution)/shard_map/all_gather | solution.py:44
  242.0 28.5 %all-gather.1 = bf16[4096,64]{1,0:T(8,128)(2,1)S(1)} all-gather(bf16[256,64]{1,0:T(8,128)(2,1)S(1)} %pad_maximum_fusion), channel_id=3, replica_groups=mesh['sp_0'=16,'sp_1'=4,'tp'=8] {'sp_0'}, dimensions={0}, use_global_device_ids=true | all-gather | bytes 557056 | tf_op jit(solution)/shard_map/all_gather | solution.py:44
  271.0 1.3 convolution_convert_fusion.1
  272.4 1.3 collective-permute-start
  277.9 0.2 convolution_bitcast_fusion.4
  278.2 0.3 fusion.57
  278.4 0.3 fusion.208
  278.7 0.2 fusion.53
  279.0 1.7 fusion.66
  280.7 11.3 %all-gather.7.cloned.1.call-done = bf16[2048,256]{1,0:T(8,128)(2,1)} async-done(((bf16[32,256]{1,0:T(8,128)(2,1)}), bf16[2048,256]{1,0:T(8,128)(2,1)}) %all-gather.7.cloned.1.call-update) | async-done | bytes 1048592 | tf_op jit(solution)/shard_map/all_gather | solution.py:84
  292.1 1.4 fusion.81
  293.5 1.5 fusion.41
  295.0 24.6 %all_to_all.5 = bf16[8,16,2048]{2,1,0:T(8,128)(2,1)S(1)} all-to-all(bf16[8,16,2048]{2,1,0:T(8,128)(2,1)S(1)} %bitcast.386), channel_id=1, replica_groups=mesh['sp_0'=16,'sp_1'=4,'tp'=8] {'tp'}, dimensions={0} | all-to-all | bytes 1048576 | tf_op jit(solution)/shard_map/all_to_all | solution.py:99
  319.6 0.7 reduce_sum.72
  (151 shorter events, 10.6 us)
Async XLA Ops:
  6.5 272.4 %copy-start = (bf16[256,128]{1,0:T(8,128)(2,1)S(1)}, bf16[256,128]{1,0:T(8,128)(2,1)}, u32[]{:S(2)}) copy-start(bf16[256,128]{1,0:T(8,128)(2,1)} %param.43) | copy-start | bytes 196612
  6.5 151.6 %copy-start.6 = (bf16[128,128]{1,0:T(8,128)(2,1)S(1)}, bf16[128,128]{1,0:T(8,128)(2,1)}, u32[]{:S(2)}) copy-start(bf16[128,128]{1,0:T(8,128)(2,1)} %param.41) | copy-start | bytes 98308
  6.5 151.6 %copy-start.8 = (f32[128]{0:T(128)S(1)}, f32[128]{0:T(128)}, u32[]{:S(2)}) copy-start(f32[128]{0:T(128)} %param.44) | copy-start | bytes 1540
  6.5 151.6 %copy-start.5 = (f32[128,128]{1,0:T(8,128)S(1)}, f32[128,128]{1,0:T(8,128)}, u32[]{:S(2)}) copy-start(f32[128,128]{1,0:T(8,128)} %param.51) | copy-start | bytes 196612
  6.5 151.6 %copy-start.4 = (f32[128,128]{1,0:T(8,128)S(1)}, f32[128,128]{1,0:T(8,128)}, u32[]{:S(2)}) copy-start(f32[128,128]{1,0:T(8,128)} %param.52) | copy-start | bytes 196612
  6.5 153.3 %copy-start.3 = (f32[128]{0:T(128)S(1)}, f32[128]{0:T(128)}, u32[]{:S(2)}) copy-start(f32[128]{0:T(128)} %param.47) | copy-start | bytes 1540
  6.6 148.1 %all-gather.5.cloned.1.call-start = ((), (), s32[]{:S(2)}) async-start(), calls=%async_computation.1 | async-start | bytes 4259840 | tf_op jit(solution)/shard_map/all_gather | solution.py:27
  11.6 0.6 copy-start.1
  12.3 279.8 %all-gather.7.cloned.1.call-start = ((), (), s32[]{:S(2)}) async-start(), calls=%async_computation.2 | async-start | bytes 1064960 | tf_op jit(solution)/shard_map/all_gather | solution.py:84
  270.4 7.5 %copy-start.2 = (f32[2,64,64]{2,1,0:T(8,128)S(1)}, f32[2,64,64]{2,1,0:T(8,128)}, u32[]{:S(2)}) copy-start(f32[2,64,64]{2,1,0:T(8,128)} %param.53) | copy-start | bytes 98308
  272.4 21.1 %collective-permute-start = (bf16[16,128]{1,0:T(8,128)(2,1)S(1)}, bf16[16,128]{1,0:T(8,128)(2,1)S(1)}, u32[]{:S(2)}, u32[]{:S(2)}) collective-permute-start(bf16[16,128]{1,0:T(8,128)(2,1)S(1)} %slice.371), channel_id=1, source_target_pairs={{0,8},{8,16},{16,24},{24,32},{32,40},{40,48},{48,56},{56,64},{64,7... | collective-permute-start | bytes 12296 | tf_op jit(solution)/shard_map/ppermute | solution.py:78
  276.3 17.2 %copy-start.7 = (bf16[1,128,128]{2,1,0:T(8,128)(2,1)S(1)}, bf16[1,128,128]{2,1,0:T(8,128)(2,1)}, u32[]{:S(2)}) copy-start(bf16[1,128,128]{2,1,0:T(8,128)(2,1)} %param.54) | copy-start | bytes 98308
  276.3 17.1 %copy-start.9 = (f32[128]{0:T(128)S(1)}, f32[128]{0:T(128)}, u32[]{:S(2)}) copy-start(f32[128]{0:T(128)} %param.55) | copy-start | bytes 1540
Sparse Core Ops, SparseCore 0:
  12.4 142.2 all-gather.4
  157.6 134.4 all-gather.6
where the time goes:
time: 328 us; the launch traced here: 327 us
  waiting for transfers between devices  146 us (45%)
  blocking collectives  62.2 us (19%)
  other arithmetic  45.4 us (14%)
  local copies, waits for them, and re-layouts  33.6 us (10%)
  matrix products  24.4 us (7%)
  between operations  14 us (4%)
    all_gather x1, waiting for transfers between devices, side_by_side(): lax.all_gather(both, axis, axis=dim, tiled=True)  135 us
    all_gather x2, blocking collectives, gathered_once(): both, at, found = (lax.all_gather(jnp.concatenate(lines), axis), 0, {})  37.6 us
    all_to_all x1, blocking collectives, sent_and_summed(): parts = lax.all_to_all(split_up(x, dim, peers), axis, 0, 0, tiled=True)  24.6 us
    while x6, local copies, waits for them, and re-layouts  22.4 us
    another operation x10, other arithmetic, block_recurrence(): jax.scipy.linalg.solve_triangular(system, a_hat, lower=True, unit_diagona...  19.9 us
    all_gather x1, waiting for transfers between devices, gather_turned(): lax.all_gather(both, axis, axis=0, tiled=True)  11.3 us
    dot_general x2, other arithmetic, block_recurrence(): lower_b = jnp.einsum('htk,hsk,htsk->hts', alpha_t, key_t, weight_before)  10.3 us
    exp x2, other arithmetic, block_recurrence(): jnp.exp(jnp.where(upto, total[:, :, None, :] - total[:, None, :, :], -jnp...  8.47 us
  transfers between devices with their start and end apart: 3, of which 2 were waited for; matrix products, arithmetic and copies ran while one was open for 29% of the time, Pallas kernels for 0%

commit v1 on v0

v1 whole, which is shorter than its diff:
```python
import functools

import jax
import jax.numpy as jnp
from jax import lax
from jax.experimental import pallas as pl
from jax.experimental.pallas import tpu as pltpu
from jax.sharding import Mesh
from jax.sharding import PartitionSpec as P

Z = ("zh", "zl")
SP = ("zh", "zl", "y")
TP = ("x", "c")
f32 = jnp.float32
bf16 = jnp.bfloat16
HEAD = 64
CHUNK = 64
ROWS = 128
LANES = 128
PAY = 160
TAIL = 128
LEFT = 144
HIGHEST = lax.Precision.HIGHEST
NT = (((1,), (1,)), ((), ()))
TN = (((0,), (0,)), ((), ()))


def iota(shape, dim):
    return lax.broadcasted_iota(jnp.int32, shape, dim)


def mm(a, b, dims=(((1,), (0,)), ((), ()))):
    return lax.dot_general(a.astype(bf16), b.astype(bf16), dims, preferred_element_type=f32)


def mm32(a, b):
    return jnp.dot(a, b, preferred_element_type=f32, precision=HIGHEST)


def call(kernel, outs, *args, flops=10**8, name=None):
    size = sum(a.size * a.dtype.itemsize for a in args)
    return pl.pallas_call(
        kernel,
        out_shape=outs,
        in_specs=[pl.BlockSpec(memory_space=pltpu.VMEM)] * len(args),
        out_specs=jax.tree.map(lambda _: pl.BlockSpec(memory_space=pltpu.VMEM), outs),
        cost_estimate=pl.CostEstimate(flops=flops, bytes_accessed=size, transcendentals=0),
        name=name,
    )(*args)


def shaped(shape, dtype):
    return jax.ShapeDtypeStruct(shape, dtype)


def prepare_tokens(tok_ref, gain_ref, bias_ref, out_ref):
    wide = tok_ref[...].astype(f32)
    center = jnp.mean(wide, axis=-1, keepdims=True)
    off = wide - center
    spread = jnp.mean(jnp.square(off), axis=-1, keepdims=True)
    normed = (off * lax.rsqrt(spread + 1e-05) * gain_ref[...] + bias_ref[...]).astype(bf16)
    source = iota((512, 512), 0)
    target = iota((512, 512), 1)
    moved = ((source >> 5) & 3) * 128 + (source >> 7) * 32 + (source & 31)
    pick = jnp.where(moved == target, 1.0, 0.0).astype(bf16)
    for j in range(4):
        turned = jnp.dot(normed[:, 512 * j : 512 * j + 512], pick, preferred_element_type=f32)
        for y in range(4):
            out_ref[y, :, 128 * j : 128 * j + 128] = turned[:, 128 * y : 128 * y + 128].astype(bf16)


def prepare_weights(q_ref, k_ref, v_ref, p_ref, d_ref, r_ref, g_ref, oa_ref, op_ref, out_ref):
    first = lax.axis_index("c") == 0
    out_ref[:, 0:128] = q_ref[...]
    out_ref[:, 128:256] = k_ref[...]
    out_ref[:, 256:384] = v_ref[...]
    out_ref[:, 384:512] = p_ref[...]
    gate = g_ref[...]
    out_ref[:, 512:640] = jnp.where(first, d_ref[...], gate[:, :128])
    out_ref[:, 640:768] = jnp.where(first, r_ref[...], gate[:, 128:])
    out_ref[:, 768:896] = oa_ref[...].astype(f32).T.astype(bf16)
    out_ref[:, 896:1023] = op_ref[...].astype(f32).T.astype(bf16)[:, :127]


def partial_products(tok_ref, w_ref, part_ref, out_ref):
    made = jnp.dot(tok_ref[...], w_ref[:, :768], preferred_element_type=f32).astype(bf16)
    for y in range(4):
        part_ref[y] = made[128 * y : 128 * y + 128]
    first = w_ref[:, 768:896]
    second = w_ref[:, 896:1023]
    for y in range(4):
        out_ref[y, :, 0:128] = first
        out_ref[y, :, 128:255] = second
        out_ref[y, :, 255:256] = jnp.zeros((512, 1), bf16)


def sum_parts(part_ref, main_ref, low_ref):
    total = part_ref[0].astype(f32)
    for y in range(1, 4):
        total = total + part_ref[y].astype(f32)
    rounded = total.astype(bf16)
    main_ref[...] = rounded[:, :512]
    low = rounded[:, 512:].astype(f32)
    first = lax.axis_index("c") == 0
    one = jnp.where(first, jnp.tanh(low[:, :128]), jax.nn.sigmoid(low[:, :128]))
    two = jnp.where(first, low[:, 128:], jax.nn.sigmoid(low[:, 128:]))
    low_ref[:, :128] = one.astype(bf16)
    low_ref[:, 128:] = two.astype(bf16)


def by_head(lane_low, zero_head, one_head):
    return jnp.where(lane_low, zero_head, one_head)


def block_diagonal(pair):
    low = iota(pair.shape, 1) < HEAD
    zero = jnp.zeros_like(pair)
    return jnp.concatenate([jnp.where(low, pair, zero), jnp.where(low, zero, pair)], axis=0)


def recurrence(
    main_ref, low_ref, dw_ref, rw_ref, gw_ref, db_ref, lb_ref, kp_ref, kl_ref, st_ref,
    re_ref, de_ref, left_ref, pay_ref, ymap_ref, yloc_ref, gate_ref,
):
    recept = main_ref[:, 0:128].astype(f32)
    keys = main_ref[:, 128:256].astype(f32)
    values_b = main_ref[:, 256:384]
    values = values_b.astype(f32)
    row = iota((ROWS, LANES), 0)
    col = iota((ROWS, LANES), 1)
    lane_low = col < HEAD
    same = (row // CHUNK) == (col // CHUNK)

    drive = db_ref[...] + jnp.dot(low_ref[0, :, :128], dw_ref[...], preferred_element_type=f32)
    log_decay = -jax.nn.sigmoid(drive) * jnp.exp(re_ref[...] - 0.5) + de_ref[...]
    rate = jax.nn.sigmoid(
        lb_ref[...] + jnp.dot(low_ref[0, :, 128:], rw_ref[...], preferred_element_type=f32)
    )
    gate_ref[...] = jnp.dot(low_ref[1], gw_ref[...], preferred_element_type=f32)

    ones = jnp.where(same, 1.0, 0.0).astype(f32)
    unit = keys * kp_ref[...]
    effective = keys * (1.0 + (rate - 1.0) * kl_ref[...])
    sums = mm32(
        jnp.concatenate([unit * unit, recept * effective * st_ref[...]], axis=0), ones
    )
    unit = unit * lax.rsqrt(sums[:ROWS] + 1e-06)
    own = sums[ROWS:] * values
    beta = unit * rate

    tril = jnp.where(same & (row >= col), 1.0, 0.0).astype(f32)
    totals = mm32(jnp.concatenate([tril, ones], axis=0), log_decay)
    total, end = totals[:ROWS], totals[ROWS:]
    ref = 0.5 * end
    grow = jnp.exp(ref - total)
    shrink = jnp.exp(total - ref)
    base = jnp.exp(ref)
    a_hat = -unit * jnp.exp(total - log_decay - ref)
    r_hat = recept * shrink
    b_hat = beta * grow
    k_hat = effective * grow

    def masked(x):
        zero = jnp.zeros_like(x)
        return [jnp.where(lane_low, x, zero), jnp.where(lane_low, zero, x)]

    left = jnp.concatenate(masked(a_hat) + masked(r_hat), axis=0)
    right = jnp.concatenate([b_hat, k_hat], axis=0)
    scores = mm(left, right, NT)
    strict = same & (row > col)
    upto = same & (row >= col)

    def score(which, head, side, mask):
        at = (2 * which + head) * ROWS
        return jnp.where(mask, scores[at : at + ROWS, side * ROWS : side * ROWS + ROWS], 0.0)

    eye = jnp.where(row == col, 1.0, 0.0).astype(f32)
    within16 = (row // 16) == (col // 16)
    within32 = (row // 32) == (col // 32)
    a_start = a_hat * base
    swapped = pltpu.roll(a_start, HEAD, 1)
    solved, reads = [], []
    power, product = [], []
    full = [score(0, h, 0, strict) for h in range(2)]
    for h in range(2):
        power.append(jnp.where(within16, full[h], 0.0))
        product.append(eye + power[h])
    for _ in range(3):
        power = [mm32(power[h], power[h]) for h in range(2)]
        product = [product[h] + mm32(product[h], power[h]) for h in range(2)]
    step = [jnp.where(within32 & ~within16, full[h], 0.0) for h in range(2)]
    mid = [mm32(product[h], step[h]) for h in range(2)]
    product = [product[h] + mm32(mid[h], product[h]) for h in range(2)]
    step = [jnp.where(within32, 0.0, full[h]) for h in range(2)]
    mid = [mm32(product[h], step[h]) for h in range(2)]
    product = [product[h] + mm32(mid[h], product[h]) for h in range(2)]
    for h in range(2):
        pushed = mm(score(0, h, 1, strict), values_b)
        side = lane_low if h == 0 else ~lane_low
        rhs = jnp.where(side, pushed, swapped)
        solved.append(mm(product[h], rhs))
        reads.append(mm(score(1, h, 0, upto), solved[h]))
    direct = [mm(score(1, h, 1, upto), values_b) for h in range(2)]
    y_local = by_head(lane_low, reads[0], reads[1]) + by_head(lane_low, direct[0], direct[1])
    y_map = r_hat * base + pltpu.roll(by_head(lane_low, reads[1], reads[0]), HEAD, 1)

    b_end = (b_hat * base).astype(bf16)
    k_end = (k_hat * base).astype(bf16)
    decay_end = jnp.exp(end)
    low64 = iota((CHUNK, LANES), 1) < HEAD
    diagonal = iota((CHUNK, LANES), 0) == (iota((CHUNK, LANES), 1) % HEAD)
    maps, states = [], []
    for c in range(2):
        at = slice(c * CHUNK, c * CHUNK + CHUNK)
        g0 = mm(solved[0][at], b_end[at], TN)
        g1 = mm(solved[1][at], b_end[at], TN)
        kv = mm(values_b[at], k_end[at], TN)
        maps.append(
            jnp.where(diagonal, decay_end[at], 0.0)
            + by_head(low64, g0[HEAD:], g1[:HEAD])
        )
        states.append(
            by_head(low64, g0[:HEAD], g1[HEAD:]) + by_head(low64, kv[:HEAD], kv[HEAD:])
        )
    joined = mm(jnp.concatenate([maps[0], states[0]], axis=0), block_diagonal(maps[1]))
    block_map = joined[:CHUNK]
    block_state = joined[CHUNK:] + states[1]
    late = mm(
        y_map[CHUNK:],
        jnp.concatenate([block_diagonal(states[0]), block_diagonal(maps[0])], axis=0),
        NT,
    )
    ymap_ref[:CHUNK] = y_map[:CHUNK]
    ymap_ref[CHUNK:] = late[:, LANES:]
    yloc_ref[0, :CHUNK] = y_local[:CHUNK]
    yloc_ref[0, CHUNK:] = y_local[CHUNK:] + late[:, :LANES]
    yloc_ref[1] = own
    y = lax.axis_index("y")
    mine = jnp.where(col[:16] // 32 == y, left_ref[...].astype(f32), 0.0)
    mine = jnp.where(row[:16] == 0, mine, 0.0).astype(bf16)
    block_map = block_map.astype(bf16)
    block_state = block_state.astype(bf16)
    tail = main_ref[ROWS - 16 :, 384:512]
    for j in range(4):
        pay_ref[j, 0:64] = block_map
        pay_ref[j, 64:128] = block_state
        pay_ref[j, TAIL : TAIL + 16] = tail
        pay_ref[j, LEFT : LEFT + 16] = mine


def identity_pair():
    eye = iota((HEAD, LANES), 0) == (iota((HEAD, LANES), 1) % HEAD)
    return jnp.concatenate([jnp.where(eye, 1.0, 0.0).astype(f32), jnp.zeros((HEAD, LANES), f32)], 0)


def compose(earlier, later):
    moved = mm(earlier, block_diagonal(later[:HEAD]))
    return jnp.concatenate([moved[:HEAD], moved[HEAD:] + later[HEAD:]], axis=0)


def prefixes(got_ref, mine):
    pieces = [got_ref[j, :128].astype(f32) for j in range(4)]
    running = pieces[0]
    before = jnp.where(mine == 0, identity_pair(), pieces[0])
    for j in range(1, 4):
        running = compose(running, pieces[j])
        if j < 3:
            before = jnp.where(mine > j, running, before)
    return before, running


def tail_before(got_ref, mine):
    zero = jnp.zeros((16, LANES), f32)
    found = zero
    for j in range(3):
        found = jnp.where(mine == j + 1, got_ref[j, TAIL : TAIL + 16].astype(f32), found)
    return found


def stage_y(got_ref, pay_ref, before_ref, tail_ref):
    y = lax.axis_index("y")
    before, running = prefixes(got_ref, y)
    before_ref[...] = before
    tail_ref[...] = tail_before(got_ref, y)
    left = got_ref[0, LEFT : LEFT + 16].astype(f32)
    for j in range(1, 4):
        left = left + got_ref[j, LEFT : LEFT + 16].astype(f32)
    running = running.astype(bf16)
    left = left.astype(bf16)
    for j in range(4):
        pay_ref[j, 0:128] = running
        pay_ref[j, TAIL : TAIL + 16] = got_ref[3, TAIL : TAIL + 16]
        pay_ref[j, LEFT : LEFT + 16] = left


def stage_zl(got_ref, before_ref, tail_ref, pay_ref, out_before_ref, out_tail_ref):
    y = lax.axis_index("y")
    zl = lax.axis_index("zl")
    before, running = prefixes(got_ref, zl)
    out_before_ref[...] = compose(before, before_ref[...])
    out_tail_ref[...] = jnp.where(y == 0, tail_before(got_ref, zl), tail_ref[...])
    row = iota((16, LANES), 0)
    left = jnp.zeros((16, LANES), f32)
    for j in range(4):
        line = got_ref[j, LEFT : LEFT + 16].astype(f32)[0:1]
        left = jnp.where(row == j, line, left)
    running = running.astype(bf16)
    left = left.astype(bf16)
    for j in range(4):
        pay_ref[j, 0:128] = running
        pay_ref[j, TAIL : TAIL + 16] = got_ref[3, TAIL : TAIL + 16]
        pay_ref[j, LEFT : LEFT + 16] = left


def finish(
    got_ref, before_ref, tail_ref, start_ref, ymap_ref, yloc_ref, gate_ref, hs_ref, hb_ref,
    pool_ref, matrix_ref, scale_ref, wout_ref, out_ref,
):
    zh, zl, y = lax.axis_index("zh"), lax.axis_index("zl"), lax.axis_index("y")
    state = jnp.concatenate([start_ref[0], start_ref[1]], axis=1)
    for j in range(3):
        piece = got_ref[j, :128].astype(f32)
        state = jnp.where(zh > j, mm(state, block_diagonal(piece[:HEAD])) + piece[HEAD:], state)
    state = mm(state, block_diagonal(before_ref[:HEAD])) + before_ref[HEAD:]
    reading = yloc_ref[0] + mm(ymap_ref[...], block_diagonal(state), NT)
    row = iota((ROWS, LANES), 0)
    col = iota((ROWS, LANES), 1)
    mean = jnp.where((row // HEAD) == (col // HEAD), 1.0 / HEAD, 0.0).astype(f32)
    off = reading - mm32(reading, mean)
    spread = mm32(off * off, mean)
    headed = off * lax.rsqrt(spread + 1e-05 * HEAD) * hs_ref[...] + hb_ref[...] + yloc_ref[1]
    attn = (headed * gate_ref[...]).astype(bf16)

    pool = pool_ref[:, 384:512].astype(f32)
    tail = jnp.where((y == 0) & (zl == 0), tail_before(got_ref, zh), tail_ref[...])
    extended = jnp.concatenate([tail, pool], axis=0)
    level = lax.axis_index("x")
    sums = extended
    chosen = None
    for k in range(4):
        width = 1 << k
        shifted = pltpu.roll(sums, width, 0)
        sums = sums + jnp.where(iota(sums.shape, 0) < width, 0.0, shifted)
        picked = sums[16:]
        chosen = picked if k == 0 else jnp.where(level >= k, picked, chosen)
    window = lax.shift_left(jnp.int32(2), level).astype(f32)
    position = (((zh * 4 + zl) * 4 + y) * ROWS + row).astype(f32)
    pooled = (chosen / jnp.minimum(position + 1.0, window) - pool).astype(bf16)
    grouped = jnp.dot(pooled, matrix_ref[0], preferred_element_type=f32)
    pool_out = (grouped * scale_ref[...]).astype(bf16)

    acts = jnp.concatenate([attn, pool_out], axis=1)
    last = pool_out[:, 127:128].astype(f32)
    for zpair in range(8):
        rows = []
        for z in (2 * zpair, 2 * zpair + 1):
            for yy in range(4):
                rows.append(wout_ref[yy, 32 * z : 32 * z + 32])
        made = mm(acts, jnp.concatenate(rows, axis=0), NT)
        for half in range(2):
            z = 2 * zpair + half
            line = got_ref[z // 4, LEFT : LEFT + 16].astype(f32)[z % 4 : z % 4 + 1]
            out_ref[:, 128 * z : 128 * z + 128] = (
                made[:, 128 * half : 128 * half + 128] + last * line
            ).astype(bf16)


def on_device(
    tokens, input_norm_scale, input_norm_bias, query_projection, key_projection,
    value_projection, pooling_input_projection, decay_input_weight, rate_input_weight,
    gate_input_weight, decay_output_weight, rate_output_weight, gate_output_weight,
    decay_bias_base, learning_rate_base, key_prenorm_scale, key_learning_scale,
    self_term_weight, head_norm_scale, head_norm_bias, rate_extra_log, decay_extra_log,
    starting_head_state, pooling_group_matrix, pooling_output_scale, output_attention_rows,
    output_pooling_rows,
):
    line = lambda v: v.reshape(1, -1)
    sent = call(
        prepare_tokens, shaped((4, 128, 512), bf16),
        tokens, line(input_norm_scale), line(input_norm_bias), name="prepare_tokens",
    )
    shard = call(
        prepare_weights, shaped((32, 1023), bf16),
        query_projection, key_projection, value_projection, pooling_input_projection,
        decay_input_weight, rate_input_weight, gate_input_weight, output_attention_rows,
        output_pooling_rows, name="prepare_weights",
    )
    gathered = lax.all_gather(shard, Z, axis=0, tiled=True)
    mixed_tokens = lax.all_to_all(sent, "y", 0, 0, tiled=True).reshape(512, 512)
    parts, out_columns = call(
        partial_products,
        [shaped((4, 128, 768), bf16), shaped((4, 512, 256), bf16)],
        mixed_tokens, gathered, name="partial_products",
    )
    parts = lax.all_to_all(parts, "y", 0, 0, tiled=True)
    main, low = call(
        sum_parts, [shaped((128, 512), bf16), shaped((128, 256), bf16)], parts, name="sum_parts"
    )
    low = lax.all_gather(low, "c", axis=0)
    left = jnp.tile(output_pooling_rows[127:128], (1, 4))
    pay, y_map, y_local, gate = call(
        recurrence,
        [
            shaped((4, PAY, 128), bf16), shaped((128, 128), f32), shaped((2, 128, 128), f32),
            shaped((128, 128), f32),
        ],
        main, low, decay_output_weight, rate_output_weight, gate_output_weight,
        line(decay_bias_base), line(learning_rate_base), line(key_prenorm_scale),
        line(key_learning_scale), line(self_term_weight), rate_extra_log, decay_extra_log,
        left, name="recurrence",
    )
    out_columns = lax.all_to_all(out_columns, "y", 0, 0, tiled=True)
    got = lax.all_to_all(pay, "y", 0, 0, tiled=True)
    pay, before, tail = call(
        stage_y,
        [shaped((4, PAY, 128), bf16), shaped((128, 128), f32), shaped((16, 128), f32)],
        got, name="stage_y",
    )
    got = lax.all_to_all(pay, "zl", 0, 0, tiled=True)
    pay, before, tail = call(
        stage_zl,
        [shaped((4, PAY, 128), bf16), shaped((128, 128), f32), shaped((16, 128), f32)],
        got, before, tail, name="stage_zl",
    )
    got = lax.all_to_all(pay, "zh", 0, 0, tiled=True)
    out = call(
        finish, shaped((128, 2048), bf16),
        got, before, tail, starting_head_state, y_map, y_local, gate, line(head_norm_scale),
        line(head_norm_bias), main, pooling_group_matrix, line(pooling_output_scale),
        out_columns, name="finish",
    )
    parts = lax.all_to_all(out.reshape(8, 16, 2048), TP, 0, 0, tiled=True)
    return jnp.sum(parts.astype(f32), axis=0).astype(bf16)


def solution(mesh):
    split = Mesh(mesh.devices.reshape(4, 4, 4, 4, 2), ("zh", "zl", "y", "x", "c"))
    in_specs = (
        P(SP, None), P(), P(),
        P(SP, TP), P(SP, TP), P(SP, TP), P(SP, TP),
        P(SP, None), P(SP, None), P(SP, None),
        P(None, TP), P(None, TP), P(None, TP),
        P(TP), P(TP), P(TP), P(TP), P(TP), P(TP), P(TP),
        P(SP, TP), P(SP, TP),
        P(TP, None, None), P(TP, None, None), P(TP),
        P(TP, SP), P(TP, SP),
    )
    out_specs = P((*SP, *TP), None)
    return jax.shard_map(
        on_device, mesh=split, in_specs=in_specs, out_specs=out_specs, check_vma=False
    )
```

time: 328 us -> 167 us (0.51)
  waiting for transfers between devices: 146 us -> 17.8 us
  blocking collectives: 62.2 us -> 108 us
  other arithmetic: 45.4 us -> 0.7 us
  local copies, waits for them, and re-layouts: 33.6 us -> 4.06 us
  matrix products: 24.4 us -> 0 us
  Pallas kernels: 0 us -> 22.8 us
  between operations: 14 us -> 0.03 us
  starting transfers between devices: 1.37 us -> 12.5 us
    all_gather x2 -> x0, waiting for transfers between devices: 146 us -> none  [the longest x1 135 us: side_by_side(): lax.all_gather(both, axis, axis=dim, tiled=True)]
    all_to_all x1 -> x4, blocking collectives: 24.6 us -> 57 us  [the longest x1 19.6 us: on_device(): got = lax.all_to_all(pay, 'zh', 0, 0, tiled=True)]
    dot_general x74 -> x0, matrix products: 23.3 us -> none  [the longest x4 5.5 us: on_device(): jnp.dot(normed, piece, preferred_element_type=f32)]
    pallas_call x0 -> x8, Pallas kernels: none -> 22.8 us  [call(): pl.pallas_call(kernel, out_shape=outs, in_specs=[pl.BlockSpec(memory_spac...]
    while x6 -> x0, local copies, waits for them, and re-layouts: 22.4 us -> none
    another operation x14 -> x0, other arithmetic: 20.1 us -> none  [the longest x10 19.9 us: block_recurrence(): jax.scipy.linalg.solve_triangular(system, a_hat, lower=True, unit_diagona...]
    all_to_all x0 -> x3, waiting for transfers between devices: none -> 17.8 us  [the longest x1 10.4 us: on_device(): out_columns = lax.all_to_all(out_columns, 'y', 0, 0, tiled=True)]
    all_gather x2, blocking collectives: 37.6 us -> 50.6 us  [the longest x1 37.6 us: on_device(): gathered = lax.all_gather(shard, Z, axis=0, tiled=True)]
  transfers between devices with their start and end apart: 3 -> 3, of which waited for: 2 -> 2; matrix products, arithmetic and copies ran while one was open for 29% -> 1% of each run, Pallas kernels for 0% -> 2%
where the time goes in v1:
time: 167 us; the launch traced here: 165 us
  blocking collectives  108 us (65%)
  Pallas kernels  22.8 us (14%)
  waiting for transfers between devices  17.8 us (11%)
  starting transfers between devices  12.5 us (7%)
  local copies, waits for them, and re-layouts  4.06 us (2%)
    all_gather x1, blocking collectives, on_device(): gathered = lax.all_gather(shard, Z, axis=0, tiled=True)  37.6 us
    pallas_call x8, Pallas kernels, call(): pl.pallas_call(kernel, out_shape=outs, in_specs=[pl.BlockSpec(memory_spac...  22.8 us
    all_to_all x1, blocking collectives, on_device(): got = lax.all_to_all(pay, 'zh', 0, 0, tiled=True)  19.6 us
    all_to_all x1, blocking collectives, on_device(): parts = lax.all_to_all(out.reshape(8, 16, 2048), TP, 0, 0, tiled=True)  18.4 us
    all_gather x1, blocking collectives, on_device(): low = lax.all_gather(low, 'c', axis=0)  13 us
    all_to_all x1, waiting for transfers between devices, on_device(): out_columns = lax.all_to_all(out_columns, 'y', 0, 0, tiled=True)  10.4 us
    all_to_all x1, blocking collectives, on_device(): got = lax.all_to_all(pay, 'zl', 0, 0, tiled=True)  9.62 us
    all_to_all x1, blocking collectives, on_device(): got = lax.all_to_all(pay, 'y', 0, 0, tiled=True)  9.3 us
  transfers between devices with their start and end apart: 3, of which 2 were waited for; matrix products, arithmetic and copies ran while one was open for 1% of the time, Pallas kernels for 2%

profile of v1, /device:TPU:1, one launch (start us, length us, event | category | flops | bytes accessed | tf_op | source)
XLA Modules:
  0.0 165.5 jit_solution(2710267293014347196)
XLA Ops:
  0.0 2.7 %prepare_tokens.1 = bf16[4,128,512]{2,1,0:T(8,128)(2,1)} custom-call(bf16[128,2048]{1,0:T(8,128)(2,1)} %tok_ref.1, f32[1,2048]{1,0:T(1,128)} %bitcast.16, f32[1,2048]{1,0:T(1,128)} %bitcast.17), custom_call_target="tpu_custom_call" | custom-call | flops 100000000 | bytes 540672 | tf_op jit(solution)/shard_map/prepare_tokens/pallas_call | solution.py:42
  2.7 0.0 copy-start.4
  2.7 5.1 %all-to-all-start = ((bf16[4,128,512]{2,1,0:T(8,128)(2,1)}), bf16[4,128,512]{2,1,0:T(8,128)(2,1)S(1)}, u32[]{:S(2)}, u32[]{:S(2)}) async-start(bf16[4,128,512]{2,1,0:T(8,128)(2,1)} %prepare_tokens.1), calls=%async_computation | async-start | bytes 1048576 | tf_op jit(solution)/shard_map/all_to_all | solution.py:389
  7.8 0.0 copy-done.4
  7.8 0.0 copy-start.3
  7.8 0.7 copy.30.oa_ref
  8.5 0.0 copy-done.3
  8.5 0.7 copy.31.op_ref
  9.3 1.6 prepare_weights.1
  10.8 37.6 %all_gather.9.w_ref = bf16[512,1023]{1,0:T(8,128)(2,1)} all-gather(bf16[32,1023]{1,0:T(8,128)(2,1)} %prepare_weights.1), channel_id=1, replica_groups=mesh['zh'=4,'zl'=4,'y'=4,'x'=4,'c'=2] {'zh','zl'}, dimensions={0}, use_global_device_ids=true | all-gather | bytes 1113024 | tf_op jit(solution)/shard_map/all_gather | solution.py:388
  48.4 0.0 all-to-all-done
  48.4 0.0 copy-start.2
  48.4 0.8 copy-done.2
  49.2 3.3 %partial_products.1 = (bf16[4,128,768]{2,1,0:T(8,128)(2,1)}, bf16[4,512,256]{2,1,0:T(8,128)(2,1)}) custom-call(bf16[512,512]{1,0:T(8,128)(2,1)} %bitcast.13, bf16[512,1023]{1,0:T(8,128)(2,1)} %all_gather.9.w_ref), custom_call_target="tpu_custom_call" | custom-call | flops 100000000 | bytes 1571840 | tf_op jit(solution)/shard_map/partial_products/pallas_call | solution.py:42
  52.6 3.8 %all-to-all-start.1 = ((bf16[4,128,768]{2,1,0:T(8,128)(2,1)}), bf16[4,128,768]{2,1,0:T(8,128)(2,1)S(1)}, u32[]{:S(2)}, u32[]{:S(2)}) async-start(bf16[4,128,768]{2,1,0:T(8,128)(2,1)} %get-tuple-element.19), calls=%async_computation.1 | async-start | bytes 1572864 | tf_op jit(solution)/shard_map/all_to_all | solution.py:395
  56.4 0.2 slice_reduce_fusion
  56.6 0.7 tile.13.left_ref
  57.3 7.5 %all-to-all-done.1.part_ref = bf16[4,128,768]{2,1,0:T(8,128)(2,1)S(1)} async-done(((bf16[4,128,768]{2,1,0:T(8,128)(2,1)}), bf16[4,128,768]{2,1,0:T(8,128)(2,1)S(1)}, u32[]{:S(2)}, u32[]{:S(2)}) %all-to-all-start.1) | async-done | bytes 786464 | tf_op jit(solution)/shard_map/all_to_all | solution.py:395
  64.7 0.0 copy-start.1
  64.7 0.9 copy-done.1
  65.7 1.9 %sum_parts.1 = (bf16[128,512]{1,0:T(8,128)(2,1)}, bf16[128,256]{1,0:T(8,128)(2,1)}) custom-call(bf16[4,128,768]{2,1,0:T(8,128)(2,1)} %copy-done.1), custom_call_target="tpu_custom_call" | custom-call | flops 100000000 | bytes 786432 | tf_op jit(solution)/shard_map/sum_parts/pallas_call | solution.py:42
  67.6 13.0 %all-gather = bf16[256,256]{1,0:T(8,128)(2,1)} all-gather(bf16[128,256]{1,0:T(8,128)(2,1)} %get-tuple-element.21), channel_id=2, replica_groups=mesh['zh'=4,'zl'=4,'y'=4,'x'=4,'c'=2] {'c'}, dimensions={0}, use_global_device_ids=true | all-gather | bytes 196608 | tf_op jit(solution)/shard_map/all_gather | solution.py:399
  80.6 5.3 %recurrence.1 = (bf16[4,160,128]{2,1,0:T(8,128)(2,1)}, f32[128,128]{1,0:T(8,128)}, f32[2,128,128]{2,1,0:T(8,128)}, f32[128,128]{1,0:T(8,128)}) custom-call(bf16[128,512]{1,0:T(8,128)(2,1)} %get-tuple-element.20.main_ref.pool_ref, bf16[2,128,256]{2,1,0:T(8,128)(2,1)} %bitcast.15, bf16[128,128]{1,0:T(8,128)(2,1)} %dw_ref.1, bf16[128,128]{1,0:T(8,128)(2,1)} %rw_ref.1, ...), custom_call_target="tpu_custom_call" | custom-call | flops 100000000 | bytes 527104 | tf_op jit(solution)/shard_map/recurrence/pallas_call | solution.py:42
  85.9 9.3 %all_to_all.35.got_ref = bf16[4,160,128]{2,1,0:T(8,128)(2,1)} all-to-all(bf16[4,160,128]{2,1,0:T(8,128)(2,1)} %get-tuple-element.22), channel_id=1, replica_groups=mesh['zh'=4,'zl'=4,'y'=4,'x'=4,'c'=2] {'y'}, dimensions={0} | all-to-all | bytes 327680 | tf_op jit(solution)/shard_map/all_to_all | solution.py:413
  95.2 2.0 %stage_y.1 = (bf16[4,160,128]{2,1,0:T(8,128)(2,1)}, f32[128,128]{1,0:T(8,128)}, f32[16,128]{1,0:T(8,128)}) custom-call(bf16[4,160,128]{2,1,0:T(8,128)(2,1)} %all_to_all.35.got_ref), custom_call_target="tpu_custom_call" | custom-call | flops 100000000 | bytes 163840 | tf_op jit(solution)/shard_map/stage_y/pallas_call | solution.py:42
  97.1 9.6 %all_to_all.36.got_ref = bf16[4,160,128]{2,1,0:T(8,128)(2,1)} all-to-all(bf16[4,160,128]{2,1,0:T(8,128)(2,1)} %get-tuple-element.23), channel_id=1, replica_groups=mesh['zh'=4,'zl'=4,'y'=4,'x'=4,'c'=2] {'zl'}, dimensions={0} | all-to-all | bytes 327680 | tf_op jit(solution)/shard_map/all_to_all | solution.py:419
  106.8 3.5 %all-to-all-start.5 = ((bf16[4,512,256]{2,1,0:T(8,128)(2,1)}), bf16[4,512,256]{2,1,0:T(8,128)(2,1)S(1)}, u32[]{:S(2)}, u32[]{:S(2)}) async-start(bf16[4,512,256]{2,1,0:T(8,128)(2,1)} %get-tuple-element.32), calls=%async_computation.5 | async-start | bytes 2097152 | tf_op jit(solution)/shard_map/all_to_all | solution.py:412
  110.3 2.1 %stage_zl.1 = (bf16[4,160,128]{2,1,0:T(8,128)(2,1)}, f32[128,128]{1,0:T(8,128)}, f32[16,128]{1,0:T(8,128)}) custom-call(bf16[4,160,128]{2,1,0:T(8,128)(2,1)} %all_to_all.36.got_ref, f32[128,128]{1,0:T(8,128)} %get-tuple-element.24.before_ref, f32[16,128]{1,0:T(8,128)} %get-tuple-element.25.tail_ref), custom_call_target="tpu_custom_call" | custom-call | flops 100000000 | bytes 237568 | tf_op jit(solution)/shard_map/stage_zl/pallas_call | solution.py:42
  112.3 10.4 %all-to-all-done.5.wout_ref = bf16[4,512,256]{2,1,0:T(8,128)(2,1)S(1)} async-done(((bf16[4,512,256]{2,1,0:T(8,128)(2,1)}), bf16[4,512,256]{2,1,0:T(8,128)(2,1)S(1)}, u32[]{:S(2)}, u32[]{:S(2)}) %all-to-all-start.5) | async-done | bytes 1048608 | tf_op jit(solution)/shard_map/all_to_all | solution.py:412
  122.7 0.0 copy-start
  122.7 19.6 %all_to_all.37.got_ref = bf16[4,160,128]{2,1,0:T(8,128)(2,1)} all-to-all(bf16[4,160,128]{2,1,0:T(8,128)(2,1)} %get-tuple-element.26), channel_id=1, replica_groups=mesh['zh'=4,'zl'=4,'y'=4,'x'=4,'c'=2] {'zh'}, dimensions={0} | all-to-all | bytes 327680 | tf_op jit(solution)/shard_map/all_to_all | solution.py:425
  142.3 0.0 copy-done
  142.3 4.0 %finish.1 = bf16[128,2048]{1,0:T(8,128)(2,1)} custom-call(bf16[4,160,128]{2,1,0:T(8,128)(2,1)} %all_to_all.37.got_ref, f32[128,128]{1,0:T(8,128)} %get-tuple-element.27.before_ref, f32[16,128]{1,0:T(8,128)} %get-tuple-element.28.tail_ref, f32[2,64,64]{2,1,0:T(8,128)} %start_ref.1, f32[128,128]{1,0:T(8,128)} %get-tuple-element.29.ymap_ref, ...), custom_call_target="tpu_custom_call" | custom-call | flops 100000000 | bytes 1746432 | tf_op jit(solution)/shard_map/finish/pallas_call | solution.py:42
  146.3 18.4 %all_to_all.38 = bf16[8,16,2048]{2,1,0:T(8,128)(2,1)S(1)} all-to-all(bf16[8,16,2048]{2,1,0:T(8,128)(2,1)} %bitcast.14), channel_id=1, replica_groups=mesh['zh'=4,'zl'=4,'y'=4,'x'=4,'c'=2] {'x','c'}, dimensions={0} | all-to-all | bytes 1048576 | tf_op jit(solution)/shard_map/all_to_all | solution.py:432
  164.8 0.7 reduce_sum.12
  (1 shorter events, 0.0 us)
Async XLA Ops:
  2.7 5.1 %copy-start.4 = (bf16[128,32]{0,1:T(8,128)(2,1)S(1)}, bf16[128,32]{0,1:T(8,128)(2,1)}, u32[]{:S(2)}) copy-start(bf16[128,32]{0,1:T(8,128)(2,1)} %param.52) | copy-start | bytes 24580
  2.7 45.8 %all-to-all-start = ((bf16[4,128,512]{2,1,0:T(8,128)(2,1)}), bf16[4,128,512]{2,1,0:T(8,128)(2,1)S(1)}, u32[]{:S(2)}, u32[]{:S(2)}) async-start(bf16[4,128,512]{2,1,0:T(8,128)(2,1)} %prepare_tokens.1), calls=%async_computation | async-start | bytes 1048576 | tf_op jit(solution)/shard_map/all_to_all | solution.py:389
  7.8 0.7 copy-start.3
  48.4 0.8 copy-start.2
  52.6 12.2 %all-to-all-start.1 = ((bf16[4,128,768]{2,1,0:T(8,128)(2,1)}), bf16[4,128,768]{2,1,0:T(8,128)(2,1)S(1)}, u32[]{:S(2)}, u32[]{:S(2)}) async-start(bf16[4,128,768]{2,1,0:T(8,128)(2,1)} %get-tuple-element.19), calls=%async_computation.1 | async-start | bytes 1572864 | tf_op jit(solution)/shard_map/all_to_all | solution.py:395
  64.7 0.9 copy-start.1
  106.8 16.0 %all-to-all-start.5 = ((bf16[4,512,256]{2,1,0:T(8,128)(2,1)}), bf16[4,512,256]{2,1,0:T(8,128)(2,1)S(1)}, u32[]{:S(2)}, u32[]{:S(2)}) async-start(bf16[4,512,256]{2,1,0:T(8,128)(2,1)} %get-tuple-element.32), calls=%async_computation.5 | async-start | bytes 2097152 | tf_op jit(solution)/shard_map/all_to_all | solution.py:412
  122.7 19.6 %copy-start = (bf16[4,512,256]{2,1,0:T(8,128)(2,1)}, bf16[4,512,256]{2,1,0:T(8,128)(2,1)S(1)}, u32[]{:S(2)}) copy-start(bf16[4,512,256]{2,1,0:T(8,128)(2,1)S(1)} %all-to-all-done.5.wout_ref) | copy-start | bytes 3145732

commit v2 on v1

v2 whole, which is shorter than its diff:
```python
import functools

import jax
import jax.numpy as jnp
from jax import lax
from jax.experimental import pallas as pl
from jax.experimental.pallas import tpu as pltpu
from jax.sharding import Mesh
from jax.sharding import PartitionSpec as P

Z = ("zh", "zl")
SP = ("zh", "zl", "y")
TP = ("x", "c")
f32 = jnp.float32
bf16 = jnp.bfloat16
HEAD = 64
CHUNK = 64
ROWS = 128
LANES = 128
PAY = 144
WIDE = 160
TAIL = 128
LEFT = 144
HIGHEST = lax.Precision.HIGHEST
NT = (((1,), (1,)), ((), ()))
TN = (((0,), (0,)), ((), ()))


def iota(shape, dim):
    return lax.broadcasted_iota(jnp.int32, shape, dim)


def mm(a, b, dims=(((1,), (0,)), ((), ()))):
    return lax.dot_general(a.astype(bf16), b.astype(bf16), dims, preferred_element_type=f32)


def mm32(a, b):
    return jnp.dot(a, b, preferred_element_type=f32, precision=HIGHEST)


def call(kernel, outs, *args, flops=10**8, name=None, vmem=16 * 2**20, space=pltpu.VMEM, scratch=()):
    size = sum(a.size * a.dtype.itemsize for a in args)
    return pl.pallas_call(
        kernel,
        out_shape=outs,
        in_specs=[pl.BlockSpec(memory_space=space)] * len(args),
        out_specs=jax.tree.map(lambda _: pl.BlockSpec(memory_space=pltpu.VMEM), outs),
        scratch_shapes=scratch,
        compiler_params=pltpu.CompilerParams(vmem_limit_bytes=vmem),
        cost_estimate=pl.CostEstimate(flops=flops, bytes_accessed=size, transcendentals=0),
        name=name,
    )(*args)


def shaped(shape, dtype):
    return jax.ShapeDtypeStruct(shape, dtype)


def prepare_tokens(tok_hbm, gain_hbm, bias_hbm, out_ref, tok, gain, bias, sems):
    halves = [
        pltpu.make_async_copy(
            tok_hbm.at[pl.ds(64 * i, 64)], tok.at[pl.ds(64 * i, 64)], sems.at[i]
        )
        for i in range(2)
    ]
    first = pltpu.make_async_copy(gain_hbm, gain, sems.at[2])
    second = pltpu.make_async_copy(bias_hbm, bias, sems.at[3])
    for copy in (halves[0], first, second, halves[1]):
        copy.start()
    source = iota((512, 512), 0)
    target = iota((512, 512), 1)
    moved = ((source >> 5) & 3) * 128 + (source >> 7) * 32 + (source & 31)
    pick = jnp.where(moved == target, 1.0, 0.0).astype(bf16)
    for i in range(2):
        halves[i].wait()
        if i == 0:
            first.wait()
            second.wait()
        rows = slice(64 * i, 64 * i + 64)
        wide = tok[rows].astype(f32)
        center = jnp.mean(wide, axis=-1, keepdims=True)
        off = wide - center
        spread = jnp.mean(jnp.square(off), axis=-1, keepdims=True)
        normed = (off * lax.rsqrt(spread + 1e-05) * gain[...] + bias[...]).astype(bf16)
        for j in range(4):
            turned = jnp.dot(normed[:, 512 * j : 512 * j + 512], pick, preferred_element_type=f32)
            turned = turned.astype(bf16)
            for y in range(4):
                out_ref[y, rows, 128 * j : 128 * j + 128] = turned[:, 128 * y : 128 * y + 128]


def prepare_weights(
    q_ref, k_ref, v_ref, p_ref, d_ref, r_ref, g_ref, oa_ref, op_ref, *rest
):
    *lines, out_ref, left_ref, lines_ref = rest
    for i, ref in enumerate(lines):
        lines_ref[i : i + 1] = ref[...]
    first = lax.axis_index("c") == 0
    out_ref[:, 0:128] = q_ref[...]
    out_ref[:, 128:256] = k_ref[...]
    out_ref[:, 256:384] = v_ref[...]
    out_ref[:, 384:512] = p_ref[...]
    gate = g_ref[...]
    out_ref[:, 512:640] = jnp.where(first, d_ref[...], gate[:, :128])
    out_ref[:, 640:768] = jnp.where(first, r_ref[...], gate[:, 128:])
    out_ref[:, 768:896] = oa_ref[...]
    out_ref[:, 896:1023] = op_ref[:, :127]
    spot = iota((32, LANES), 1) == lax.axis_index("y") * 32 + iota((32, LANES), 0)
    column = op_ref[...].astype(f32)[:, 127:128]
    line = jnp.sum(jnp.where(spot, column, 0.0), axis=0, keepdims=True)
    left_ref[...] = jnp.where(iota((16, LANES), 0) == 0, line, 0.0)


def partial_products(tok_ref, w_ref, part_ref):
    made = jnp.dot(tok_ref[...], w_ref[:, :768], preferred_element_type=f32).astype(bf16)
    for y in range(4):
        part_ref[y] = made[128 * y : 128 * y + 128]


def spread_columns(w_ref, out_ref):
    first = w_ref[:, 768:896]
    second = w_ref[:, 896:1023]
    for y in range(4):
        out_ref[y, :, 0:128] = first
        out_ref[y, :, 128:255] = second
        out_ref[y, :, 255:256] = jnp.zeros((512, 1), bf16)


def sum_parts(part_ref, main_ref, low_ref):
    total = part_ref[0].astype(f32)
    for y in range(1, 4):
        total = total + part_ref[y].astype(f32)
    rounded = total.astype(bf16)
    main_ref[...] = rounded[:, :512]
    low = rounded[:, 512:].astype(f32)
    first = lax.axis_index("c") == 0
    one = jnp.where(first, jnp.tanh(low[:, :128]), jax.nn.sigmoid(low[:, :128]))
    two = jnp.where(first, low[:, 128:], jax.nn.sigmoid(low[:, 128:]))
    low_ref[:, :128] = one.astype(bf16)
    low_ref[:, 128:] = two.astype(bf16)


def masked(x, lane_low):
    zero = jnp.zeros_like(x)
    return [jnp.where(lane_low, x, zero), jnp.where(lane_low, zero, x)]


def block_diagonal(pair):
    low = iota(pair.shape, 1) < HEAD
    zero = jnp.zeros_like(pair)
    return jnp.concatenate([jnp.where(low, pair, zero), jnp.where(low, zero, pair)], axis=0)


def block_maps(
    main_ref, low_ref, dw_ref, rw_ref, lines_ref, re_ref, de_ref, left_ref, pay_ref, solved_ref, hats_ref, first_ref, wide_ref,
):
    line = lambda i: lines_ref[i : i + 1]
    recept = main_ref[:, 0:128].astype(f32)
    keys = main_ref[:, 128:256].astype(f32)
    values_b = main_ref[:, 256:384]
    values = values_b.astype(f32)
    row = iota((ROWS, LANES), 0)
    col = iota((ROWS, LANES), 1)
    lane_low = col < HEAD
    same = (row // CHUNK) == (col // CHUNK)

    drive = line(0) + jnp.dot(low_ref[0, :, :128], dw_ref[...], preferred_element_type=f32)
    log_decay = -jax.nn.sigmoid(drive) * jnp.exp(re_ref[...] - 0.5) + de_ref[...]
    rate = jax.nn.sigmoid(
        line(1) + jnp.dot(low_ref[0, :, 128:], rw_ref[...], preferred_element_type=f32)
    )

    ones = jnp.where(same, 1.0, 0.0).astype(f32)
    unit = keys * line(2)
    effective = keys * (1.0 + (rate - 1.0) * line(3))
    sums = mm32(
        jnp.concatenate([unit * unit, recept * effective * line(4)], axis=0), ones
    )
    unit = unit * lax.rsqrt(sums[:ROWS] + 1e-06)
    wide_ref[1] = sums[ROWS:] * values
    beta = unit * rate

    tril = jnp.where(same & (row >= col), 1.0, 0.0).astype(f32)
    totals = mm32(jnp.concatenate([tril, ones], axis=0), log_decay)
    total, end = totals[:ROWS], totals[ROWS:]
    ref = 0.5 * end
    grow = jnp.exp(ref - total)
    shrink = jnp.exp(total - ref)
    base = jnp.exp(ref)
    a_hat = -unit * jnp.exp(total - log_decay - ref)
    r_hat = recept * shrink
    b_hat = beta * grow
    k_hat = effective * grow
    wide_ref[0] = r_hat * base
    hats_ref[0] = r_hat.astype(bf16)
    hats_ref[1] = b_hat.astype(bf16)
    hats_ref[2] = k_hat.astype(bf16)

    left = jnp.concatenate(masked(a_hat, lane_low), axis=0)
    right = jnp.concatenate([b_hat, k_hat], axis=0)
    scores = mm(left, right, NT)
    strict = same & (row > col)
    eye = jnp.where(row == col, 1.0, 0.0).astype(f32)
    within16 = (row // 16) == (col // 16)
    within32 = (row // 32) == (col // 32)
    swapped = pltpu.roll(a_hat * base, HEAD, 1)
    full = [jnp.where(strict, scores[h * ROWS : h * ROWS + ROWS, :ROWS], 0.0) for h in range(2)]
    power = [jnp.where(within16, full[h], 0.0) for h in range(2)]
    product = [eye + power[h] for h in range(2)]
    for _ in range(3):
        power = [mm32(power[h], power[h]) for h in range(2)]
        product = [product[h] + mm32(product[h], power[h]) for h in range(2)]
    for step in (
        [jnp.where(within32 & ~within16, full[h], 0.0) for h in range(2)],
        [jnp.where(within32, 0.0, full[h]) for h in range(2)],
    ):
        mid = [mm32(product[h], step[h]) for h in range(2)]
        product = [product[h] + mm32(mid[h], product[h]) for h in range(2)]
    solved = []
    for h in range(2):
        pushed = mm(jnp.where(strict, scores[h * ROWS : h * ROWS + ROWS, ROWS:], 0.0), values_b)
        rhs = jnp.where(lane_low if h == 0 else ~lane_low, pushed, swapped)
        solved.append(mm(product[h], rhs).astype(bf16))
        solved_ref[h] = solved[h]

    b_end = (b_hat * base).astype(bf16)
    k_end = (k_hat * base).astype(bf16)
    decay_end = jnp.exp(end)
    low64 = iota((CHUNK, LANES), 1) < HEAD
    diagonal = iota((CHUNK, LANES), 0) == (iota((CHUNK, LANES), 1) % HEAD)
    maps, states = [], []
    for c in range(2):
        at = slice(c * CHUNK, c * CHUNK + CHUNK)
        g0 = mm(solved[0][at], b_end[at], TN)
        g1 = mm(solved[1][at], b_end[at], TN)
        kv = mm(values_b[at], k_end[at], TN)
        maps.append(
            jnp.where(diagonal, decay_end[at], 0.0) + jnp.where(low64, g0[HEAD:], g1[:HEAD])
        )
        states.append(
            jnp.where(low64, g0[:HEAD], g1[HEAD:]) + jnp.where(low64, kv[:HEAD], kv[HEAD:])
        )
    chunk0 = jnp.concatenate([maps[0], states[0]], axis=0).astype(bf16)
    first_ref[...] = chunk0
    joined = mm(chunk0, block_diagonal(maps[1]))
    block_map = joined[:CHUNK].astype(bf16)
    block_state = (joined[CHUNK:] + states[1]).astype(bf16)
    tail = main_ref[ROWS - 16 :, 384:512].astype(f32)
    extra = jnp.where(row[:16] == 0, left_ref[...], tail).astype(bf16)
    for j in range(4):
        pay_ref[j, 0:64] = block_map
        pay_ref[j, 64:128] = block_state
        pay_ref[j, TAIL : TAIL + 16] = extra


def block_readings(main_ref, low_ref, gw_ref, solved_ref, hats_ref, first_ref, wide_ref, ymap_ref, out_ref):
    values_b = main_ref[:, 256:384]
    row = iota((ROWS, LANES), 0)
    col = iota((ROWS, LANES), 1)
    lane_low = col < HEAD
    upto = ((row // CHUNK) == (col // CHUNK)) & (row >= col)
    out_ref[1] = wide_ref[1]
    out_ref[2] = jnp.dot(low_ref[1], gw_ref[...], preferred_element_type=f32)
    scores = mm(
        jnp.concatenate(masked(hats_ref[0].astype(f32), lane_low), axis=0),
        jnp.concatenate([hats_ref[1], hats_ref[2]], axis=0),
        NT,
    )
    reads, direct = [], []
    for h in range(2):
        at = slice(h * ROWS, h * ROWS + ROWS)
        reads.append(mm(jnp.where(upto, scores[at, :ROWS], 0.0), solved_ref[h]))
        direct.append(mm(jnp.where(upto, scores[at, ROWS:], 0.0), values_b))
    y_local = jnp.where(lane_low, reads[0] + direct[0], reads[1] + direct[1])
    y_map = wide_ref[0] + pltpu.roll(jnp.where(lane_low, reads[1], reads[0]), HEAD, 1)
    first = first_ref[...].astype(f32)
    late = mm(
        y_map[CHUNK:],
        jnp.concatenate([block_diagonal(first[CHUNK:]), block_diagonal(first[:CHUNK])], axis=0),
        NT,
    )
    ymap_ref[:CHUNK] = y_map[:CHUNK].astype(bf16)
    ymap_ref[CHUNK:] = late[:, LANES:].astype(bf16)
    out_ref[0, :CHUNK] = y_local[:CHUNK]
    out_ref[0, CHUNK:] = y_local[CHUNK:] + late[:, :LANES]


def identity_pair():
    eye = iota((HEAD, LANES), 0) == (iota((HEAD, LANES), 1) % HEAD)
    return jnp.concatenate([jnp.where(eye, 1.0, 0.0).astype(f32), jnp.zeros((HEAD, LANES), f32)], 0)


def compose(earlier, later):
    moved = mm(earlier, block_diagonal(later[:HEAD]))
    return jnp.concatenate([moved[:HEAD], moved[HEAD:] + later[HEAD:]], axis=0)


def chain(first, others):
    made = [first]
    for other in others:
        made.append(compose(made[-1], other))
    return made


def chosen_before(made, mine):
    before = jnp.where(mine == 0, identity_pair(), made[0])
    for j in (1, 2):
        before = jnp.where(mine > j, made[j], before)
    return before


def tail_before(got_ref, mine):
    found = jnp.zeros((16, LANES), f32)
    for j in range(3):
        found = jnp.where(mine == j + 1, got_ref[j, TAIL : TAIL + 16].astype(f32), found)
    return found


def prefixes(got_ref, mine):
    pieces = [got_ref[j, :128].astype(f32) for j in range(4)]
    made = chain(pieces[0], pieces[1:])
    return chosen_before(made, mine), made[3].astype(bf16)


def stage_y(got_ref, pay_ref, before_ref, tail_ref):
    y = lax.axis_index("y")
    before, running = prefixes(got_ref, y)
    before_ref[...] = before
    tail_ref[...] = tail_before(got_ref, y)
    extras = [got_ref[j, TAIL : TAIL + 16].astype(f32) for j in range(4)]
    line = extras[0] + extras[1] + extras[2] + extras[3]
    extra = jnp.where(iota((16, LANES), 0) == 0, line, extras[3]).astype(bf16)
    for j in range(4):
        pay_ref[j, 0:128] = running
        pay_ref[j, TAIL : TAIL + 16] = extra


def stage_zl(got_ref, before_ref, tail_ref, pay_ref, out_before_ref, out_tail_ref):
    y, zl = lax.axis_index("y"), lax.axis_index("zl")
    before, running = prefixes(got_ref, zl)
    out_before_ref[...] = compose(before, before_ref[...])
    out_tail_ref[...] = jnp.where(y == 0, tail_before(got_ref, zl), tail_ref[...])
    row = iota((16, LANES), 0)
    left = jnp.zeros((16, LANES), f32)
    for j in range(4):
        left = jnp.where(row == j, got_ref[j, TAIL : TAIL + 16].astype(f32)[0:1], left)
    pay_ref[0:128] = running
    pay_ref[TAIL : TAIL + 16] = got_ref[3, TAIL : TAIL + 16]
    pay_ref[LEFT : LEFT + 16] = left.astype(bf16)


def finish(
    got_ref, before_ref, tail_ref, start_ref, ymap_ref, yloc_ref, lines_ref,
    pool_ref, matrix_ref, wout_ref, out_ref,
):
    zh, zl, y = lax.axis_index("zh"), lax.axis_index("zl"), lax.axis_index("y")
    state = jnp.concatenate([start_ref[0], start_ref[1]], axis=1)
    for j in range(3):
        piece = got_ref[j, :128].astype(f32)
        state = jnp.where(zh > j, mm(state, block_diagonal(piece[:HEAD])) + piece[HEAD:], state)
    state = mm(state, block_diagonal(before_ref[:HEAD])) + before_ref[HEAD:]
    reading = yloc_ref[0] + mm(ymap_ref[...], block_diagonal(state), NT)
    row = iota((ROWS, LANES), 0)
    col = iota((ROWS, LANES), 1)
    mean = jnp.where((row // HEAD) == (col // HEAD), 1.0 / HEAD, 0.0).astype(f32)
    off = reading - mm32(reading, mean)
    spread = mm32(off * off, mean)
    headed = off * lax.rsqrt(spread + 1e-05 * HEAD) * lines_ref[5:6] + lines_ref[6:7] + yloc_ref[1]
    attn = (headed * yloc_ref[2]).astype(bf16)

    pool = pool_ref[:, 384:512].astype(f32)
    tail = jnp.where((y == 0) & (zl == 0), tail_before(got_ref, zh), tail_ref[...])
    extended = jnp.concatenate([tail, pool], axis=0)
    level = lax.axis_index("x")
    sums = extended
    chosen = None
    for k in range(4):
        width = 1 << k
        shifted = pltpu.roll(sums, width, 0)
        sums = sums + jnp.where(iota(sums.shape, 0) < width, 0.0, shifted)
        picked = sums[16:]
        chosen = picked if k == 0 else jnp.where(level >= k, picked, chosen)
    window = lax.shift_left(jnp.int32(2), level).astype(f32)
    position = (((zh * 4 + zl) * 4 + y) * ROWS + row).astype(f32)
    pooled = (chosen / jnp.minimum(position + 1.0, window) - pool).astype(bf16)
    grouped = jnp.dot(pooled, matrix_ref[0], preferred_element_type=f32)
    pool_out = (grouped * lines_ref[7:8]).astype(bf16)

    acts = jnp.concatenate([attn, pool_out], axis=1)
    last = pool_out[:, 127:128].astype(f32)
    for zpair in range(8):
        rows = []
        for z in (2 * zpair, 2 * zpair + 1):
            for yy in range(4):
                rows.append(wout_ref[yy, 32 * z : 32 * z + 32])
        made = mm(acts, jnp.concatenate(rows, axis=0), NT)
        for half in range(2):
            z = 2 * zpair + half
            line = got_ref[z // 4, LEFT : LEFT + 16].astype(f32)[z % 4 : z % 4 + 1]
            out_ref[:, 128 * z : 128 * z + 128] = (
                made[:, 128 * half : 128 * half + 128] + last * line
            ).astype(bf16)


def add_parts(part_ref, out_ref):
    total = part_ref[0].astype(f32)
    for j in range(1, 8):
        total = total + part_ref[j].astype(f32)
    out_ref[...] = total.astype(bf16)


def on_device(
    tokens, input_norm_scale, input_norm_bias, query_projection, key_projection,
    value_projection, pooling_input_projection, decay_input_weight, rate_input_weight,
    gate_input_weight, decay_output_weight, rate_output_weight, gate_output_weight,
    decay_bias_base, learning_rate_base, key_prenorm_scale, key_learning_scale,
    self_term_weight, head_norm_scale, head_norm_bias, rate_extra_log, decay_extra_log,
    starting_head_state, pooling_group_matrix, pooling_output_scale, output_attention_rows,
    output_pooling_rows,
):
    line = lambda v: v.reshape(1, -1)
    sent = call(
        prepare_tokens, shaped((4, 128, 512), bf16),
        tokens, line(input_norm_scale), line(input_norm_bias), name="prepare_tokens",
        space=pltpu.HBM, vmem=60 * 2**20,
        scratch=[
            pltpu.VMEM((128, 2048), bf16), pltpu.VMEM((1, 2048), f32), pltpu.VMEM((1, 2048), f32),
            pltpu.SemaphoreType.DMA((4,)),
        ],
    )
    shard, left, lines = call(
        prepare_weights,
        [shaped((32, 1023), bf16), shaped((16, 128), f32), shaped((8, 128), f32)],
        query_projection, key_projection, value_projection, pooling_input_projection,
        decay_input_weight, rate_input_weight, gate_input_weight, output_attention_rows.T,
        output_pooling_rows.T, line(decay_bias_base), line(learning_rate_base),
        line(key_prenorm_scale), line(key_learning_scale), line(self_term_weight),
        line(head_norm_scale), line(head_norm_bias), line(pooling_output_scale),
        name="prepare_weights",
    )
    gathered = lax.all_gather(shard, Z, axis=0, tiled=True)
    mixed_tokens = lax.all_to_all(sent, "y", 0, 0, tiled=True).reshape(512, 512)
    parts = call(
        partial_products, shaped((4, 128, 768), bf16), mixed_tokens, gathered,
        name="partial_products",
    )
    parts = lax.all_to_all(parts, "y", 0, 0, tiled=True)
    main, low = call(
        sum_parts, [shaped((128, 512), bf16), shaped((128, 256), bf16)], parts, name="sum_parts"
    )
    low = lax.all_gather(low, "c", axis=0)
    pay, solved, hats, first, wide = call(
        block_maps,
        [
            shaped((4, PAY, 128), bf16), shaped((2, 128, 128), bf16), shaped((3, 128, 128), bf16),
            shaped((128, 128), bf16), shaped((2, 128, 128), f32),
        ],
        main, low, decay_output_weight, rate_output_weight, lines, rate_extra_log,
        decay_extra_log, left, name="block_maps",
    )
    columns, pay = lax.optimization_barrier((gathered, pay))
    got = lax.all_to_all(pay, "y", 0, 0, tiled=True)
    y_map, y_local = call(
        block_readings, [shaped((128, 128), bf16), shaped((3, 128, 128), f32)],
        main, low, gate_output_weight, solved, hats, first, wide, name="block_readings",
    )
    columns = call(spread_columns, shaped((4, 512, 256), bf16), columns, name="spread_columns")
    pay, before, tail = call(
        stage_y,
        [shaped((4, PAY, 128), bf16), shaped((128, 128), f32), shaped((16, 128), f32)],
        got, name="stage_y",
    )
    got = lax.all_to_all(pay, "zl", 0, 0, tiled=True)
    columns, got = lax.optimization_barrier((columns, got))
    columns = lax.all_to_all(columns, "y", 0, 0, tiled=True)
    pay, before, tail = call(
        stage_zl,
        [shaped((WIDE, 128), bf16), shaped((128, 128), f32), shaped((16, 128), f32)],
        got, before, tail, name="stage_zl",
    )
    got = lax.all_gather(pay, "zh", axis=0)
    out = call(
        finish, shaped((128, 2048), bf16),
        got, before, tail, starting_head_state, y_map, y_local, lines, main,
        pooling_group_matrix, columns, name="finish",
    )
    parts = lax.all_to_all(out.reshape(8, 16, 2048), TP, 0, 0, tiled=True)
    return call(add_parts, shaped((16, 2048), bf16), parts, name="add_parts")


def solution(mesh):
    split = Mesh(mesh.devices.reshape(4, 4, 4, 4, 2), ("zh", "zl", "y", "x", "c"))
    in_specs = (
        P(SP, None), P(), P(),
        P(SP, TP), P(SP, TP), P(SP, TP), P(SP, TP),
        P(SP, None), P(SP, None), P(SP, None),
        P(None, TP), P(None, TP), P(None, TP),
        P(TP), P(TP), P(TP), P(TP), P(TP), P(TP), P(TP),
        P(SP, TP), P(SP, TP),
        P(TP, None, None), P(TP, None, None), P(TP),
        P(TP, SP), P(TP, SP),
    )
    out_specs = P((*SP, *TP), None)
    return jax.shard_map(
        on_device, mesh=split, in_specs=in_specs, out_specs=out_specs, check_vma=False
    )
```

time: 167 us -> 131 us (0.78)
  waiting for transfers between devices: 17.8 us -> 3.62 us
  Pallas kernels: 22.8 us -> 12.7 us
  blocking collectives: 108 us -> 99.7 us
  local copies, waits for them, and re-layouts: 4.06 us -> 0.7 us
    all_to_all x2 -> x1, blocking collectives: 29.2 us -> 12.5 us  [on_device(): parts = lax.all_to_all(parts, 'y', 0, 0, tiled=True)]
    all_gather x0 -> x1, blocking collectives: none -> 15.6 us  [on_device(): got = lax.all_gather(pay, 'zh', axis=0)]
    all_to_all x2, waiting for transfers between devices: 17.8 us -> 3.62 us  [the longest x1 3.61 us: on_device(): got = lax.all_to_all(pay, 'zl', 0, 0, tiled=True)]
    pallas_call x8 -> x11, Pallas kernels: 22.8 us -> 12.7 us  [call(): pl.pallas_call(kernel, out_shape=outs, in_specs=[pl.BlockSpec(memory_spac...]
    all_gather x1, blocking collectives: 37.6 us -> 35 us  [on_device(): gathered = lax.all_gather(shard, Z, axis=0, tiled=True)]
    unnamed x12 -> x48, local copies, waits for them, and re-layouts: 3.19 us -> 0.7 us
    all_to_all x1, blocking collectives: 9.3 us -> 7.26 us  [on_device(): got = lax.all_to_all(pay, 'y', 0, 0, tiled=True)]
    all_gather x1, blocking collectives: 13 us -> 11.1 us  [on_device(): low = lax.all_gather(low, 'c', axis=0)]
  transfers between devices with their start and end apart: 3 -> 3, of which waited for: 2 -> 1; matrix products, arithmetic and copies ran while one was open for 1% -> 0% of each run, Pallas kernels for 2% -> 2%
where the time goes in v2:
time: 131 us; the launch traced here: 129 us
  blocking collectives  99.7 us (76%)
  Pallas kernels  12.7 us (10%)
  starting transfers between devices  12 us (9%)
  waiting for transfers between devices  3.62 us (3%)
    all_gather x1, blocking collectives, on_device(): gathered = lax.all_gather(shard, Z, axis=0, tiled=True)  35 us
    all_to_all x1, blocking collectives, on_device(): parts = lax.all_to_all(out.reshape(8, 16, 2048), TP, 0, 0, tiled=True)  18.2 us
    all_gather x1, blocking collectives, on_device(): got = lax.all_gather(pay, 'zh', axis=0)  15.6 us
    pallas_call x11, Pallas kernels, call(): pl.pallas_call(kernel, out_shape=outs, in_specs=[pl.BlockSpec(memory_spac...  12.7 us
    all_to_all x1, blocking collectives, on_device(): parts = lax.all_to_all(parts, 'y', 0, 0, tiled=True)  12.5 us
    all_gather x1, blocking collectives, on_device(): low = lax.all_gather(low, 'c', axis=0)  11.1 us
    all_to_all x1, blocking collectives, on_device(): got = lax.all_to_all(pay, 'y', 0, 0, tiled=True)  7.26 us
    all_to_all x1, starting transfers between devices, on_device(): mixed_tokens = lax.all_to_all(sent, 'y', 0, 0, tiled=True).reshape(512, 512)  5.14 us
  transfers between devices with their start and end apart: 3, of which 1 were waited for; matrix products, arithmetic and copies ran while one was open for 0% of the time, Pallas kernels for 2%

profile of v2, /device:TPU:1, one launch (start us, length us, event | category | flops | bytes accessed | tf_op | source)
XLA Modules:
  0.0 129.0 jit_solution(4575661358995532188)
XLA Ops:
  0.0 3.2 %prepare_tokens.1 = bf16[4,128,512]{2,1,0:T(8,128)(2,1)} custom-call(bf16[128,2048]{1,0:T(8,128)(2,1)} %tok_hbm.1, f32[1,2048]{1,0:T(1,128)} %bitcast.31, f32[1,2048]{1,0:T(1,128)} %bitcast.32), custom_call_target="tpu_custom_call" | custom-call | flops 100000000 | bytes 540672 | tf_op jit(solution)/shard_map/prepare_tokens/pallas_call | solution.py:43
  3.2 0.0 copy-start.8
  3.2 0.0 copy-start.9
  3.2 0.0 copy-start.10
  3.2 0.0 copy-start.11
  3.2 0.0 copy-start.12
  3.2 0.0 copy-start.13
  3.2 0.0 copy-start.14
  3.2 0.0 copy-start.15
  3.3 0.0 copy-start.19
  3.3 0.0 copy-start.20
  3.3 0.0 copy-start.21
  3.3 0.0 copy-start.22
  3.3 0.0 copy-start.23
  3.3 5.1 %all-to-all-start = ((bf16[4,128,512]{2,1,0:T(8,128)(2,1)}), bf16[4,128,512]{2,1,0:T(8,128)(2,1)S(1)}, u32[]{:S(2)}, u32[]{:S(2)}) async-start(bf16[4,128,512]{2,1,0:T(8,128)(2,1)} %prepare_tokens.1), calls=%async_computation | async-start | bytes 1048576 | tf_op jit(solution)/shard_map/all_to_all | solution.py:442
  8.5 0.0 copy-start.18
  8.5 0.0 copy-done.8
  8.5 0.0 copy-done.9
  8.5 0.0 copy-done.10
  8.5 0.0 copy-done.11
  8.5 0.0 copy-done.12
  8.5 0.0 copy-done.13
  8.5 0.0 copy-done.14
  8.6 0.0 copy-done.15
  8.6 0.0 copy-done.19
  8.6 0.0 copy-done.20
  8.6 0.0 copy-done.21
  8.6 0.0 copy-done.22
  8.6 0.0 copy-done.23
  8.6 0.6 copy-done.7
  9.2 0.0 copy-done.16
  9.2 0.0 copy-done.17
  9.2 0.0 copy-done.18
  9.2 0.1 prepare_weights.1
  9.3 35.0 %all_gather.15.w_ref = bf16[512,1023]{1,0:T(8,128)(2,1)S(1)} all-gather(bf16[32,1023]{1,0:T(8,128)(2,1)S(1)} %get-tuple-element.27), channel_id=1, replica_groups=mesh['zh'=4,'zl'=4,'y'=4,'x'=4,'c'=2] {'zh','zl'}, dimensions={0}, use_global_device_ids=true | all-gather | bytes 1113024 | tf_op jit(solution)/shard_map/all_gather | solution.py:441
  44.3 0.0 all-to-all-done
  44.3 0.6 partial_products.1
  44.8 12.5 %all_to_all.30.part_ref = bf16[4,128,768]{2,1,0:T(8,128)(2,1)S(1)} all-to-all(bf16[4,128,768]{2,1,0:T(8,128)(2,1)S(1)} %partial_products.1), channel_id=1, replica_groups=mesh['zh'=4,'zl'=4,'y'=4,'x'=4,'c'=2] {'y'}, dimensions={0} | all-to-all | bytes 1572864 | tf_op jit(solution)/shard_map/all_to_all | solution.py:447
  57.3 0.1 sum_parts.1
  57.4 0.0 copy-start
  57.4 0.0 copy-start.1
  57.5 0.0 copy-start.5
  57.5 0.0 copy-start.6
  57.5 11.1 %all-gather = bf16[256,256]{1,0:T(8,128)(2,1)S(1)} all-gather(bf16[128,256]{1,0:T(8,128)(2,1)S(1)} %get-tuple-element.29), channel_id=2, replica_groups=mesh['zh'=4,'zl'=4,'y'=4,'x'=4,'c'=2] {'c'}, dimensions={0}, use_global_device_ids=true | all-gather | bytes 196608 | tf_op jit(solution)/shard_map/all_gather | solution.py:451
  68.6 0.0 copy-done
  68.6 0.0 copy-done.1
  68.6 0.0 copy-done.5
  68.6 0.0 copy-done.6
  68.6 3.3 %block_maps.1 = (bf16[4,144,128]{2,1,0:T(8,128)(2,1)S(1)}, bf16[2,128,128]{2,1,0:T(8,128)(2,1)S(1)}, bf16[3,128,128]{2,1,0:T(8,128)(2,1)S(1)}, bf16[128,128]{1,0:T(8,128)(2,1)S(1)}, f32[2,128,128]{2,1,0:T(8,128)S(1)}) custom-call(bf16[128,512]{1,0:T(8,128)(2,1)S(1)} %get-tuple-element.28.main_ref.pool_ref, bf16[2,128,256]{2,1,0:T(8,128)(2,1)S(1)} %bitcast.18, ...), custom_call_target="tpu_custom_call" | custom-call | flops 100000000 | bytes 471040 | tf_op jit(solution)/shard_map/block_maps/pallas_call | solution.py:43
  72.0 7.3 %all_to_all.31.got_ref = bf16[4,144,128]{2,1,0:T(8,128)(2,1)S(1)} all-to-all(bf16[4,144,128]{2,1,0:T(8,128)(2,1)S(1)} %get-tuple-element.34), channel_id=1, replica_groups=mesh['zh'=4,'zl'=4,'y'=4,'x'=4,'c'=2] {'y'}, dimensions={0} | all-to-all | bytes 294912 | tf_op jit(solution)/shard_map/all_to_all | solution.py:462
  79.3 1.1 stage_y.1
  80.3 3.3 %all-to-all-start.3 = ((bf16[4,144,128]{2,1,0:T(8,128)(2,1)}), bf16[4,144,128]{2,1,0:T(8,128)(2,1)S(1)}, u32[]{:S(2)}, u32[]{:S(2)}) async-start(bf16[4,144,128]{2,1,0:T(8,128)(2,1)} %get-tuple-element.35), calls=%async_computation.3 | async-start | bytes 294912 | tf_op jit(solution)/shard_map/all_to_all | solution.py:473
  83.7 1.2 spread_columns.1
  84.8 3.6 %all-to-all-done.3.got_ref = bf16[4,144,128]{2,1,0:T(8,128)(2,1)S(1)} async-done(((bf16[4,144,128]{2,1,0:T(8,128)(2,1)}), bf16[4,144,128]{2,1,0:T(8,128)(2,1)S(1)}, u32[]{:S(2)}, u32[]{:S(2)}) %all-to-all-start.3) | async-done | bytes 147488 | tf_op jit(solution)/shard_map/all_to_all | solution.py:473
  88.5 3.5 %all-to-all-start.4 = ((bf16[4,512,256]{2,1,0:T(8,128)(2,1)}), bf16[4,512,256]{2,1,0:T(8,128)(2,1)S(1)}, u32[]{:S(2)}, u32[]{:S(2)}) async-start(bf16[4,512,256]{2,1,0:T(8,128)(2,1)} %spread_columns.1), calls=%async_computation.4 | async-start | bytes 2097152 | tf_op jit(solution)/shard_map/all_to_all | solution.py:475
  92.0 0.0 copy-done.2
  92.0 0.5 block_readings.1
  92.5 0.4 stage_zl.1
  92.9 0.0 copy-start.4
  92.9 15.6 %all-gather.1 = bf16[640,128]{1,0:T(8,128)(2,1)S(1)} all-gather(bf16[160,128]{1,0:T(8,128)(2,1)S(1)} %get-tuple-element.39), channel_id=3, replica_groups=mesh['zh'=4,'zl'=4,'y'=4,'x'=4,'c'=2] {'zh'}, dimensions={0}, use_global_device_ids=true | all-gather | bytes 204800 | tf_op jit(solution)/shard_map/all_gather | solution.py:481
  108.6 0.0 all-to-all-done.4.wout_ref
  108.6 1.5 %finish.1 = bf16[128,2048]{1,0:T(8,128)(2,1)S(1)} custom-call(bf16[4,160,128]{2,1,0:T(8,128)(2,1)S(1)} %bitcast.20, f32[128,128]{1,0:T(8,128)S(1)} %get-tuple-element.40.before_ref, f32[16,128]{1,0:T(8,128)S(1)} %get-tuple-element.41.tail_ref, f32[2,64,64]{2,1,0:T(8,128)S(1)} %copy-done.3, bf16[128,128]{1,0:T(8,128)(2,1)S(1)} %get-tuple-element.46.ymap_ref, ...), custom_call_target="tpu_custom_call" | custom-call | flops 100000000 | bytes 1716224 | tf_op jit(solution)/shard_map/finish/pallas_call | solution.py:43
  110.1 18.2 %all_to_all.32.part_ref = bf16[8,16,2048]{2,1,0:T(8,128)(2,1)S(1)} all-to-all(bf16[8,16,2048]{2,1,0:T(8,128)(2,1)S(1)} %bitcast.16), channel_id=1, replica_groups=mesh['zh'=4,'zl'=4,'y'=4,'x'=4,'c'=2] {'x','c'}, dimensions={0} | all-to-all | bytes 1048576 | tf_op jit(solution)/shard_map/all_to_all | solution.py:487
  128.3 0.7 add_parts.1
  (7 shorter events, 0.0 us)
Async XLA Ops:
  3.2 5.3 %copy-start.8 = (bf16[32,128]{1,0:T(8,128)(2,1)S(1)}, bf16[32,128]{1,0:T(8,128)(2,1)}, u32[]{:S(2)}) copy-start(bf16[32,128]{1,0:T(8,128)(2,1)} %q_ref.1) | copy-start | bytes 24580
  3.2 5.3 %copy-start.9 = (bf16[32,128]{1,0:T(8,128)(2,1)S(1)}, bf16[32,128]{1,0:T(8,128)(2,1)}, u32[]{:S(2)}) copy-start(bf16[32,128]{1,0:T(8,128)(2,1)} %k_ref.1) | copy-start | bytes 24580
  3.2 5.3 %copy-start.10 = (bf16[32,128]{1,0:T(8,128)(2,1)S(1)}, bf16[32,128]{1,0:T(8,128)(2,1)}, u32[]{:S(2)}) copy-start(bf16[32,128]{1,0:T(8,128)(2,1)} %v_ref.1) | copy-start | bytes 24580
  3.2 5.3 %copy-start.11 = (bf16[32,128]{1,0:T(8,128)(2,1)S(1)}, bf16[32,128]{1,0:T(8,128)(2,1)}, u32[]{:S(2)}) copy-start(bf16[32,128]{1,0:T(8,128)(2,1)} %p_ref.1) | copy-start | bytes 24580
  3.2 5.3 %copy-start.12 = (bf16[32,128]{1,0:T(8,128)(2,1)S(1)}, bf16[32,128]{1,0:T(8,128)(2,1)}, u32[]{:S(2)}) copy-start(bf16[32,128]{1,0:T(8,128)(2,1)} %d_ref.1) | copy-start | bytes 24580
  3.2 5.3 %copy-start.13 = (bf16[32,128]{1,0:T(8,128)(2,1)S(1)}, bf16[32,128]{1,0:T(8,128)(2,1)}, u32[]{:S(2)}) copy-start(bf16[32,128]{1,0:T(8,128)(2,1)} %r_ref.1) | copy-start | bytes 24580
  3.2 5.3 %copy-start.14 = (bf16[128,32]{0,1:T(8,128)(2,1)S(1)}, bf16[128,32]{0,1:T(8,128)(2,1)}, u32[]{:S(2)}) copy-start(bf16[128,32]{0,1:T(8,128)(2,1)} %param.52) | copy-start | bytes 24580
  3.2 5.3 %copy-start.15 = (bf16[128,32]{0,1:T(8,128)(2,1)S(1)}, bf16[128,32]{0,1:T(8,128)(2,1)}, u32[]{:S(2)}) copy-start(bf16[128,32]{0,1:T(8,128)(2,1)} %param.53) | copy-start | bytes 24580
  3.3 5.3 %copy-start.19 = (f32[128]{0:T(128)S(1)}, f32[128]{0:T(128)}, u32[]{:S(2)}) copy-start(f32[128]{0:T(128)} %param.43) | copy-start | bytes 1540
  3.3 5.3 %copy-start.20 = (f32[128]{0:T(128)S(1)}, f32[128]{0:T(128)}, u32[]{:S(2)}) copy-start(f32[128]{0:T(128)} %param.44) | copy-start | bytes 1540
  3.3 5.3 %copy-start.21 = (f32[128]{0:T(128)S(1)}, f32[128]{0:T(128)}, u32[]{:S(2)}) copy-start(f32[128]{0:T(128)} %param.45) | copy-start | bytes 1540
  3.3 5.3 %copy-start.22 = (f32[128]{0:T(128)S(1)}, f32[128]{0:T(128)}, u32[]{:S(2)}) copy-start(f32[128]{0:T(128)} %param.46) | copy-start | bytes 1540
  3.3 5.3 %copy-start.23 = (f32[128]{0:T(128)S(1)}, f32[128]{0:T(128)}, u32[]{:S(2)}) copy-start(f32[128]{0:T(128)} %param.51) | copy-start | bytes 1540
  3.3 40.9 %all-to-all-start = ((bf16[4,128,512]{2,1,0:T(8,128)(2,1)}), bf16[4,128,512]{2,1,0:T(8,128)(2,1)S(1)}, u32[]{:S(2)}, u32[]{:S(2)}) async-start(bf16[4,128,512]{2,1,0:T(8,128)(2,1)} %prepare_tokens.1), calls=%async_computation | async-start | bytes 1048576 | tf_op jit(solution)/shard_map/all_to_all | solution.py:442
  8.5 0.7 copy-start.7
  8.5 0.7 copy-start.16
  8.5 0.7 copy-start.17
  8.5 0.7 copy-start.18
  57.4 11.2 %copy-start = (f32[128,128]{1,0:T(8,128)S(1)}, f32[128,128]{1,0:T(8,128)}, u32[]{:S(2)}) copy-start(f32[128,128]{1,0:T(8,128)} %re_ref.1) | copy-start | bytes 196612
  57.4 11.2 %copy-start.1 = (f32[128,128]{1,0:T(8,128)S(1)}, f32[128,128]{1,0:T(8,128)}, u32[]{:S(2)}) copy-start(f32[128,128]{1,0:T(8,128)} %de_ref.1) | copy-start | bytes 196612
  57.5 11.2 %copy-start.5 = (bf16[128,128]{1,0:T(8,128)(2,1)S(1)}, bf16[128,128]{1,0:T(8,128)(2,1)}, u32[]{:S(2)}) copy-start(bf16[128,128]{1,0:T(8,128)(2,1)} %dw_ref.1) | copy-start | bytes 98308
  57.5 11.2 %copy-start.6 = (bf16[128,128]{1,0:T(8,128)(2,1)S(1)}, bf16[128,128]{1,0:T(8,128)(2,1)}, u32[]{:S(2)}) copy-start(bf16[128,128]{1,0:T(8,128)(2,1)} %rw_ref.1) | copy-start | bytes 98308
  80.3 8.1 %all-to-all-start.3 = ((bf16[4,144,128]{2,1,0:T(8,128)(2,1)}), bf16[4,144,128]{2,1,0:T(8,128)(2,1)S(1)}, u32[]{:S(2)}, u32[]{:S(2)}) async-start(bf16[4,144,128]{2,1,0:T(8,128)(2,1)} %get-tuple-element.35), calls=%async_computation.3 | async-start | bytes 294912 | tf_op jit(solution)/shard_map/all_to_all | solution.py:473
  84.8 7.1 %copy-start.2 = (bf16[256,128]{1,0:T(8,128)(2,1)S(1)}, bf16[256,128]{1,0:T(8,128)(2,1)}, u32[]{:S(2)}) copy-start(bf16[256,128]{1,0:T(8,128)(2,1)} %gw_ref.1) | copy-start | bytes 196612
  88.5 20.1 %all-to-all-start.4 = ((bf16[4,512,256]{2,1,0:T(8,128)(2,1)}), bf16[4,512,256]{2,1,0:T(8,128)(2,1)S(1)}, u32[]{:S(2)}, u32[]{:S(2)}) async-start(bf16[4,512,256]{2,1,0:T(8,128)(2,1)} %spread_columns.1), calls=%async_computation.4 | async-start | bytes 2097152 | tf_op jit(solution)/shard_map/all_to_all | solution.py:475
  92.9 15.7 %copy-start.3 = (f32[2,64,64]{2,1,0:T(8,128)S(1)}, f32[2,64,64]{2,1,0:T(8,128)}, u32[]{:S(2)}) copy-start(f32[2,64,64]{2,1,0:T(8,128)} %start_ref.1) | copy-start | bytes 98308
  92.9 15.7 %copy-start.4 = (bf16[1,128,128]{2,1,0:T(8,128)(2,1)S(1)}, bf16[1,128,128]{2,1,0:T(8,128)(2,1)}, u32[]{:S(2)}) copy-start(bf16[1,128,128]{2,1,0:T(8,128)(2,1)} %matrix_ref.1) | copy-start | bytes 98308

commit v3 on v2

--- a/solution.py
+++ b/solution.py
@@ -21,7 +21,6 @@
 WIDE = 160
 TAIL = 128
 LEFT = 144
-HIGHEST = lax.Precision.HIGHEST
 NT = (((1,), (1,)), ((), ()))
 TN = (((0,), (0,)), ((), ()))
 
@@ -34,8 +33,39 @@
     return lax.dot_general(a.astype(bf16), b.astype(bf16), dims, preferred_element_type=f32)
 
 
-def mm32(a, b):
-    return jnp.dot(a, b, preferred_element_type=f32, precision=HIGHEST)
+def split(x, parts):
+    found = []
+    for _ in range(parts):
+        piece = x.astype(bf16)
+        found.append(piece)
+        x = x - piece.astype(f32)
+    return found
+
+
+def mm_exact_right(x, exact):
+    return jnp.dot(
+        jnp.concatenate(split(x, 3), axis=1),
+        jnp.concatenate([exact] * 3, axis=0),
+        preferred_element_type=f32,
+    )
+
+
+def mm_exact_left(exact, x):
+    return jnp.dot(
+        jnp.concatenate([exact] * 3, axis=1),
+        jnp.concatenate(split(x, 3), axis=0),
+        preferred_element_type=f32,
+    )
+
+
+def mm_wide(a, b):
+    a0, a1 = split(a, 2)
+    b0, b1 = split(b, 2)
+    return jnp.dot(
+        jnp.concatenate([a0, a0, a1], axis=1),
+        jnp.concatenate([b0, b1, b0], axis=0),
+        preferred_element_type=f32,
+    )
 
 
 def call(kernel, outs, *args, flops=10**8, name=None, vmem=16 * 2**20, space=pltpu.VMEM, scratch=()):
@@ -56,45 +86,40 @@
     return jax.ShapeDtypeStruct(shape, dtype)
 
 
-def prepare_tokens(tok_hbm, gain_hbm, bias_hbm, out_ref, tok, gain, bias, sems):
-    halves = [
-        pltpu.make_async_copy(
-            tok_hbm.at[pl.ds(64 * i, 64)], tok.at[pl.ds(64 * i, 64)], sems.at[i]
-        )
-        for i in range(2)
+def prepare_tokens(tok_hbm, gain_hbm, bias_hbm, *rest):
+    *vectors, out_ref, lines_ref, tok, gain, bias, sems = rest
+    lines = [
+        pltpu.make_async_copy(ref, lines_ref.at[pl.ds(i, 1)], sems.at[3 + i])
+        for i, ref in enumerate(vectors)
     ]
-    first = pltpu.make_async_copy(gain_hbm, gain, sems.at[2])
-    second = pltpu.make_async_copy(bias_hbm, bias, sems.at[3])
-    for copy in (halves[0], first, second, halves[1]):
+    copies = [
+        pltpu.make_async_copy(tok_hbm, tok, sems.at[0]),
+        pltpu.make_async_copy(gain_hbm, gain, sems.at[1]),
+        pltpu.make_async_copy(bias_hbm, bias, sems.at[2]),
+        *lines,
+    ]
+    for copy in copies:
         copy.start()
     source = iota((512, 512), 0)
     target = iota((512, 512), 1)
     moved = ((source >> 5) & 3) * 128 + (source >> 7) * 32 + (source & 31)
     pick = jnp.where(moved == target, 1.0, 0.0).astype(bf16)
-    for i in range(2):
-        halves[i].wait()
-        if i == 0:
-            first.wait()
-            second.wait()
-        rows = slice(64 * i, 64 * i + 64)
-        wide = tok[rows].astype(f32)
-        center = jnp.mean(wide, axis=-1, keepdims=True)
-        off = wide - center
-        spread = jnp.mean(jnp.square(off), axis=-1, keepdims=True)
-        normed = (off * lax.rsqrt(spread + 1e-05) * gain[...] + bias[...]).astype(bf16)
-        for j in range(4):
-            turned = jnp.dot(normed[:, 512 * j : 512 * j + 512], pick, preferred_element_type=f32)
-            turned = turned.astype(bf16)
-            for y in range(4):
-                out_ref[y, rows, 128 * j : 128 * j + 128] = turned[:, 128 * y : 128 * y + 128]
+    for copy in copies:
+        copy.wait()
+    wide = tok[...].astype(f32)
+    center = jnp.mean(wide, axis=-1, keepdims=True)
+    off = wide - center
+    spread = jnp.mean(jnp.square(off), axis=-1, keepdims=True)
+    normed = (off * lax.rsqrt(spread + 1e-05) * gain[...] + bias[...]).astype(bf16)
+    for j in range(4):
+        turned = jnp.dot(normed[:, 512 * j : 512 * j + 512], pick, preferred_element_type=f32)
+        for y in range(4):
+            out_ref[y, :, 128 * j : 128 * j + 128] = turned[:, 128 * y : 128 * y + 128].astype(bf16)
 
 
 def prepare_weights(
-    q_ref, k_ref, v_ref, p_ref, d_ref, r_ref, g_ref, oa_ref, op_ref, *rest
+    q_ref, k_ref, v_ref, p_ref, d_ref, r_ref, g_ref, oa_ref, op_ref, out_ref, left_ref
 ):
-    *lines, out_ref, left_ref, lines_ref = rest
-    for i, ref in enumerate(lines):
-        lines_ref[i : i + 1] = ref[...]
     first = lax.axis_index("c") == 0
     out_ref[:, 0:128] = q_ref[...]
     out_ref[:, 128:256] = k_ref[...]
@@ -158,7 +183,6 @@
     recept = main_ref[:, 0:128].astype(f32)
     keys = main_ref[:, 128:256].astype(f32)
     values_b = main_ref[:, 256:384]
-    values = values_b.astype(f32)
     row = iota((ROWS, LANES), 0)
     col = iota((ROWS, LANES), 1)
     lane_low = col < HEAD
@@ -170,18 +194,15 @@
         line(1) + jnp.dot(low_ref[0, :, 128:], rw_ref[...], preferred_element_type=f32)
     )
 
-    ones = jnp.where(same, 1.0, 0.0).astype(f32)
+    ones = jnp.where(same, 1.0, 0.0).astype(bf16)
     unit = keys * line(2)
     effective = keys * (1.0 + (rate - 1.0) * line(3))
-    sums = mm32(
-        jnp.concatenate([unit * unit, recept * effective * line(4)], axis=0), ones
-    )
-    unit = unit * lax.rsqrt(sums[:ROWS] + 1e-06)
-    wide_ref[1] = sums[ROWS:] * values
+    unit = unit * lax.rsqrt(mm_exact_right(unit * unit, ones) + 1e-06)
+    wide_ref[1] = recept * effective
     beta = unit * rate
 
-    tril = jnp.where(same & (row >= col), 1.0, 0.0).astype(f32)
-    totals = mm32(jnp.concatenate([tril, ones], axis=0), log_decay)
+    tril = jnp.where(same & (row >= col), 1.0, 0.0).astype(bf16)
+    totals = mm_exact_left(jnp.concatenate([tril, ones], axis=0), log_decay)
     total, end = totals[:ROWS], totals[ROWS:]
     ref = 0.5 * end
     grow = jnp.exp(ref - total)
@@ -201,21 +222,17 @@
     scores = mm(left, right, NT)
     strict = same & (row > col)
     eye = jnp.where(row == col, 1.0, 0.0).astype(f32)
-    within16 = (row // 16) == (col // 16)
-    within32 = (row // 32) == (col // 32)
     swapped = pltpu.roll(a_hat * base, HEAD, 1)
     full = [jnp.where(strict, scores[h * ROWS : h * ROWS + ROWS, :ROWS], 0.0) for h in range(2)]
-    power = [jnp.where(within16, full[h], 0.0) for h in range(2)]
+    within = {n: (row // n) == (col // n) for n in (8, 16, 32)}
+    power = [jnp.where(within[8], full[h], 0.0) for h in range(2)]
     product = [eye + power[h] for h in range(2)]
-    for _ in range(3):
-        power = [mm32(power[h], power[h]) for h in range(2)]
-        product = [product[h] + mm32(product[h], power[h]) for h in range(2)]
-    for step in (
-        [jnp.where(within32 & ~within16, full[h], 0.0) for h in range(2)],
-        [jnp.where(within32, 0.0, full[h]) for h in range(2)],
-    ):
-        mid = [mm32(product[h], step[h]) for h in range(2)]
-        product = [product[h] + mm32(mid[h], product[h]) for h in range(2)]
+    for _ in range(2):
+        power = [mm_wide(power[h], power[h]) for h in range(2)]
+        product = [product[h] + mm_wide(product[h], power[h]) for h in range(2)]
+    for here in (within[16] & ~within[8], within[32] & ~within[16], ~within[32]):
+        mid = [mm_wide(product[h], jnp.where(here, full[h], 0.0)) for h in range(2)]
+        product = [product[h] + mm_wide(mid[h], product[h]) for h in range(2)]
     solved = []
     for h in range(2):
         pushed = mm(jnp.where(strict, scores[h * ROWS : h * ROWS + ROWS, ROWS:], 0.0), values_b)
@@ -253,13 +270,39 @@
         pay_ref[j, TAIL : TAIL + 16] = extra
 
 
-def block_readings(main_ref, low_ref, gw_ref, solved_ref, hats_ref, first_ref, wide_ref, ymap_ref, out_ref):
+def pool_rows(extended, own, place, matrix, scale):
+    level = lax.axis_index("x")
+    sums = extended
+    chosen = None
+    for k in range(4):
+        width = 1 << k
+        sums = sums + pltpu.roll(sums, width, 0)
+        picked = sums[16:]
+        chosen = picked if k == 0 else jnp.where(level >= k, picked, chosen)
+    window = lax.shift_left(jnp.int32(2), level).astype(f32)
+    position = (place + iota(own.shape, 0)).astype(f32)
+    pooled = (chosen / jnp.minimum(position + 1.0, window) - own).astype(bf16)
+    return jnp.dot(pooled, matrix, preferred_element_type=f32) * scale
+
+
+def block_readings(
+    main_ref, low_ref, gw_ref, solved_ref, hats_ref, first_ref, wide_ref, lines_ref, matrix_ref,
+    ymap_ref, out_ref, pool_ref,
+):
+    pool = main_ref[:, 384:512].astype(f32)
+    place = ((lax.axis_index("zh") * 4 + lax.axis_index("zl")) * 4 + lax.axis_index("y")) * ROWS
+    pool_ref[0:16] = jnp.zeros((16, LANES), bf16)
+    pool_ref[16:] = pool_rows(
+        pool, pool[16:], place + 16, matrix_ref[0], lines_ref[6:7]
+    ).astype(bf16)
     values_b = main_ref[:, 256:384]
     row = iota((ROWS, LANES), 0)
     col = iota((ROWS, LANES), 1)
     lane_low = col < HEAD
     upto = ((row // CHUNK) == (col // CHUNK)) & (row >= col)
-    out_ref[1] = wide_ref[1]
+    heads = (row // HEAD) == (col // HEAD)
+    ones = jnp.where(heads, 1.0, 0.0).astype(bf16)
+    out_ref[1] = mm_exact_right(wide_ref[1] * lines_ref[7:8], ones) * values_b.astype(f32)
     out_ref[2] = jnp.dot(low_ref[1], gw_ref[...], preferred_element_type=f32)
     scores = mm(
         jnp.concatenate(masked(hats_ref[0].astype(f32), lane_low), axis=0),
@@ -281,8 +324,9 @@
     )
     ymap_ref[:CHUNK] = y_map[:CHUNK].astype(bf16)
     ymap_ref[CHUNK:] = late[:, LANES:].astype(bf16)
-    out_ref[0, :CHUNK] = y_local[:CHUNK]
-    out_ref[0, CHUNK:] = y_local[CHUNK:] + late[:, :LANES]
+    y_local = jnp.concatenate([y_local[:CHUNK], y_local[CHUNK:] + late[:, :LANES]], axis=0)
+    mean = jnp.where(heads, 1.0 / HEAD, 0.0).astype(bf16)
+    out_ref[0] = y_local - mm_exact_right(y_local, mean)
 
 
 def identity_pair():
@@ -351,40 +395,33 @@
 
 def finish(
     got_ref, before_ref, tail_ref, start_ref, ymap_ref, yloc_ref, lines_ref,
-    pool_ref, matrix_ref, wout_ref, out_ref,
+    main_ref, pool_ref, matrix_ref, wout_ref, out_ref,
 ):
     zh, zl, y = lax.axis_index("zh"), lax.axis_index("zl"), lax.axis_index("y")
     state = jnp.concatenate([start_ref[0], start_ref[1]], axis=1)
-    for j in range(3):
-        piece = got_ref[j, :128].astype(f32)
-        state = jnp.where(zh > j, mm(state, block_diagonal(piece[:HEAD])) + piece[HEAD:], state)
-    state = mm(state, block_diagonal(before_ref[:HEAD])) + before_ref[HEAD:]
-    reading = yloc_ref[0] + mm(ymap_ref[...], block_diagonal(state), NT)
+    pieces = [got_ref[j, :128].astype(f32) for j in range(3)]
+    advance = lambda old, piece: mm(old, block_diagonal(piece[:HEAD])) + piece[HEAD:]
+    both = compose(pieces[1], pieces[2])
+    state = jnp.where(zh > 0, advance(state, pieces[0]), state)
+    after = jnp.where(zh > 2, both, pieces[1])
+    state = jnp.where(zh > 1, advance(state, after), state)
+    state = advance(state, before_ref[...])
+    state = state - jnp.mean(state, axis=0, keepdims=True)
+    off = yloc_ref[0] + mm(ymap_ref[...], block_diagonal(state), NT)
     row = iota((ROWS, LANES), 0)
     col = iota((ROWS, LANES), 1)
-    mean = jnp.where((row // HEAD) == (col // HEAD), 1.0 / HEAD, 0.0).astype(f32)
-    off = reading - mm32(reading, mean)
-    spread = mm32(off * off, mean)
-    headed = off * lax.rsqrt(spread + 1e-05 * HEAD) * lines_ref[5:6] + lines_ref[6:7] + yloc_ref[1]
+    mean = jnp.where((row // HEAD) == (col // HEAD), 1.0 / HEAD, 0.0).astype(bf16)
+    spread = mm_exact_right(off * off, mean)
+    headed = off * lax.rsqrt(spread + 1e-05 * HEAD) * lines_ref[4:5] + lines_ref[5:6] + yloc_ref[1]
     attn = (headed * yloc_ref[2]).astype(bf16)
 
-    pool = pool_ref[:, 384:512].astype(f32)
     tail = jnp.where((y == 0) & (zl == 0), tail_before(got_ref, zh), tail_ref[...])
-    extended = jnp.concatenate([tail, pool], axis=0)
-    level = lax.axis_index("x")
-    sums = extended
-    chosen = None
-    for k in range(4):
-        width = 1 << k
-        shifted = pltpu.roll(sums, width, 0)
-        sums = sums + jnp.where(iota(sums.shape, 0) < width, 0.0, shifted)
-        picked = sums[16:]
-        chosen = picked if k == 0 else jnp.where(level >= k, picked, chosen)
-    window = lax.shift_left(jnp.int32(2), level).astype(f32)
-    position = (((zh * 4 + zl) * 4 + y) * ROWS + row).astype(f32)
-    pooled = (chosen / jnp.minimum(position + 1.0, window) - pool).astype(bf16)
-    grouped = jnp.dot(pooled, matrix_ref[0], preferred_element_type=f32)
-    pool_out = (grouped * lines_ref[7:8]).astype(bf16)
+    head = main_ref[0:16, 384:512].astype(f32)
+    place = ((zh * 4 + zl) * 4 + y) * ROWS
+    opening = pool_rows(
+        jnp.concatenate([tail, head], axis=0), head, place, matrix_ref[0], lines_ref[6:7]
+    ).astype(bf16)
+    pool_out = jnp.concatenate([opening, pool_ref[16:]], axis=0)
 
     acts = jnp.concatenate([attn, pool_out], axis=1)
     last = pool_out[:, 127:128].astype(f32)
@@ -419,24 +456,23 @@
     output_pooling_rows,
 ):
     line = lambda v: v.reshape(1, -1)
-    sent = call(
-        prepare_tokens, shaped((4, 128, 512), bf16),
-        tokens, line(input_norm_scale), line(input_norm_bias), name="prepare_tokens",
+    sent, lines = call(
+        prepare_tokens, [shaped((4, 128, 512), bf16), shaped((8, 128), f32)],
+        tokens, line(input_norm_scale), line(input_norm_bias), line(decay_bias_base),
+        line(learning_rate_base), line(key_prenorm_scale), line(key_learning_scale),
+        line(head_norm_scale), line(head_norm_bias), line(pooling_output_scale),
+        line(self_term_weight), name="prepare_tokens",
         space=pltpu.HBM, vmem=60 * 2**20,
         scratch=[
             pltpu.VMEM((128, 2048), bf16), pltpu.VMEM((1, 2048), f32), pltpu.VMEM((1, 2048), f32),
-            pltpu.SemaphoreType.DMA((4,)),
+            pltpu.SemaphoreType.DMA((11,)),
         ],
     )
-    shard, left, lines = call(
-        prepare_weights,
-        [shaped((32, 1023), bf16), shaped((16, 128), f32), shaped((8, 128), f32)],
+    shard, left = call(
+        prepare_weights, [shaped((32, 1023), bf16), shaped((16, 128), f32)],
         query_projection, key_projection, value_projection, pooling_input_projection,
         decay_input_weight, rate_input_weight, gate_input_weight, output_attention_rows.T,
-        output_pooling_rows.T, line(decay_bias_base), line(learning_rate_base),
-        line(key_prenorm_scale), line(key_learning_scale), line(self_term_weight),
-        line(head_norm_scale), line(head_norm_bias), line(pooling_output_scale),
-        name="prepare_weights",
+        output_pooling_rows.T, name="prepare_weights",
     )
     gathered = lax.all_gather(shard, Z, axis=0, tiled=True)
     mixed_tokens = lax.all_to_all(sent, "y", 0, 0, tiled=True).reshape(512, 512)
@@ -460,18 +496,20 @@
     )
     columns, pay = lax.optimization_barrier((gathered, pay))
     got = lax.all_to_all(pay, "y", 0, 0, tiled=True)
-    y_map, y_local = call(
-        block_readings, [shaped((128, 128), bf16), shaped((3, 128, 128), f32)],
-        main, low, gate_output_weight, solved, hats, first, wide, name="block_readings",
-    )
     columns = call(spread_columns, shaped((4, 512, 256), bf16), columns, name="spread_columns")
+    y_map, y_local, pool_out = call(
+        block_readings,
+        [shaped((128, 128), bf16), shaped((3, 128, 128), f32), shaped((128, 128), bf16)],
+        main, low, gate_output_weight, solved, hats, first, wide, lines, pooling_group_matrix,
+        name="block_readings",
+    )
     pay, before, tail = call(
         stage_y,
         [shaped((4, PAY, 128), bf16), shaped((128, 128), f32), shaped((16, 128), f32)],
         got, name="stage_y",
     )
     got = lax.all_to_all(pay, "zl", 0, 0, tiled=True)
-    columns, got = lax.optimization_barrier((columns, got))
+    columns, got, y_map = lax.optimization_barrier((columns, got, y_map))
     columns = lax.all_to_all(columns, "y", 0, 0, tiled=True)
     pay, before, tail = call(
         stage_zl,
@@ -481,7 +519,7 @@
     got = lax.all_gather(pay, "zh", axis=0)
     out = call(
         finish, shaped((128, 2048), bf16),
-        got, before, tail, starting_head_state, y_map, y_local, lines, main,
+        got, before, tail, starting_head_state, y_map, y_local, lines, main, pool_out,
         pooling_group_matrix, columns, name="finish",
     )
     parts = lax.all_to_all(out.reshape(8, 16, 2048), TP, 0, 0, tiled=True)

time: 131 us -> 127 us (0.969); the launches traced: 129 us -> 127 us
  Pallas kernels: 12.7 us -> 11.1 us
    pallas_call x11, Pallas kernels: 12.7 us -> 11.1 us  [call(): pl.pallas_call(kernel, out_shape=outs, in_specs=[pl.BlockSpec(memory_spac...]
where the time goes in v3:
time: 127 us
  blocking collectives  99.9 us (79%)
  starting transfers between devices  12 us (9%)
  Pallas kernels  11.1 us (9%)
  waiting for transfers between devices  2.85 us (2%)
    all_gather x1, blocking collectives, on_device(): gathered = lax.all_gather(shard, Z, axis=0, tiled=True)  34.8 us
    all_to_all x1, blocking collectives, on_device(): parts = lax.all_to_all(out.reshape(8, 16, 2048), TP, 0, 0, tiled=True)  18.1 us
    all_gather x1, blocking collectives, on_device(): got = lax.all_gather(pay, 'zh', axis=0)  16 us
    all_to_all x1, blocking collectives, on_device(): parts = lax.all_to_all(parts, 'y', 0, 0, tiled=True)  12.7 us
    pallas_call x11, Pallas kernels, call(): pl.pallas_call(kernel, out_shape=outs, in_specs=[pl.BlockSpec(memory_spac...  11.1 us
    all_gather x1, blocking collectives, on_device(): low = lax.all_gather(low, 'c', axis=0)  11.1 us
    all_to_all x1, blocking collectives, on_device(): got = lax.all_to_all(pay, 'y', 0, 0, tiled=True)  7.26 us
    all_to_all x1, starting transfers between devices, on_device(): mixed_tokens = lax.all_to_all(sent, 'y', 0, 0, tiled=True).reshape(512, 512)  5.15 us
  transfers between devices with their start and end apart: 3, of which 1 were waited for; matrix products, arithmetic and copies ran while one was open for 0% of the time, Pallas kernels for 2%

profile of v3, /device:TPU:1, one launch (start us, length us, event | category | flops | bytes accessed | tf_op | source)
XLA Modules:
  0.0 126.9 jit_solution(4772184246780631750)
XLA Ops:
  0.0 2.7 %prepare_tokens.1 = (bf16[4,128,512]{2,1,0:T(8,128)(2,1)}, f32[8,128]{1,0:T(8,128)}) custom-call(bf16[128,2048]{1,0:T(8,128)(2,1)} %tok_hbm.1, f32[1,2048]{1,0:T(1,128)} %bitcast.23, f32[1,2048]{1,0:T(1,128)} %bitcast.24, f32[1,128]{1,0:T(1,128)} %bitcast.25, f32[1,128]{1,0:T(1,128)} %bitcast.26, f32[1,128]{1,0:T(1,128)} %bitcast.27, f32[1,128]{1,0:T(1,128)} %bitcast.28, ...), custom_call_target="tpu_custom_call" | custom-call | flops 100000000 | bytes 544768 | tf_op jit(solution)/shard_map/prepare_tokens/pallas_call | solution.py:73
  2.7 0.0 copy-start.8
  2.7 0.0 copy-start.9
  2.7 0.0 copy-start.10
  2.7 0.0 copy-start.11
  2.7 0.0 copy-start.12
  2.7 0.0 copy-start.13
  2.7 0.0 copy-start.14
  2.8 0.0 copy-start.15
  2.8 0.0 copy-start.16
  2.8 5.1 %all-to-all-start = ((bf16[4,128,512]{2,1,0:T(8,128)(2,1)}), bf16[4,128,512]{2,1,0:T(8,128)(2,1)S(1)}, u32[]{:S(2)}, u32[]{:S(2)}) async-start(bf16[4,128,512]{2,1,0:T(8,128)(2,1)} %get-tuple-element.31), calls=%async_computation | async-start | bytes 1048576 | tf_op jit(solution)/shard_map/all_to_all | solution.py:478
  7.9 0.0 copy-done.8
  7.9 0.0 copy-done.9
  7.9 0.0 copy-done.10
  7.9 0.0 copy-done.11
  8.0 0.0 copy-done.12
  8.0 0.0 copy-done.13
  8.0 0.0 copy-done.14
  8.0 0.0 copy-done.15
  8.0 0.0 copy-done.16
  8.0 0.1 prepare_weights.1
  8.1 34.8 %all_gather.15.w_ref = bf16[512,1023]{1,0:T(8,128)(2,1)S(1)} all-gather(bf16[32,1023]{1,0:T(8,128)(2,1)S(1)} %get-tuple-element.30), channel_id=1, replica_groups=mesh['zh'=4,'zl'=4,'y'=4,'x'=4,'c'=2] {'zh','zl'}, dimensions={0}, use_global_device_ids=true | all-gather | bytes 1113024 | tf_op jit(solution)/shard_map/all_gather | solution.py:477
  42.9 0.0 all-to-all-done
  42.9 0.6 partial_products.1
  43.5 12.7 %all_to_all.30.part_ref = bf16[4,128,768]{2,1,0:T(8,128)(2,1)S(1)} all-to-all(bf16[4,128,768]{2,1,0:T(8,128)(2,1)S(1)} %partial_products.1), channel_id=1, replica_groups=mesh['zh'=4,'zl'=4,'y'=4,'x'=4,'c'=2] {'y'}, dimensions={0} | all-to-all | bytes 1572864 | tf_op jit(solution)/shard_map/all_to_all | solution.py:483
  56.1 0.1 sum_parts.1
  56.2 0.0 copy-start.1
  56.3 0.0 copy-start.2
  56.3 0.0 copy-start.6
  56.3 0.0 copy-start.7
  56.3 11.1 %all-gather = bf16[256,256]{1,0:T(8,128)(2,1)S(1)} all-gather(bf16[128,256]{1,0:T(8,128)(2,1)S(1)} %get-tuple-element.33), channel_id=2, replica_groups=mesh['zh'=4,'zl'=4,'y'=4,'x'=4,'c'=2] {'c'}, dimensions={0}, use_global_device_ids=true | all-gather | bytes 196608 | tf_op jit(solution)/shard_map/all_gather | solution.py:487
  67.4 0.0 copy-start.5
  67.4 0.0 copy-done.1
  67.4 0.0 copy-done.2
  67.4 0.0 copy-done.6
  67.4 0.0 copy-done.7
  67.4 0.7 copy-done.5
  68.1 2.4 %block_maps.1 = (bf16[4,144,128]{2,1,0:T(8,128)(2,1)S(1)}, bf16[2,128,128]{2,1,0:T(8,128)(2,1)S(1)}, bf16[3,128,128]{2,1,0:T(8,128)(2,1)S(1)}, bf16[128,128]{1,0:T(8,128)(2,1)S(1)}, f32[2,128,128]{2,1,0:T(8,128)S(1)}) custom-call(bf16[128,512]{1,0:T(8,128)(2,1)S(1)} %get-tuple-element.32.main_ref, bf16[2,128,256]{2,1,0:T(8,128)(2,1)S(1)} %bitcast.18, ...), custom_call_target="tpu_custom_call" | custom-call | flops 100000000 | bytes 471040 | tf_op jit(solution)/shard_map/block_maps/pallas_call | solution.py:73
  70.5 7.3 %all_to_all.31.got_ref = bf16[4,144,128]{2,1,0:T(8,128)(2,1)S(1)} all-to-all(bf16[4,144,128]{2,1,0:T(8,128)(2,1)S(1)} %get-tuple-element.38), channel_id=1, replica_groups=mesh['zh'=4,'zl'=4,'y'=4,'x'=4,'c'=2] {'y'}, dimensions={0} | all-to-all | bytes 294912 | tf_op jit(solution)/shard_map/all_to_all | solution.py:498
  77.8 1.0 stage_y.1
  78.8 3.3 %all-to-all-start.3 = ((bf16[4,144,128]{2,1,0:T(8,128)(2,1)}), bf16[4,144,128]{2,1,0:T(8,128)(2,1)S(1)}, u32[]{:S(2)}, u32[]{:S(2)}) async-start(bf16[4,144,128]{2,1,0:T(8,128)(2,1)} %get-tuple-element.39), calls=%async_computation.3 | async-start | bytes 294912 | tf_op jit(solution)/shard_map/all_to_all | solution.py:511
  82.2 0.0 copy-start
  82.2 0.0 copy-start.4
  82.2 1.2 spread_columns.1
  83.4 0.0 copy-done
  83.4 0.0 copy-done.4
  83.4 0.7 block_readings.1
  84.1 2.8 %all-to-all-done.3.got_ref = bf16[4,144,128]{2,1,0:T(8,128)(2,1)S(1)} async-done(((bf16[4,144,128]{2,1,0:T(8,128)(2,1)}), bf16[4,144,128]{2,1,0:T(8,128)(2,1)S(1)}, u32[]{:S(2)}, u32[]{:S(2)}) %all-to-all-start.3) | async-done | bytes 147488 | tf_op jit(solution)/shard_map/all_to_all | solution.py:511
  87.0 3.5 %all-to-all-start.4 = ((bf16[4,512,256]{2,1,0:T(8,128)(2,1)}), bf16[4,512,256]{2,1,0:T(8,128)(2,1)S(1)}, u32[]{:S(2)}, u32[]{:S(2)}) async-start(bf16[4,512,256]{2,1,0:T(8,128)(2,1)} %spread_columns.1), calls=%async_computation.4 | async-start | bytes 2097152 | tf_op jit(solution)/shard_map/all_to_all | solution.py:513
  90.5 0.4 stage_zl.1
  90.9 0.0 copy-start.3
  90.9 16.0 %all-gather.1 = bf16[640,128]{1,0:T(8,128)(2,1)S(1)} all-gather(bf16[160,128]{1,0:T(8,128)(2,1)S(1)} %get-tuple-element.48), channel_id=3, replica_groups=mesh['zh'=4,'zl'=4,'y'=4,'x'=4,'c'=2] {'zh'}, dimensions={0}, use_global_device_ids=true | all-gather | bytes 204800 | tf_op jit(solution)/shard_map/all_gather | solution.py:519
  106.9 0.0 all-to-all-done.4.wout_ref
  106.9 0.0 copy-done.3
  106.9 1.2 finish.1
  108.1 18.1 %all_to_all.32.part_ref = bf16[8,16,2048]{2,1,0:T(8,128)(2,1)S(1)} all-to-all(bf16[8,16,2048]{2,1,0:T(8,128)(2,1)S(1)} %bitcast.17), channel_id=1, replica_groups=mesh['zh'=4,'zl'=4,'y'=4,'x'=4,'c'=2] {'x','c'}, dimensions={0} | all-to-all | bytes 1048576 | tf_op jit(solution)/shard_map/all_to_all | solution.py:525
  126.2 0.7 add_parts.1
Async XLA Ops:
  2.7 5.3 %copy-start.8 = (bf16[32,256]{1,0:T(8,128)(2,1)S(1)}, bf16[32,256]{1,0:T(8,128)(2,1)}, u32[]{:S(2)}) copy-start(bf16[32,256]{1,0:T(8,128)(2,1)} %g_ref.1) | copy-start | bytes 49156
  2.7 5.2 %copy-start.9 = (bf16[32,128]{1,0:T(8,128)(2,1)S(1)}, bf16[32,128]{1,0:T(8,128)(2,1)}, u32[]{:S(2)}) copy-start(bf16[32,128]{1,0:T(8,128)(2,1)} %q_ref.1) | copy-start | bytes 24580
  2.7 5.2 %copy-start.10 = (bf16[32,128]{1,0:T(8,128)(2,1)S(1)}, bf16[32,128]{1,0:T(8,128)(2,1)}, u32[]{:S(2)}) copy-start(bf16[32,128]{1,0:T(8,128)(2,1)} %k_ref.1) | copy-start | bytes 24580
  2.7 5.2 %copy-start.11 = (bf16[32,128]{1,0:T(8,128)(2,1)S(1)}, bf16[32,128]{1,0:T(8,128)(2,1)}, u32[]{:S(2)}) copy-start(bf16[32,128]{1,0:T(8,128)(2,1)} %v_ref.1) | copy-start | bytes 24580
  2.7 5.2 %copy-start.12 = (bf16[32,128]{1,0:T(8,128)(2,1)S(1)}, bf16[32,128]{1,0:T(8,128)(2,1)}, u32[]{:S(2)}) copy-start(bf16[32,128]{1,0:T(8,128)(2,1)} %p_ref.1) | copy-start | bytes 24580
  2.7 5.2 %copy-start.13 = (bf16[32,128]{1,0:T(8,128)(2,1)S(1)}, bf16[32,128]{1,0:T(8,128)(2,1)}, u32[]{:S(2)}) copy-start(bf16[32,128]{1,0:T(8,128)(2,1)} %d_ref.1) | copy-start | bytes 24580
  2.7 5.2 %copy-start.14 = (bf16[32,128]{1,0:T(8,128)(2,1)S(1)}, bf16[32,128]{1,0:T(8,128)(2,1)}, u32[]{:S(2)}) copy-start(bf16[32,128]{1,0:T(8,128)(2,1)} %r_ref.1) | copy-start | bytes 24580
  2.8 5.2 %copy-start.15 = (bf16[128,32]{0,1:T(8,128)(2,1)S(1)}, bf16[128,32]{0,1:T(8,128)(2,1)}, u32[]{:S(2)}) copy-start(bf16[128,32]{0,1:T(8,128)(2,1)} %param.52) | copy-start | bytes 24580
  2.8 5.2 %copy-start.16 = (bf16[128,32]{0,1:T(8,128)(2,1)S(1)}, bf16[128,32]{0,1:T(8,128)(2,1)}, u32[]{:S(2)}) copy-start(bf16[128,32]{0,1:T(8,128)(2,1)} %param.53) | copy-start | bytes 24580
  2.8 40.1 %all-to-all-start = ((bf16[4,128,512]{2,1,0:T(8,128)(2,1)}), bf16[4,128,512]{2,1,0:T(8,128)(2,1)S(1)}, u32[]{:S(2)}, u32[]{:S(2)}) async-start(bf16[4,128,512]{2,1,0:T(8,128)(2,1)} %get-tuple-element.31), calls=%async_computation | async-start | bytes 1048576 | tf_op jit(solution)/shard_map/all_to_all | solution.py:478
  56.2 11.2 %copy-start.1 = (f32[128,128]{1,0:T(8,128)S(1)}, f32[128,128]{1,0:T(8,128)}, u32[]{:S(2)}) copy-start(f32[128,128]{1,0:T(8,128)} %re_ref.1) | copy-start | bytes 196612
  56.3 11.2 %copy-start.2 = (f32[128,128]{1,0:T(8,128)S(1)}, f32[128,128]{1,0:T(8,128)}, u32[]{:S(2)}) copy-start(f32[128,128]{1,0:T(8,128)} %de_ref.1) | copy-start | bytes 196612
  56.3 11.1 %copy-start.6 = (bf16[128,128]{1,0:T(8,128)(2,1)S(1)}, bf16[128,128]{1,0:T(8,128)(2,1)}, u32[]{:S(2)}) copy-start(bf16[128,128]{1,0:T(8,128)(2,1)} %dw_ref.1) | copy-start | bytes 98308
  56.3 11.1 %copy-start.7 = (bf16[128,128]{1,0:T(8,128)(2,1)S(1)}, bf16[128,128]{1,0:T(8,128)(2,1)}, u32[]{:S(2)}) copy-start(bf16[128,128]{1,0:T(8,128)(2,1)} %rw_ref.1) | copy-start | bytes 98308
  67.4 0.7 copy-start.5
  78.8 8.1 %all-to-all-start.3 = ((bf16[4,144,128]{2,1,0:T(8,128)(2,1)}), bf16[4,144,128]{2,1,0:T(8,128)(2,1)S(1)}, u32[]{:S(2)}, u32[]{:S(2)}) async-start(bf16[4,144,128]{2,1,0:T(8,128)(2,1)} %get-tuple-element.39), calls=%async_computation.3 | async-start | bytes 294912 | tf_op jit(solution)/shard_map/all_to_all | solution.py:511
  82.2 1.2 copy-start
  82.2 1.2 copy-start.4
  87.0 19.9 %all-to-all-start.4 = ((bf16[4,512,256]{2,1,0:T(8,128)(2,1)}), bf16[4,512,256]{2,1,0:T(8,128)(2,1)S(1)}, u32[]{:S(2)}, u32[]{:S(2)}) async-start(bf16[4,512,256]{2,1,0:T(8,128)(2,1)} %spread_columns.1), calls=%async_computation.4 | async-start | bytes 2097152 | tf_op jit(solution)/shard_map/all_to_all | solution.py:513
  90.9 16.0 %copy-start.3 = (f32[2,64,64]{2,1,0:T(8,128)S(1)}, f32[2,64,64]{2,1,0:T(8,128)}, u32[]{:S(2)}) copy-start(f32[2,64,64]{2,1,0:T(8,128)} %start_ref.1) | copy-start | bytes 98308

commit v4 on v3

--- a/solution.py
+++ b/solution.py
@@ -136,7 +136,8 @@
     left_ref[...] = jnp.where(iota((16, LANES), 0) == 0, line, 0.0)
 
 
-def partial_products(tok_ref, w_ref, part_ref):
+def partial_products(tok_ref, w_ref, lines_ref, part_ref, out_lines_ref):
+    out_lines_ref[...] = lines_ref[...]
     made = jnp.dot(tok_ref[...], w_ref[:, :768], preferred_element_type=f32).astype(bf16)
     for y in range(4):
         part_ref[y] = made[128 * y : 128 * y + 128]
@@ -339,20 +340,6 @@
     return jnp.concatenate([moved[:HEAD], moved[HEAD:] + later[HEAD:]], axis=0)
 
 
-def chain(first, others):
-    made = [first]
-    for other in others:
-        made.append(compose(made[-1], other))
-    return made
-
-
-def chosen_before(made, mine):
-    before = jnp.where(mine == 0, identity_pair(), made[0])
-    for j in (1, 2):
-        before = jnp.where(mine > j, made[j], before)
-    return before
-
-
 def tail_before(got_ref, mine):
     found = jnp.zeros((16, LANES), f32)
     for j in range(3):
@@ -362,8 +349,13 @@
 
 def prefixes(got_ref, mine):
     pieces = [got_ref[j, :128].astype(f32) for j in range(4)]
-    made = chain(pieces[0], pieces[1:])
-    return chosen_before(made, mine), made[3].astype(bf16)
+    two = compose(pieces[0], pieces[1])
+    three = compose(two, pieces[2])
+    whole = compose(two, compose(pieces[2], pieces[3]))
+    before = jnp.where(mine == 0, identity_pair(), pieces[0])
+    before = jnp.where(mine > 1, two, before)
+    before = jnp.where(mine > 2, three, before)
+    return before, whole.astype(bf16)
 
 
 def stage_y(got_ref, pay_ref, before_ref, tail_ref):
@@ -476,9 +468,9 @@
     )
     gathered = lax.all_gather(shard, Z, axis=0, tiled=True)
     mixed_tokens = lax.all_to_all(sent, "y", 0, 0, tiled=True).reshape(512, 512)
-    parts = call(
-        partial_products, shaped((4, 128, 768), bf16), mixed_tokens, gathered,
-        name="partial_products",
+    parts, lines = call(
+        partial_products, [shaped((4, 128, 768), bf16), shaped((8, 128), f32)],
+        mixed_tokens, gathered, lines, name="partial_products",
     )
     parts = lax.all_to_all(parts, "y", 0, 0, tiled=True)
     main, low = call(

time: 127 us -> 127 us (level)
  no operation moved by 1% of the time
where the time goes in v4:
time: 127 us; the launch traced here: 126 us
  blocking collectives  99.9 us (79%)
  starting transfers between devices  12 us (9%)
  Pallas kernels  11 us (9%)
  waiting for transfers between devices  2.85 us (2%)
    all_gather x1, blocking collectives, on_device(): gathered = lax.all_gather(shard, Z, axis=0, tiled=True)  35.1 us
    all_to_all x1, blocking collectives, on_device(): parts = lax.all_to_all(out.reshape(8, 16, 2048), TP, 0, 0, tiled=True)  18.4 us
    all_gather x1, blocking collectives, on_device(): got = lax.all_gather(pay, 'zh', axis=0)  15.5 us
    all_to_all x1, blocking collectives, on_device(): parts = lax.all_to_all(parts, 'y', 0, 0, tiled=True)  12.5 us
    all_gather x1, blocking collectives, on_device(): low = lax.all_gather(low, 'c', axis=0)  11.1 us
    pallas_call x11, Pallas kernels, call(): pl.pallas_call(kernel, out_shape=outs, in_specs=[pl.BlockSpec(memory_spac...  11 us
    all_to_all x1, blocking collectives, on_device(): got = lax.all_to_all(pay, 'y', 0, 0, tiled=True)  7.26 us
    all_to_all x1, starting transfers between devices, on_device(): mixed_tokens = lax.all_to_all(sent, 'y', 0, 0, tiled=True).reshape(512, 512)  5.15 us
  transfers between devices with their start and end apart: 3, of which 1 were waited for; matrix products, arithmetic and copies ran while one was open for 0% of the time, Pallas kernels for 2%

profile of v4, /device:TPU:1, one launch (start us, length us, event | category | flops | bytes accessed | tf_op | source)
XLA Modules:
  0.0 126.2 jit_solution(1553961087559881042)
XLA Ops:
  0.0 2.7 %prepare_tokens.1 = (bf16[4,128,512]{2,1,0:T(8,128)(2,1)}, f32[8,128]{1,0:T(8,128)}) custom-call(bf16[128,2048]{1,0:T(8,128)(2,1)} %tok_hbm.1, f32[1,2048]{1,0:T(1,128)} %bitcast.23, f32[1,2048]{1,0:T(1,128)} %bitcast.24, f32[1,128]{1,0:T(1,128)} %bitcast.25, f32[1,128]{1,0:T(1,128)} %bitcast.26, f32[1,128]{1,0:T(1,128)} %bitcast.27, f32[1,128]{1,0:T(1,128)} %bitcast.28, ...), custom_call_target="tpu_custom_call" | custom-call | flops 100000000 | bytes 544768 | tf_op jit(solution)/shard_map/prepare_tokens/pallas_call | solution.py:73
  2.7 0.0 copy-start.8
  2.7 0.0 copy-start.9
  2.7 0.0 copy-start.10
  2.7 0.0 copy-start.11
  2.7 0.0 copy-start.12
  2.8 0.0 copy-start.13
  2.8 0.0 copy-start.14
  2.8 0.0 copy-start.15
  2.8 0.0 copy-start.16
  2.8 5.1 %all-to-all-start = ((bf16[4,128,512]{2,1,0:T(8,128)(2,1)}), bf16[4,128,512]{2,1,0:T(8,128)(2,1)S(1)}, u32[]{:S(2)}, u32[]{:S(2)}) async-start(bf16[4,128,512]{2,1,0:T(8,128)(2,1)} %get-tuple-element.33), calls=%async_computation | async-start | bytes 1048576 | tf_op jit(solution)/shard_map/all_to_all | solution.py:470
  7.9 0.0 copy-done.8
  8.0 0.0 copy-done.9
  8.0 0.0 copy-done.10
  8.0 0.0 copy-done.11
  8.0 0.0 copy-done.12
  8.0 0.0 copy-done.13
  8.0 0.0 copy-done.14
  8.0 0.0 copy-done.15
  8.0 0.0 copy-done.16
  8.0 0.1 prepare_weights.1
  8.1 0.0 copy-start.7
  8.1 35.1 %all_gather.15.w_ref = bf16[512,1023]{1,0:T(8,128)(2,1)S(1)} all-gather(bf16[32,1023]{1,0:T(8,128)(2,1)S(1)} %get-tuple-element.32), channel_id=1, replica_groups=mesh['zh'=4,'zl'=4,'y'=4,'x'=4,'c'=2] {'zh','zl'}, dimensions={0}, use_global_device_ids=true | all-gather | bytes 1113024 | tf_op jit(solution)/shard_map/all_gather | solution.py:469
  43.2 0.0 all-to-all-done
  43.2 0.0 copy-done.7
  43.2 0.6 partial_products.1
  43.8 12.5 %all_to_all.30.part_ref = bf16[4,128,768]{2,1,0:T(8,128)(2,1)S(1)} all-to-all(bf16[4,128,768]{2,1,0:T(8,128)(2,1)S(1)} %get-tuple-element.35), channel_id=1, replica_groups=mesh['zh'=4,'zl'=4,'y'=4,'x'=4,'c'=2] {'y'}, dimensions={0} | all-to-all | bytes 1572864 | tf_op jit(solution)/shard_map/all_to_all | solution.py:475
  56.3 0.1 sum_parts.1
  56.4 0.0 copy-start.1
  56.4 0.0 copy-start.2
  56.4 0.0 copy-start.5
  56.4 0.0 copy-start.6
  56.5 11.1 %all-gather = bf16[256,256]{1,0:T(8,128)(2,1)S(1)} all-gather(bf16[128,256]{1,0:T(8,128)(2,1)S(1)} %get-tuple-element.37), channel_id=2, replica_groups=mesh['zh'=4,'zl'=4,'y'=4,'x'=4,'c'=2] {'c'}, dimensions={0}, use_global_device_ids=true | all-gather | bytes 196608 | tf_op jit(solution)/shard_map/all_gather | solution.py:479
  67.6 0.0 copy-done.1
  67.6 0.0 copy-done.2
  67.6 0.0 copy-done.5
  67.6 0.0 copy-done.6
  67.6 2.4 %block_maps.1 = (bf16[4,144,128]{2,1,0:T(8,128)(2,1)S(1)}, bf16[2,128,128]{2,1,0:T(8,128)(2,1)S(1)}, bf16[3,128,128]{2,1,0:T(8,128)(2,1)S(1)}, bf16[128,128]{1,0:T(8,128)(2,1)S(1)}, f32[2,128,128]{2,1,0:T(8,128)S(1)}) custom-call(bf16[128,512]{1,0:T(8,128)(2,1)S(1)} %get-tuple-element.36.main_ref, bf16[2,128,256]{2,1,0:T(8,128)(2,1)S(1)} %bitcast.18, ...), custom_call_target="tpu_custom_call" | custom-call | flops 100000000 | bytes 471040 | tf_op jit(solution)/shard_map/block_maps/pallas_call | solution.py:73
  70.1 7.3 %all_to_all.31.got_ref = bf16[4,144,128]{2,1,0:T(8,128)(2,1)S(1)} all-to-all(bf16[4,144,128]{2,1,0:T(8,128)(2,1)S(1)} %get-tuple-element.42), channel_id=1, replica_groups=mesh['zh'=4,'zl'=4,'y'=4,'x'=4,'c'=2] {'y'}, dimensions={0} | all-to-all | bytes 294912 | tf_op jit(solution)/shard_map/all_to_all | solution.py:490
  77.3 0.9 stage_y.1
  78.3 3.3 %all-to-all-start.3 = ((bf16[4,144,128]{2,1,0:T(8,128)(2,1)}), bf16[4,144,128]{2,1,0:T(8,128)(2,1)S(1)}, u32[]{:S(2)}, u32[]{:S(2)}) async-start(bf16[4,144,128]{2,1,0:T(8,128)(2,1)} %get-tuple-element.43), calls=%async_computation.3 | async-start | bytes 294912 | tf_op jit(solution)/shard_map/all_to_all | solution.py:503
  81.6 0.0 copy-start
  81.6 0.0 copy-start.4
  81.6 1.2 spread_columns.1
  82.8 0.0 copy-done
  82.8 0.0 copy-done.4
  82.8 0.7 block_readings.1
  83.6 2.8 %all-to-all-done.3.got_ref = bf16[4,144,128]{2,1,0:T(8,128)(2,1)S(1)} async-done(((bf16[4,144,128]{2,1,0:T(8,128)(2,1)}), bf16[4,144,128]{2,1,0:T(8,128)(2,1)S(1)}, u32[]{:S(2)}, u32[]{:S(2)}) %all-to-all-start.3) | async-done | bytes 147488 | tf_op jit(solution)/shard_map/all_to_all | solution.py:503
  86.4 3.5 %all-to-all-start.4 = ((bf16[4,512,256]{2,1,0:T(8,128)(2,1)}), bf16[4,512,256]{2,1,0:T(8,128)(2,1)S(1)}, u32[]{:S(2)}, u32[]{:S(2)}) async-start(bf16[4,512,256]{2,1,0:T(8,128)(2,1)} %spread_columns.1), calls=%async_computation.4 | async-start | bytes 2097152 | tf_op jit(solution)/shard_map/all_to_all | solution.py:505
  89.9 0.4 stage_zl.1
  90.3 0.0 copy-start.3
  90.3 15.5 %all-gather.1 = bf16[640,128]{1,0:T(8,128)(2,1)S(1)} all-gather(bf16[160,128]{1,0:T(8,128)(2,1)S(1)} %get-tuple-element.52), channel_id=3, replica_groups=mesh['zh'=4,'zl'=4,'y'=4,'x'=4,'c'=2] {'zh'}, dimensions={0}, use_global_device_ids=true | all-gather | bytes 204800 | tf_op jit(solution)/shard_map/all_gather | solution.py:511
  105.9 0.0 all-to-all-done.4.wout_ref
  105.9 0.0 copy-done.3
  105.9 1.2 finish.1
  107.1 18.4 %all_to_all.32.part_ref = bf16[8,16,2048]{2,1,0:T(8,128)(2,1)S(1)} all-to-all(bf16[8,16,2048]{2,1,0:T(8,128)(2,1)S(1)} %bitcast.17), channel_id=1, replica_groups=mesh['zh'=4,'zl'=4,'y'=4,'x'=4,'c'=2] {'x','c'}, dimensions={0} | all-to-all | bytes 1048576 | tf_op jit(solution)/shard_map/all_to_all | solution.py:517
  125.5 0.7 add_parts.1
Async XLA Ops:
  2.7 5.3 %copy-start.8 = (bf16[32,256]{1,0:T(8,128)(2,1)S(1)}, bf16[32,256]{1,0:T(8,128)(2,1)}, u32[]{:S(2)}) copy-start(bf16[32,256]{1,0:T(8,128)(2,1)} %g_ref.1) | copy-start | bytes 49156
  2.7 5.2 %copy-start.9 = (bf16[32,128]{1,0:T(8,128)(2,1)S(1)}, bf16[32,128]{1,0:T(8,128)(2,1)}, u32[]{:S(2)}) copy-start(bf16[32,128]{1,0:T(8,128)(2,1)} %q_ref.1) | copy-start | bytes 24580
  2.7 5.2 %copy-start.10 = (bf16[32,128]{1,0:T(8,128)(2,1)S(1)}, bf16[32,128]{1,0:T(8,128)(2,1)}, u32[]{:S(2)}) copy-start(bf16[32,128]{1,0:T(8,128)(2,1)} %k_ref.1) | copy-start | bytes 24580
  2.7 5.2 %copy-start.11 = (bf16[32,128]{1,0:T(8,128)(2,1)S(1)}, bf16[32,128]{1,0:T(8,128)(2,1)}, u32[]{:S(2)}) copy-start(bf16[32,128]{1,0:T(8,128)(2,1)} %v_ref.1) | copy-start | bytes 24580
  2.7 5.2 %copy-start.12 = (bf16[32,128]{1,0:T(8,128)(2,1)S(1)}, bf16[32,128]{1,0:T(8,128)(2,1)}, u32[]{:S(2)}) copy-start(bf16[32,128]{1,0:T(8,128)(2,1)} %p_ref.1) | copy-start | bytes 24580
  2.8 5.2 %copy-start.13 = (bf16[32,128]{1,0:T(8,128)(2,1)S(1)}, bf16[32,128]{1,0:T(8,128)(2,1)}, u32[]{:S(2)}) copy-start(bf16[32,128]{1,0:T(8,128)(2,1)} %d_ref.1) | copy-start | bytes 24580
  2.8 5.2 %copy-start.14 = (bf16[32,128]{1,0:T(8,128)(2,1)S(1)}, bf16[32,128]{1,0:T(8,128)(2,1)}, u32[]{:S(2)}) copy-start(bf16[32,128]{1,0:T(8,128)(2,1)} %r_ref.1) | copy-start | bytes 24580
  2.8 5.2 %copy-start.15 = (bf16[128,32]{0,1:T(8,128)(2,1)S(1)}, bf16[128,32]{0,1:T(8,128)(2,1)}, u32[]{:S(2)}) copy-start(bf16[128,32]{0,1:T(8,128)(2,1)} %param.52) | copy-start | bytes 24580
  2.8 5.2 %copy-start.16 = (bf16[128,32]{0,1:T(8,128)(2,1)S(1)}, bf16[128,32]{0,1:T(8,128)(2,1)}, u32[]{:S(2)}) copy-start(bf16[128,32]{0,1:T(8,128)(2,1)} %param.53) | copy-start | bytes 24580
  2.8 40.4 %all-to-all-start = ((bf16[4,128,512]{2,1,0:T(8,128)(2,1)}), bf16[4,128,512]{2,1,0:T(8,128)(2,1)S(1)}, u32[]{:S(2)}, u32[]{:S(2)}) async-start(bf16[4,128,512]{2,1,0:T(8,128)(2,1)} %get-tuple-element.33), calls=%async_computation | async-start | bytes 1048576 | tf_op jit(solution)/shard_map/all_to_all | solution.py:470
  8.1 35.1 %copy-start.7 = (f32[8,128]{1,0:T(8,128)S(1)}, f32[8,128]{1,0:T(8,128)}, u32[]{:S(2)}) copy-start(f32[8,128]{1,0:T(8,128)} %get-tuple-element.34.lines_ref) | copy-start | bytes 12292
  56.4 11.2 %copy-start.1 = (f32[128,128]{1,0:T(8,128)S(1)}, f32[128,128]{1,0:T(8,128)}, u32[]{:S(2)}) copy-start(f32[128,128]{1,0:T(8,128)} %re_ref.1) | copy-start | bytes 196612
  56.4 11.2 %copy-start.2 = (f32[128,128]{1,0:T(8,128)S(1)}, f32[128,128]{1,0:T(8,128)}, u32[]{:S(2)}) copy-start(f32[128,128]{1,0:T(8,128)} %de_ref.1) | copy-start | bytes 196612
  56.4 11.2 %copy-start.5 = (bf16[128,128]{1,0:T(8,128)(2,1)S(1)}, bf16[128,128]{1,0:T(8,128)(2,1)}, u32[]{:S(2)}) copy-start(bf16[128,128]{1,0:T(8,128)(2,1)} %dw_ref.1) | copy-start | bytes 98308
  56.4 11.2 %copy-start.6 = (bf16[128,128]{1,0:T(8,128)(2,1)S(1)}, bf16[128,128]{1,0:T(8,128)(2,1)}, u32[]{:S(2)}) copy-start(bf16[128,128]{1,0:T(8,128)(2,1)} %rw_ref.1) | copy-start | bytes 98308
  78.3 8.1 %all-to-all-start.3 = ((bf16[4,144,128]{2,1,0:T(8,128)(2,1)}), bf16[4,144,128]{2,1,0:T(8,128)(2,1)S(1)}, u32[]{:S(2)}, u32[]{:S(2)}) async-start(bf16[4,144,128]{2,1,0:T(8,128)(2,1)} %get-tuple-element.43), calls=%async_computation.3 | async-start | bytes 294912 | tf_op jit(solution)/shard_map/all_to_all | solution.py:503
  81.6 1.2 copy-start
  81.6 1.2 copy-start.4
  86.4 19.5 %all-to-all-start.4 = ((bf16[4,512,256]{2,1,0:T(8,128)(2,1)}), bf16[4,512,256]{2,1,0:T(8,128)(2,1)S(1)}, u32[]{:S(2)}, u32[]{:S(2)}) async-start(bf16[4,512,256]{2,1,0:T(8,128)(2,1)} %spread_columns.1), calls=%async_computation.4 | async-start | bytes 2097152 | tf_op jit(solution)/shard_map/all_to_all | solution.py:505
  90.3 15.6 %copy-start.3 = (f32[2,64,64]{2,1,0:T(8,128)S(1)}, f32[2,64,64]{2,1,0:T(8,128)}, u32[]{:S(2)}) copy-start(f32[2,64,64]{2,1,0:T(8,128)} %start_ref.1) | copy-start | bytes 98308

commit v5 on v4

--- a/solution.py
+++ b/solution.py
@@ -68,13 +68,13 @@
     )
 
 
-def call(kernel, outs, *args, flops=10**8, name=None, vmem=16 * 2**20, space=pltpu.VMEM, scratch=()):
+def call(kernel, outs, *args, flops=10**8, name=None, vmem=16 * 2**20, space=pltpu.VMEM, scratch=(), places=None):
     size = sum(a.size * a.dtype.itemsize for a in args)
     return pl.pallas_call(
         kernel,
         out_shape=outs,
         in_specs=[pl.BlockSpec(memory_space=space)] * len(args),
-        out_specs=jax.tree.map(lambda _: pl.BlockSpec(memory_space=pltpu.VMEM), outs),
+        out_specs=places or jax.tree.map(lambda _: pl.BlockSpec(memory_space=pltpu.VMEM), outs),
         scratch_shapes=scratch,
         compiler_params=pltpu.CompilerParams(vmem_limit_bytes=vmem),
         cost_estimate=pl.CostEstimate(flops=flops, bytes_accessed=size, transcendentals=0),
@@ -136,20 +136,14 @@
     left_ref[...] = jnp.where(iota((16, LANES), 0) == 0, line, 0.0)
 
 
-def partial_products(tok_ref, w_ref, lines_ref, part_ref, out_lines_ref):
+def partial_products(tok_ref, w_ref, lines_ref, part_ref, out_lines_ref, cols_ref):
     out_lines_ref[...] = lines_ref[...]
+    cols_ref[:, 0:128] = w_ref[:, 768:896]
+    cols_ref[:, 128:255] = w_ref[:, 896:1023]
+    cols_ref[:, 255:256] = jnp.zeros((512, 1), bf16)
     made = jnp.dot(tok_ref[...], w_ref[:, :768], preferred_element_type=f32).astype(bf16)
     for y in range(4):
         part_ref[y] = made[128 * y : 128 * y + 128]
-
-
-def spread_columns(w_ref, out_ref):
-    first = w_ref[:, 768:896]
-    second = w_ref[:, 896:1023]
-    for y in range(4):
-        out_ref[y, :, 0:128] = first
-        out_ref[y, :, 128:255] = second
-        out_ref[y, :, 255:256] = jnp.zeros((512, 1), bf16)
 
 
 def sum_parts(part_ref, main_ref, low_ref):
@@ -178,8 +172,12 @@
 
 
 def block_maps(
-    main_ref, low_ref, dw_ref, rw_ref, lines_ref, re_ref, de_ref, left_ref, pay_ref, solved_ref, hats_ref, first_ref, wide_ref,
+    main_ref, low_ref, dw_ref, rw_ref, lines_ref, re_ref, de_ref, left_ref, cols_ref,
+    pay_ref, solved_ref, hats_ref, first_ref, wide_ref, spread_ref, sems,
 ):
+    copies = [pltpu.make_async_copy(cols_ref, spread_ref.at[j], sems.at[j]) for j in range(4)]
+    for copy in copies:
+        copy.start()
     line = lambda i: lines_ref[i : i + 1]
     recept = main_ref[:, 0:128].astype(f32)
     keys = main_ref[:, 128:256].astype(f32)
@@ -269,6 +267,8 @@
         pay_ref[j, 0:64] = block_map
         pay_ref[j, 64:128] = block_state
         pay_ref[j, TAIL : TAIL + 16] = extra
+    for copy in copies:
+        copy.wait()
 
 
 def pool_rows(extended, own, place, matrix, scale):
@@ -468,8 +468,9 @@
     )
     gathered = lax.all_gather(shard, Z, axis=0, tiled=True)
     mixed_tokens = lax.all_to_all(sent, "y", 0, 0, tiled=True).reshape(512, 512)
-    parts, lines = call(
-        partial_products, [shaped((4, 128, 768), bf16), shaped((8, 128), f32)],
+    parts, lines, columns = call(
+        partial_products,
+        [shaped((4, 128, 768), bf16), shaped((8, 128), f32), shaped((512, 256), bf16)],
         mixed_tokens, gathered, lines, name="partial_products",
     )
     parts = lax.all_to_all(parts, "y", 0, 0, tiled=True)
@@ -477,32 +478,32 @@
         sum_parts, [shaped((128, 512), bf16), shaped((128, 256), bf16)], parts, name="sum_parts"
     )
     low = lax.all_gather(low, "c", axis=0)
-    pay, solved, hats, first, wide = call(
+    pay, solved, hats, first, wide, columns = call(
         block_maps,
         [
             shaped((4, PAY, 128), bf16), shaped((2, 128, 128), bf16), shaped((3, 128, 128), bf16),
-            shaped((128, 128), bf16), shaped((2, 128, 128), f32),
+            shaped((128, 128), bf16), shaped((2, 128, 128), f32), shaped((4, 512, 256), bf16),
         ],
         main, low, decay_output_weight, rate_output_weight, lines, rate_extra_log,
-        decay_extra_log, left, name="block_maps",
-    )
-    columns, pay = lax.optimization_barrier((gathered, pay))
+        decay_extra_log, left, columns, name="block_maps",
+        places=[pl.BlockSpec(memory_space=pltpu.VMEM)] * 5 + [pl.BlockSpec(memory_space=pltpu.HBM)],
+        scratch=[pltpu.SemaphoreType.DMA((4,))],
+    )
     got = lax.all_to_all(pay, "y", 0, 0, tiled=True)
-    columns = call(spread_columns, shaped((4, 512, 256), bf16), columns, name="spread_columns")
+    pay, before, tail = call(
+        stage_y,
+        [shaped((4, PAY, 128), bf16), shaped((128, 128), f32), shaped((16, 128), f32)],
+        got, name="stage_y",
+    )
+    got = lax.all_to_all(pay, "zl", 0, 0, tiled=True)
+    columns, got, solved = lax.optimization_barrier((columns, got, solved))
+    columns = lax.all_to_all(columns, "y", 0, 0, tiled=True)
     y_map, y_local, pool_out = call(
         block_readings,
         [shaped((128, 128), bf16), shaped((3, 128, 128), f32), shaped((128, 128), bf16)],
         main, low, gate_output_weight, solved, hats, first, wide, lines, pooling_group_matrix,
         name="block_readings",
     )
-    pay, before, tail = call(
-        stage_y,
-        [shaped((4, PAY, 128), bf16), shaped((128, 128), f32), shaped((16, 128), f32)],
-        got, name="stage_y",
-    )
-    got = lax.all_to_all(pay, "zl", 0, 0, tiled=True)
-    columns, got, y_map = lax.optimization_barrier((columns, got, y_map))
-    columns = lax.all_to_all(columns, "y", 0, 0, tiled=True)
     pay, before, tail = call(
         stage_zl,
         [shaped((WIDE, 128), bf16), shaped((128, 128), f32), shaped((16, 128), f32)],

time: 127 us -> 129 us (1.016)
  blocking collectives: 99.9 us -> 108 us
  starting transfers between devices: 12 us -> 8.66 us
  waiting for transfers between devices: 2.85 us -> 0.01 us
    all_to_all x0 -> x1, blocking collectives: none -> 7.87 us  [on_device(): got = lax.all_to_all(pay, 'zl', 0, 0, tiled=True)]
    all_to_all x1 -> x0, starting transfers between devices: 3.33 us -> none  [on_device(): got = lax.all_to_all(pay, 'zl', 0, 0, tiled=True)]
    all_to_all x1 -> x0, waiting for transfers between devices: 2.84 us -> none  [on_device(): got = lax.all_to_all(pay, 'zl', 0, 0, tiled=True)]
    pallas_call x11 -> x10, Pallas kernels: 11 us -> 9.98 us  [call(): pl.pallas_call(kernel, out_shape=outs, in_specs=[pl.BlockSpec(memory_spac...]
  transfers between devices with their start and end apart: 3 -> 2, of which waited for: 1 -> 0; matrix products, arithmetic and copies ran while one was open for 0% -> 0% of each run, Pallas kernels for 2% -> 1%
where the time goes in v5:
time: 129 us; the launch traced here: 127 us
  blocking collectives  108 us (84%)
  Pallas kernels  9.98 us (8%)
  starting transfers between devices  8.66 us (7%)
    all_gather x1, blocking collectives, on_device(): gathered = lax.all_gather(shard, Z, axis=0, tiled=True)  35.1 us
    all_to_all x1, blocking collectives, on_device(): parts = lax.all_to_all(out.reshape(8, 16, 2048), TP, 0, 0, tiled=True)  17.6 us
    all_gather x1, blocking collectives, on_device(): got = lax.all_gather(pay, 'zh', axis=0)  16.6 us
    all_to_all x1, blocking collectives, on_device(): parts = lax.all_to_all(parts, 'y', 0, 0, tiled=True)  12.5 us
    all_gather x1, blocking collectives, on_device(): low = lax.all_gather(low, 'c', axis=0)  11.1 us
    pallas_call x10, Pallas kernels, call(): pl.pallas_call(kernel, out_shape=outs, in_specs=[pl.BlockSpec(memory_spac...  9.98 us
    all_to_all x1, blocking collectives, on_device(): got = lax.all_to_all(pay, 'zl', 0, 0, tiled=True)  7.87 us
    all_to_all x1, blocking collectives, on_device(): got = lax.all_to_all(pay, 'y', 0, 0, tiled=True)  7.26 us
  transfers between devices with their start and end apart: 2, of which 0 were waited for; matrix products, arithmetic and copies ran while one was open for 0% of the time, Pallas kernels for 1%

profile of v5, /device:TPU:1, one launch (start us, length us, event | category | flops | bytes accessed | tf_op | source)
XLA Modules:
  0.0 127.5 jit_solution(3328205813274855649)
XLA Ops:
  0.0 2.7 %prepare_tokens.1 = (bf16[4,128,512]{2,1,0:T(8,128)(2,1)}, f32[8,128]{1,0:T(8,128)}) custom-call(bf16[128,2048]{1,0:T(8,128)(2,1)} %tok_hbm.1, f32[1,2048]{1,0:T(1,128)} %bitcast.23, f32[1,2048]{1,0:T(1,128)} %bitcast.24, f32[1,128]{1,0:T(1,128)} %bitcast.25, f32[1,128]{1,0:T(1,128)} %bitcast.26, f32[1,128]{1,0:T(1,128)} %bitcast.27, f32[1,128]{1,0:T(1,128)} %bitcast.28, ...), custom_call_target="tpu_custom_call" | custom-call | flops 100000000 | bytes 544768 | tf_op jit(solution)/shard_map/prepare_tokens/pallas_call | solution.py:73
  2.7 0.0 copy-start.8
  2.7 0.0 copy-start.9
  2.7 0.0 copy-start.10
  2.7 0.0 copy-start.11
  2.7 0.0 copy-start.12
  2.7 0.0 copy-start.13
  2.8 0.0 copy-start.14
  2.8 0.0 copy-start.15
  2.8 0.0 copy-start.16
  2.8 5.1 %all-to-all-start = ((bf16[4,128,512]{2,1,0:T(8,128)(2,1)}), bf16[4,128,512]{2,1,0:T(8,128)(2,1)S(1)}, u32[]{:S(2)}, u32[]{:S(2)}) async-start(bf16[4,128,512]{2,1,0:T(8,128)(2,1)} %get-tuple-element.32), calls=%async_computation | async-start | bytes 1048576 | tf_op jit(solution)/shard_map/all_to_all | solution.py:470
  7.9 0.0 copy-done.8
  7.9 0.0 copy-done.9
  7.9 0.0 copy-done.10
  7.9 0.0 copy-done.11
  8.0 0.0 copy-done.12
  8.0 0.0 copy-done.13
  8.0 0.0 copy-done.14
  8.0 0.0 copy-done.15
  8.0 0.0 copy-done.16
  8.0 0.1 prepare_weights.1
  8.1 0.0 copy-start.7
  8.1 35.1 %all_gather.15.w_ref = bf16[512,1023]{1,0:T(8,128)(2,1)S(1)} all-gather(bf16[32,1023]{1,0:T(8,128)(2,1)S(1)} %get-tuple-element.33), channel_id=1, replica_groups=mesh['zh'=4,'zl'=4,'y'=4,'x'=4,'c'=2] {'zh','zl'}, dimensions={0}, use_global_device_ids=true | all-gather | bytes 1113024 | tf_op jit(solution)/shard_map/all_gather | solution.py:469
  43.2 0.0 all-to-all-done
  43.2 0.0 copy-done.7
  43.2 0.6 partial_products.1
  43.8 12.5 %all_to_all.30.part_ref = bf16[4,128,768]{2,1,0:T(8,128)(2,1)S(1)} all-to-all(bf16[4,128,768]{2,1,0:T(8,128)(2,1)S(1)} %get-tuple-element.35), channel_id=1, replica_groups=mesh['zh'=4,'zl'=4,'y'=4,'x'=4,'c'=2] {'y'}, dimensions={0} | all-to-all | bytes 1572864 | tf_op jit(solution)/shard_map/all_to_all | solution.py:476
  56.3 0.1 sum_parts.1
  56.5 0.0 copy-start.1
  56.5 0.0 copy-start.2
  56.5 0.0 copy-start.5
  56.5 0.0 copy-start.6
  56.5 11.1 %all-gather = bf16[256,256]{1,0:T(8,128)(2,1)S(1)} all-gather(bf16[128,256]{1,0:T(8,128)(2,1)S(1)} %get-tuple-element.37), channel_id=2, replica_groups=mesh['zh'=4,'zl'=4,'y'=4,'x'=4,'c'=2] {'c'}, dimensions={0}, use_global_device_ids=true | all-gather | bytes 196608 | tf_op jit(solution)/shard_map/all_gather | solution.py:480
  67.6 0.0 copy-done.1
  67.6 0.0 copy-done.2
  67.6 0.0 copy-done.5
  67.6 0.0 copy-done.6
  67.7 3.2 %block_maps.1 = (bf16[4,144,128]{2,1,0:T(8,128)(2,1)S(1)}, bf16[2,128,128]{2,1,0:T(8,128)(2,1)S(1)}, bf16[3,128,128]{2,1,0:T(8,128)(2,1)S(1)}, bf16[128,128]{1,0...) custom-call(bf16[128,512]{1,0:T(8,128)(2,1)S(1)} %get-tuple-element.36.main_ref, ...), custom_call_target="tpu_custom_call" | custom-call | flops 100000000 | bytes 733184 | tf_op jit(solution)/shard_map/block_maps/pallas_call | solution.py:73
  70.8 7.3 %all_to_all.31.got_ref = bf16[4,144,128]{2,1,0:T(8,128)(2,1)S(1)} all-to-all(bf16[4,144,128]{2,1,0:T(8,128)(2,1)S(1)} %get-tuple-element.42), channel_id=1, replica_groups=mesh['zh'=4,'zl'=4,'y'=4,'x'=4,'c'=2] {'y'}, dimensions={0} | all-to-all | bytes 294912 | tf_op jit(solution)/shard_map/all_to_all | solution.py:492
  78.1 0.3 stage_y.1
  78.4 7.9 %all_to_all.32.got_ref = bf16[4,144,128]{2,1,0:T(8,128)(2,1)S(1)} all-to-all(bf16[4,144,128]{2,1,0:T(8,128)(2,1)S(1)} %get-tuple-element.43), channel_id=1, replica_groups=mesh['zh'=4,'zl'=4,'y'=4,'x'=4,'c'=2] {'zl'}, dimensions={0} | all-to-all | bytes 294912 | tf_op jit(solution)/shard_map/all_to_all | solution.py:498
  86.3 3.5 %all-to-all-start.4 = ((bf16[4,512,256]{2,1,0:T(8,128)(2,1)}), bf16[4,512,256]{2,1,0:T(8,128)(2,1)S(1)}, u32[]{:S(2)}, u32[]{:S(2)}) async-start(bf16[4,512,256]{2,1,0:T(8,128)(2,1)} %get-tuple-element.58), calls=%async_computation.4 | async-start | bytes 2097152 | tf_op jit(solution)/shard_map/all_to_all | solution.py:500
  89.8 0.0 copy-start
  89.8 0.0 copy-start.4
  89.8 0.4 stage_zl.1
  90.2 0.4 copy-done
  90.6 0.1 copy-done.4
  90.7 0.7 block_readings.1
  91.4 0.0 copy-start.3
  91.4 16.6 %all-gather.1 = bf16[640,128]{1,0:T(8,128)(2,1)S(1)} all-gather(bf16[160,128]{1,0:T(8,128)(2,1)S(1)} %get-tuple-element.48), channel_id=3, replica_groups=mesh['zh'=4,'zl'=4,'y'=4,'x'=4,'c'=2] {'zh'}, dimensions={0}, use_global_device_ids=true | all-gather | bytes 204800 | tf_op jit(solution)/shard_map/all_gather | solution.py:512
  108.0 0.0 all-to-all-done.4.wout_ref
  108.0 0.0 copy-done.3
  108.0 1.2 finish.1
  109.2 17.6 %all_to_all.33.part_ref = bf16[8,16,2048]{2,1,0:T(8,128)(2,1)S(1)} all-to-all(bf16[8,16,2048]{2,1,0:T(8,128)(2,1)S(1)} %bitcast.17), channel_id=1, replica_groups=mesh['zh'=4,'zl'=4,'y'=4,'x'=4,'c'=2] {'x','c'}, dimensions={0} | all-to-all | bytes 1048576 | tf_op jit(solution)/shard_map/all_to_all | solution.py:518
  126.8 0.7 add_parts.1
Async XLA Ops:
  2.7 5.3 %copy-start.8 = (bf16[32,256]{1,0:T(8,128)(2,1)S(1)}, bf16[32,256]{1,0:T(8,128)(2,1)}, u32[]{:S(2)}) copy-start(bf16[32,256]{1,0:T(8,128)(2,1)} %g_ref.1) | copy-start | bytes 49156
  2.7 5.2 %copy-start.9 = (bf16[32,128]{1,0:T(8,128)(2,1)S(1)}, bf16[32,128]{1,0:T(8,128)(2,1)}, u32[]{:S(2)}) copy-start(bf16[32,128]{1,0:T(8,128)(2,1)} %q_ref.1) | copy-start | bytes 24580
  2.7 5.2 %copy-start.10 = (bf16[32,128]{1,0:T(8,128)(2,1)S(1)}, bf16[32,128]{1,0:T(8,128)(2,1)}, u32[]{:S(2)}) copy-start(bf16[32,128]{1,0:T(8,128)(2,1)} %k_ref.1) | copy-start | bytes 24580
  2.7 5.2 %copy-start.11 = (bf16[32,128]{1,0:T(8,128)(2,1)S(1)}, bf16[32,128]{1,0:T(8,128)(2,1)}, u32[]{:S(2)}) copy-start(bf16[32,128]{1,0:T(8,128)(2,1)} %v_ref.1) | copy-start | bytes 24580
  2.7 5.2 %copy-start.12 = (bf16[32,128]{1,0:T(8,128)(2,1)S(1)}, bf16[32,128]{1,0:T(8,128)(2,1)}, u32[]{:S(2)}) copy-start(bf16[32,128]{1,0:T(8,128)(2,1)} %p_ref.1) | copy-start | bytes 24580
  2.7 5.2 %copy-start.13 = (bf16[32,128]{1,0:T(8,128)(2,1)S(1)}, bf16[32,128]{1,0:T(8,128)(2,1)}, u32[]{:S(2)}) copy-start(bf16[32,128]{1,0:T(8,128)(2,1)} %d_ref.1) | copy-start | bytes 24580
  2.8 5.2 %copy-start.14 = (bf16[32,128]{1,0:T(8,128)(2,1)S(1)}, bf16[32,128]{1,0:T(8,128)(2,1)}, u32[]{:S(2)}) copy-start(bf16[32,128]{1,0:T(8,128)(2,1)} %r_ref.1) | copy-start | bytes 24580
  2.8 5.2 %copy-start.15 = (bf16[128,32]{0,1:T(8,128)(2,1)S(1)}, bf16[128,32]{0,1:T(8,128)(2,1)}, u32[]{:S(2)}) copy-start(bf16[128,32]{0,1:T(8,128)(2,1)} %param.52) | copy-start | bytes 24580
  2.8 5.2 %copy-start.16 = (bf16[128,32]{0,1:T(8,128)(2,1)S(1)}, bf16[128,32]{0,1:T(8,128)(2,1)}, u32[]{:S(2)}) copy-start(bf16[128,32]{0,1:T(8,128)(2,1)} %param.53) | copy-start | bytes 24580
  2.8 40.4 %all-to-all-start = ((bf16[4,128,512]{2,1,0:T(8,128)(2,1)}), bf16[4,128,512]{2,1,0:T(8,128)(2,1)S(1)}, u32[]{:S(2)}, u32[]{:S(2)}) async-start(bf16[4,128,512]{2,1,0:T(8,128)(2,1)} %get-tuple-element.32), calls=%async_computation | async-start | bytes 1048576 | tf_op jit(solution)/shard_map/all_to_all | solution.py:470
  8.1 35.1 %copy-start.7 = (f32[8,128]{1,0:T(8,128)S(1)}, f32[8,128]{1,0:T(8,128)}, u32[]{:S(2)}) copy-start(f32[8,128]{1,0:T(8,128)} %get-tuple-element.34.lines_ref) | copy-start | bytes 12292
  56.5 11.2 %copy-start.1 = (f32[128,128]{1,0:T(8,128)S(1)}, f32[128,128]{1,0:T(8,128)}, u32[]{:S(2)}) copy-start(f32[128,128]{1,0:T(8,128)} %re_ref.1) | copy-start | bytes 196612
  56.5 11.2 %copy-start.2 = (f32[128,128]{1,0:T(8,128)S(1)}, f32[128,128]{1,0:T(8,128)}, u32[]{:S(2)}) copy-start(f32[128,128]{1,0:T(8,128)} %de_ref.1) | copy-start | bytes 196612
  56.5 11.2 %copy-start.5 = (bf16[128,128]{1,0:T(8,128)(2,1)S(1)}, bf16[128,128]{1,0:T(8,128)(2,1)}, u32[]{:S(2)}) copy-start(bf16[128,128]{1,0:T(8,128)(2,1)} %dw_ref.1) | copy-start | bytes 98308
  56.5 11.2 %copy-start.6 = (bf16[128,128]{1,0:T(8,128)(2,1)S(1)}, bf16[128,128]{1,0:T(8,128)(2,1)}, u32[]{:S(2)}) copy-start(bf16[128,128]{1,0:T(8,128)(2,1)} %rw_ref.1) | copy-start | bytes 98308
  86.3 21.7 %all-to-all-start.4 = ((bf16[4,512,256]{2,1,0:T(8,128)(2,1)}), bf16[4,512,256]{2,1,0:T(8,128)(2,1)S(1)}, u32[]{:S(2)}, u32[]{:S(2)}) async-start(bf16[4,512,256]{2,1,0:T(8,128)(2,1)} %get-tuple-element.58), calls=%async_computation.4 | async-start | bytes 2097152 | tf_op jit(solution)/shard_map/all_to_all | solution.py:500
  89.8 0.8 copy-start
  89.8 0.8 copy-start.4
  91.4 16.6 %copy-start.3 = (f32[2,64,64]{2,1,0:T(8,128)S(1)}, f32[2,64,64]{2,1,0:T(8,128)}, u32[]{:S(2)}) copy-start(f32[2,64,64]{2,1,0:T(8,128)} %start_ref.1) | copy-start | bytes 98308

commit v6 on v4

--- a/solution.py
+++ b/solution.py
@@ -231,14 +231,16 @@
     for _ in range(2):
         power = [mm_wide(power[h], power[h]) for h in range(2)]
         product = [product[h] + mm_wide(product[h], power[h]) for h in range(2)]
-    for here in (within[16] & ~within[8], within[32] & ~within[16], ~within[32]):
+    for here in (within[16] & ~within[8], within[32] & ~within[16]):
         mid = [mm_wide(product[h], jnp.where(here, full[h], 0.0)) for h in range(2)]
         product = [product[h] + mm_wide(mid[h], product[h]) for h in range(2)]
     solved = []
     for h in range(2):
         pushed = mm(jnp.where(strict, scores[h * ROWS : h * ROWS + ROWS, ROWS:], 0.0), values_b)
         rhs = jnp.where(lane_low if h == 0 else ~lane_low, pushed, swapped)
-        solved.append(mm(product[h], rhs).astype(bf16))
+        part = mm(product[h], rhs)
+        across = jnp.where(within[32], 0.0, full[h])
+        solved.append((part + mm(product[h], mm(across, part))).astype(bf16))
         solved_ref[h] = solved[h]
 
     b_end = (b_hat * base).astype(bf16)

time: 127 us -> 127 us (level)
  no operation moved by 1% of the time
where the time goes in v6:
time: 127 us; the launch traced here: 126 us
  blocking collectives  99.8 us (79%)
  starting transfers between devices  12 us (9%)
  Pallas kernels  11.3 us (9%)
  waiting for transfers between devices  2.85 us (2%)
    all_gather x1, blocking collectives, on_device(): gathered = lax.all_gather(shard, Z, axis=0, tiled=True)  35.1 us
    all_to_all x1, blocking collectives, on_device(): parts = lax.all_to_all(out.reshape(8, 16, 2048), TP, 0, 0, tiled=True)  18.3 us
    all_gather x1, blocking collectives, on_device(): got = lax.all_gather(pay, 'zh', axis=0)  15.6 us
    all_to_all x1, blocking collectives, on_device(): parts = lax.all_to_all(parts, 'y', 0, 0, tiled=True)  12.5 us
    pallas_call x11, Pallas kernels, call(): pl.pallas_call(kernel, out_shape=outs, in_specs=[pl.BlockSpec(memory_spac...  11.3 us
    all_gather x1, blocking collectives, on_device(): low = lax.all_gather(low, 'c', axis=0)  11.1 us
    all_to_all x1, blocking collectives, on_device(): got = lax.all_to_all(pay, 'y', 0, 0, tiled=True)  7.26 us
    all_to_all x1, starting transfers between devices, on_device(): mixed_tokens = lax.all_to_all(sent, 'y', 0, 0, tiled=True).reshape(512, 512)  5.15 us
  transfers between devices with their start and end apart: 3, of which 1 were waited for; matrix products, arithmetic and copies ran while one was open for 0% of the time, Pallas kernels for 2%

profile of v6, /device:TPU:1, one launch (start us, length us, event | category | flops | bytes accessed | tf_op | source)
XLA Modules:
  0.0 126.4 jit_solution(17276716495942494931)
XLA Ops:
  0.0 2.7 %prepare_tokens.1 = (bf16[4,128,512]{2,1,0:T(8,128)(2,1)}, f32[8,128]{1,0:T(8,128)}) custom-call(bf16[128,2048]{1,0:T(8,128)(2,1)} %tok_hbm.1, f32[1,2048]{1,0:T(1,128)} %bitcast.23, f32[1,2048]{1,0:T(1,128)} %bitcast.24, f32[1,128]{1,0:T(1,128)} %bitcast.25, f32[1,128]{1,0:T(1,128)} %bitcast.26, f32[1,128]{1,0:T(1,128)} %bitcast.27, f32[1,128]{1,0:T(1,128)} %bitcast.28, ...), custom_call_target="tpu_custom_call" | custom-call | flops 100000000 | bytes 544768 | tf_op jit(solution)/shard_map/prepare_tokens/pallas_call | solution.py:73
  2.7 0.0 copy-start.8
  2.7 0.0 copy-start.9
  2.7 0.0 copy-start.10
  2.7 0.0 copy-start.11
  2.7 0.0 copy-start.12
  2.8 0.0 copy-start.13
  2.8 0.0 copy-start.14
  2.8 0.0 copy-start.15
  2.8 0.0 copy-start.16
  2.8 5.1 %all-to-all-start = ((bf16[4,128,512]{2,1,0:T(8,128)(2,1)}), bf16[4,128,512]{2,1,0:T(8,128)(2,1)S(1)}, u32[]{:S(2)}, u32[]{:S(2)}) async-start(bf16[4,128,512]{2,1,0:T(8,128)(2,1)} %get-tuple-element.33), calls=%async_computation | async-start | bytes 1048576 | tf_op jit(solution)/shard_map/all_to_all | solution.py:472
  7.9 0.0 copy-done.8
  8.0 0.0 copy-done.9
  8.0 0.0 copy-done.10
  8.0 0.0 copy-done.11
  8.0 0.0 copy-done.12
  8.0 0.0 copy-done.13
  8.0 0.0 copy-done.14
  8.0 0.0 copy-done.15
  8.0 0.0 copy-done.16
  8.0 0.1 prepare_weights.1
  8.1 0.0 copy-start.7
  8.1 35.1 %all_gather.15.w_ref = bf16[512,1023]{1,0:T(8,128)(2,1)S(1)} all-gather(bf16[32,1023]{1,0:T(8,128)(2,1)S(1)} %get-tuple-element.32), channel_id=1, replica_groups=mesh['zh'=4,'zl'=4,'y'=4,'x'=4,'c'=2] {'zh','zl'}, dimensions={0}, use_global_device_ids=true | all-gather | bytes 1113024 | tf_op jit(solution)/shard_map/all_gather | solution.py:471
  43.2 0.0 all-to-all-done
  43.2 0.0 copy-done.7
  43.2 0.6 partial_products.1
  43.8 12.5 %all_to_all.30.part_ref = bf16[4,128,768]{2,1,0:T(8,128)(2,1)S(1)} all-to-all(bf16[4,128,768]{2,1,0:T(8,128)(2,1)S(1)} %get-tuple-element.35), channel_id=1, replica_groups=mesh['zh'=4,'zl'=4,'y'=4,'x'=4,'c'=2] {'y'}, dimensions={0} | all-to-all | bytes 1572864 | tf_op jit(solution)/shard_map/all_to_all | solution.py:477
  56.3 0.1 sum_parts.1
  56.4 0.0 copy-start.1
  56.4 0.0 copy-start.2
  56.4 0.0 copy-start.5
  56.4 0.0 copy-start.6
  56.5 11.1 %all-gather = bf16[256,256]{1,0:T(8,128)(2,1)S(1)} all-gather(bf16[128,256]{1,0:T(8,128)(2,1)S(1)} %get-tuple-element.37), channel_id=2, replica_groups=mesh['zh'=4,'zl'=4,'y'=4,'x'=4,'c'=2] {'c'}, dimensions={0}, use_global_device_ids=true | all-gather | bytes 196608 | tf_op jit(solution)/shard_map/all_gather | solution.py:481
  67.6 0.0 copy-done.1
  67.6 0.0 copy-done.2
  67.6 0.0 copy-done.5
  67.6 0.0 copy-done.6
  67.6 2.7 %block_maps.1 = (bf16[4,144,128]{2,1,0:T(8,128)(2,1)S(1)}, bf16[2,128,128]{2,1,0:T(8,128)(2,1)S(1)}, bf16[3,128,128]{2,1,0:T(8,128)(2,1)S(1)}, bf16[128,128]{1,0:T(8,128)(2,1)S(1)}, f32[2,128,128]{2,1,0:T(8,128)S(1)}) custom-call(bf16[128,512]{1,0:T(8,128)(2,1)S(1)} %get-tuple-element.36.main_ref, bf16[2,128,256]{2,1,0:T(8,128)(2,1)S(1)} %bitcast.18, ...), custom_call_target="tpu_custom_call" | custom-call | flops 100000000 | bytes 471040 | tf_op jit(solution)/shard_map/block_maps/pallas_call | solution.py:73
  70.4 7.3 %all_to_all.31.got_ref = bf16[4,144,128]{2,1,0:T(8,128)(2,1)S(1)} all-to-all(bf16[4,144,128]{2,1,0:T(8,128)(2,1)S(1)} %get-tuple-element.42), channel_id=1, replica_groups=mesh['zh'=4,'zl'=4,'y'=4,'x'=4,'c'=2] {'y'}, dimensions={0} | all-to-all | bytes 294912 | tf_op jit(solution)/shard_map/all_to_all | solution.py:492
  77.6 0.9 stage_y.1
  78.6 3.3 %all-to-all-start.3 = ((bf16[4,144,128]{2,1,0:T(8,128)(2,1)}), bf16[4,144,128]{2,1,0:T(8,128)(2,1)S(1)}, u32[]{:S(2)}, u32[]{:S(2)}) async-start(bf16[4,144,128]{2,1,0:T(8,128)(2,1)} %get-tuple-element.43), calls=%async_computation.3 | async-start | bytes 294912 | tf_op jit(solution)/shard_map/all_to_all | solution.py:505
  81.9 0.0 copy-start
  81.9 0.0 copy-start.4
  81.9 1.2 spread_columns.1
  83.1 0.0 copy-done
  83.1 0.0 copy-done.4
  83.1 0.7 block_readings.1
  83.9 2.8 %all-to-all-done.3.got_ref = bf16[4,144,128]{2,1,0:T(8,128)(2,1)S(1)} async-done(((bf16[4,144,128]{2,1,0:T(8,128)(2,1)}), bf16[4,144,128]{2,1,0:T(8,128)(2,1)S(1)}, u32[]{:S(2)}, u32[]{:S(2)}) %all-to-all-start.3) | async-done | bytes 147488 | tf_op jit(solution)/shard_map/all_to_all | solution.py:505
  86.7 3.5 %all-to-all-start.4 = ((bf16[4,512,256]{2,1,0:T(8,128)(2,1)}), bf16[4,512,256]{2,1,0:T(8,128)(2,1)S(1)}, u32[]{:S(2)}, u32[]{:S(2)}) async-start(bf16[4,512,256]{2,1,0:T(8,128)(2,1)} %spread_columns.1), calls=%async_computation.4 | async-start | bytes 2097152 | tf_op jit(solution)/shard_map/all_to_all | solution.py:507
  90.2 0.4 stage_zl.1
  90.6 0.0 copy-start.3
  90.6 15.6 %all-gather.1 = bf16[640,128]{1,0:T(8,128)(2,1)S(1)} all-gather(bf16[160,128]{1,0:T(8,128)(2,1)S(1)} %get-tuple-element.52), channel_id=3, replica_groups=mesh['zh'=4,'zl'=4,'y'=4,'x'=4,'c'=2] {'zh'}, dimensions={0}, use_global_device_ids=true | all-gather | bytes 204800 | tf_op jit(solution)/shard_map/all_gather | solution.py:513
  106.2 0.0 all-to-all-done.4.wout_ref
  106.2 0.0 copy-done.3
  106.2 1.2 finish.1
  107.4 18.3 %all_to_all.32.part_ref = bf16[8,16,2048]{2,1,0:T(8,128)(2,1)S(1)} all-to-all(bf16[8,16,2048]{2,1,0:T(8,128)(2,1)S(1)} %bitcast.17), channel_id=1, replica_groups=mesh['zh'=4,'zl'=4,'y'=4,'x'=4,'c'=2] {'x','c'}, dimensions={0} | all-to-all | bytes 1048576 | tf_op jit(solution)/shard_map/all_to_all | solution.py:519
  125.7 0.7 add_parts.1
Async XLA Ops:
  2.7 5.3 %copy-start.8 = (bf16[32,256]{1,0:T(8,128)(2,1)S(1)}, bf16[32,256]{1,0:T(8,128)(2,1)}, u32[]{:S(2)}) copy-start(bf16[32,256]{1,0:T(8,128)(2,1)} %g_ref.1) | copy-start | bytes 49156
  2.7 5.2 %copy-start.9 = (bf16[32,128]{1,0:T(8,128)(2,1)S(1)}, bf16[32,128]{1,0:T(8,128)(2,1)}, u32[]{:S(2)}) copy-start(bf16[32,128]{1,0:T(8,128)(2,1)} %q_ref.1) | copy-start | bytes 24580
  2.7 5.2 %copy-start.10 = (bf16[32,128]{1,0:T(8,128)(2,1)S(1)}, bf16[32,128]{1,0:T(8,128)(2,1)}, u32[]{:S(2)}) copy-start(bf16[32,128]{1,0:T(8,128)(2,1)} %k_ref.1) | copy-start | bytes 24580
  2.7 5.2 %copy-start.11 = (bf16[32,128]{1,0:T(8,128)(2,1)S(1)}, bf16[32,128]{1,0:T(8,128)(2,1)}, u32[]{:S(2)}) copy-start(bf16[32,128]{1,0:T(8,128)(2,1)} %v_ref.1) | copy-start | bytes 24580
  2.7 5.2 %copy-start.12 = (bf16[32,128]{1,0:T(8,128)(2,1)S(1)}, bf16[32,128]{1,0:T(8,128)(2,1)}, u32[]{:S(2)}) copy-start(bf16[32,128]{1,0:T(8,128)(2,1)} %p_ref.1) | copy-start | bytes 24580
  2.8 5.2 %copy-start.13 = (bf16[32,128]{1,0:T(8,128)(2,1)S(1)}, bf16[32,128]{1,0:T(8,128)(2,1)}, u32[]{:S(2)}) copy-start(bf16[32,128]{1,0:T(8,128)(2,1)} %d_ref.1) | copy-start | bytes 24580
  2.8 5.2 %copy-start.14 = (bf16[32,128]{1,0:T(8,128)(2,1)S(1)}, bf16[32,128]{1,0:T(8,128)(2,1)}, u32[]{:S(2)}) copy-start(bf16[32,128]{1,0:T(8,128)(2,1)} %r_ref.1) | copy-start | bytes 24580
  2.8 5.2 %copy-start.15 = (bf16[128,32]{0,1:T(8,128)(2,1)S(1)}, bf16[128,32]{0,1:T(8,128)(2,1)}, u32[]{:S(2)}) copy-start(bf16[128,32]{0,1:T(8,128)(2,1)} %param.52) | copy-start | bytes 24580
  2.8 5.2 %copy-start.16 = (bf16[128,32]{0,1:T(8,128)(2,1)S(1)}, bf16[128,32]{0,1:T(8,128)(2,1)}, u32[]{:S(2)}) copy-start(bf16[128,32]{0,1:T(8,128)(2,1)} %param.53) | copy-start | bytes 24580
  2.8 40.4 %all-to-all-start = ((bf16[4,128,512]{2,1,0:T(8,128)(2,1)}), bf16[4,128,512]{2,1,0:T(8,128)(2,1)S(1)}, u32[]{:S(2)}, u32[]{:S(2)}) async-start(bf16[4,128,512]{2,1,0:T(8,128)(2,1)} %get-tuple-element.33), calls=%async_computation | async-start | bytes 1048576 | tf_op jit(solution)/shard_map/all_to_all | solution.py:472
  8.1 35.1 %copy-start.7 = (f32[8,128]{1,0:T(8,128)S(1)}, f32[8,128]{1,0:T(8,128)}, u32[]{:S(2)}) copy-start(f32[8,128]{1,0:T(8,128)} %get-tuple-element.34.lines_ref) | copy-start | bytes 12292
  56.4 11.2 %copy-start.1 = (f32[128,128]{1,0:T(8,128)S(1)}, f32[128,128]{1,0:T(8,128)}, u32[]{:S(2)}) copy-start(f32[128,128]{1,0:T(8,128)} %re_ref.1) | copy-start | bytes 196612
  56.4 11.2 %copy-start.2 = (f32[128,128]{1,0:T(8,128)S(1)}, f32[128,128]{1,0:T(8,128)}, u32[]{:S(2)}) copy-start(f32[128,128]{1,0:T(8,128)} %de_ref.1) | copy-start | bytes 196612
  56.4 11.2 %copy-start.5 = (bf16[128,128]{1,0:T(8,128)(2,1)S(1)}, bf16[128,128]{1,0:T(8,128)(2,1)}, u32[]{:S(2)}) copy-start(bf16[128,128]{1,0:T(8,128)(2,1)} %dw_ref.1) | copy-start | bytes 98308
  56.4 11.2 %copy-start.6 = (bf16[128,128]{1,0:T(8,128)(2,1)S(1)}, bf16[128,128]{1,0:T(8,128)(2,1)}, u32[]{:S(2)}) copy-start(bf16[128,128]{1,0:T(8,128)(2,1)} %rw_ref.1) | copy-start | bytes 98308
  78.6 8.1 %all-to-all-start.3 = ((bf16[4,144,128]{2,1,0:T(8,128)(2,1)}), bf16[4,144,128]{2,1,0:T(8,128)(2,1)S(1)}, u32[]{:S(2)}, u32[]{:S(2)}) async-start(bf16[4,144,128]{2,1,0:T(8,128)(2,1)} %get-tuple-element.43), calls=%async_computation.3 | async-start | bytes 294912 | tf_op jit(solution)/shard_map/all_to_all | solution.py:505
  81.9 1.2 copy-start
  81.9 1.2 copy-start.4
  86.7 19.5 %all-to-all-start.4 = ((bf16[4,512,256]{2,1,0:T(8,128)(2,1)}), bf16[4,512,256]{2,1,0:T(8,128)(2,1)S(1)}, u32[]{:S(2)}, u32[]{:S(2)}) async-start(bf16[4,512,256]{2,1,0:T(8,128)(2,1)} %spread_columns.1), calls=%async_computation.4 | async-start | bytes 2097152 | tf_op jit(solution)/shard_map/all_to_all | solution.py:507
  90.6 15.6 %copy-start.3 = (f32[2,64,64]{2,1,0:T(8,128)S(1)}, f32[2,64,64]{2,1,0:T(8,128)}, u32[]{:S(2)}) copy-start(f32[2,64,64]{2,1,0:T(8,128)} %start_ref.1) | copy-start | bytes 98308
